TPU v7x, 128 devices: a whole 4x4x4 slice. The times are simulated.
128 devices in a mesh: sp: 16 (over z, x), tp: 8 (over y, core).
Axes of the slice: x: 4, y: 4, z: 4, core: 2. Of those that a mesh axis runs over, the one named last changes fastest.
Arguments:
- inputs: bfloat16 [16384, 2048], P('sp'), may hold values from -9 to 9
- w_query: bfloat16 [2048, 1024], P(None, 'tp'), may hold values from -0.15692044 to 0.15692044
- w_key: bfloat16 [2048, 1024], P(None, 'tp'), may hold values from -0.15692044 to 0.15692044
- w_value: bfloat16 [2048, 1024], P(None, 'tp'), may hold values from -0.125 to 0.125
- w_glu_value: bfloat16 [2048, 1024], P(None, 'tp'), may hold values from -0.37565048 to 0.37565048
- w_glu_gate: bfloat16 [2048, 1024], P(None, 'tp'), may hold values from -0.125 to 0.125
- conv_taps: float32 [31, 1024], P(None, 'tp'), may hold values from -4 to 4
- conv_gain: float32 [1024], P('tp'), may hold values from 0.1 to 1.9
- log_forget: float32 [16384, 8], P('sp', 'tp'), may hold values from -16384 to 0, as said below
- w_out: bfloat16 [2048, 2048], replicated, may hold values from -0.125 to 0.125
Outputs:
- result: bfloat16 [16384, 2048], P(('sp', 'tp'))
Inputs may be any that keep to these rules, and one draw needn't show every extreme that they name: `log_forget`: for each head, non-increasing along positions and at most zero.
All inputs are finite; a program needn't handle non-finite values.
Results may differ from a plain program's by a relative error of at most 0.014.
Values may be sent and summed in bfloat16 or wider, within the bound.
No kernel may reach another device: no remote copies, remote signals or barrier semaphores. Data moves between devices by JAX's collectives and lax.ppermute only.
A program may use at most 128 MiB of HBM per device.

v0:
```python
import math

import jax
import jax.numpy as jnp
from jax import lax
from jax.sharding import PartitionSpec as P

HEAD_DIM = 128


NORM_EPS = 1e-05


def passed_along(value, axis, steps):
    count = lax.axis_size(axis)
    leading, last = (max(0, -steps), min(count, count - steps))
    return lax.ppermute(value, axis, [(source, source + steps) for source in range(leading, last)])


def from_everyone(shard, axis):
    length = lax.axis_size(axis)
    return lax.all_to_all(
        jnp.broadcast_to(shard[None], (length, *shard.shape)), axis, 0, 0, tiled=True
    )


def over_copies(shard, axis):
    everything = from_everyone(shard, axis)
    return jnp.sum(everything, axis=0)


def packed_total(arrays, axis):
    ends = [0]
    for a in arrays:
        ends.append(ends[-1] + a.size)
    running = over_copies(jnp.concatenate([a.ravel() for a in arrays]), axis)
    return tuple((running[b:e].reshape(a.shape) for a, b, e in zip(arrays, ends, ends[1:])))


def in_order(parts, dim):
    lengths = list(parts.shape[1:])
    lengths[dim] *= parts.shape[0]
    return jnp.moveaxis(parts, 0, dim).reshape(lengths)


def collect(shard, axis, dim):
    return in_order(from_everyone(shard, axis), dim)


def in_one_piece(arrays, axis, dim, along):
    both = jnp.concatenate(arrays, axis=along)
    result, at, gathered = (lax.all_gather(both, axis, axis=dim, tiled=True), 0, [])
    for a in arrays:
        gathered.append(lax.slice_in_dim(result, at, at + a.shape[along], axis=along))
        at += a.shape[along]
    return tuple(gathered)


def on_device(
    inputs,
    w_query,
    w_key,
    w_value,
    w_glu_value,
    w_glu_gate,
    conv_taps,
    conv_gain,
    log_forget,
    w_out,
):
    tok_rows = inputs.shape[0]
    channels = w_glu_value.shape[1]
    heads_here = w_query.shape[1] // HEAD_DIM
    attn_width = heads_here * HEAD_DIM
    tp_count = lax.axis_size("tp")
    total_channels = channels * tp_count
    row_start = lax.axis_index("sp") * tok_rows
    last_row = row_start + tok_rows - 1
    glu_value = jnp.dot(inputs, w_glu_value, preferred_element_type=jnp.float32)
    glu_gate = jnp.dot(inputs, w_glu_gate, preferred_element_type=jnp.float32)
    gated = (glu_value * jax.nn.sigmoid(glu_gate)).astype(jnp.bfloat16)
    kernel = conv_taps.shape[0]
    halo_rows = passed_along(gated[tok_rows - (kernel - 1) :], "sp", 1)
    padded = jnp.concatenate([halo_rows, gated], axis=0).astype(jnp.float32)
    conv_sum = jnp.zeros((tok_rows, channels), jnp.float32)
    for offset in range(kernel):
        conv_sum = conv_sum + conv_taps[offset] * padded[offset : offset + tok_rows]
    plain_sums, squares = packed_total(
        (jnp.sum(conv_sum, axis=1), jnp.sum(conv_sum * conv_sum, axis=1)), "tp"
    )
    mean_value = plain_sums / total_channels
    spread = squares / total_channels - mean_value * mean_value
    centered = conv_sum - mean_value[:, None]
    conv_rows = jax.nn.silu(centered * lax.rsqrt(spread + NORM_EPS)[:, None] * conv_gain).astype(
        jnp.bfloat16
    )
    query_rows = jnp.dot(inputs, w_query, preferred_element_type=jnp.float32).astype(jnp.bfloat16)
    key_rows = jnp.dot(inputs, w_key, preferred_element_type=jnp.float32).astype(jnp.bfloat16)
    value_rows = jnp.dot(inputs, w_value, preferred_element_type=jnp.float32).astype(jnp.bfloat16)
    query_heads = query_rows.reshape(tok_rows, heads_here, HEAD_DIM)
    own_gates = jnp.transpose(log_forget)
    gates_all = collect(log_forget, "sp", 0)
    score_scale = HEAD_DIM ** (-0.5)
    query_pos = row_start + jnp.arange(tok_rows, dtype=jnp.int32)
    start_state = (
        jnp.full((heads_here, tok_rows), -1e30, jnp.float32),
        jnp.zeros((heads_here, tok_rows), jnp.float32),
        jnp.zeros((heads_here, tok_rows, HEAD_DIM), jnp.float32),
    )
    piece_keys, piece_values = in_one_piece((key_rows, value_rows), "sp", 0, 1)
    block_rows = math.gcd(piece_keys.shape[0], tok_rows)
    shards = piece_keys.shape[0] // block_rows
    key_iota = jnp.arange(block_rows, dtype=jnp.int32)

    def one_shard(shard_number, carried_state):
        offset = shard_number * block_rows
        key_first = offset

        def attend(state_in):
            running_max, running_sum, running_out = state_in
            shard_keys = lax.dynamic_slice_in_dim(piece_keys, offset, block_rows, 0).reshape(
                block_rows, heads_here, HEAD_DIM
            )
            shard_values = lax.dynamic_slice_in_dim(piece_values, offset, block_rows, 0).reshape(
                block_rows, heads_here, HEAD_DIM
            )
            shard_gates = jnp.transpose(
                lax.dynamic_slice_in_dim(gates_all, key_first, block_rows, 0)
            )
            scores = (
                jnp.einsum(
                    "qhd,khd->hqk", query_heads, shard_keys, preferred_element_type=jnp.float32
                )
                * score_scale
            )
            scores = scores + own_gates[:, :, None] - shard_gates[:, None, :]
            allowed = ((key_first + key_iota)[None, :] <= query_pos[:, None])[None]
            masked = jnp.where(allowed, scores, -1e30)
            new_max = jnp.maximum(running_max, jnp.max(masked, axis=2))
            weights = jnp.where(allowed, jnp.exp(masked - new_max[:, :, None]), 0.0)
            rescale = jnp.exp(running_max - new_max)
            new_sum = running_sum * rescale + jnp.sum(weights, axis=2)
            mixture = jnp.einsum(
                "hqk,khd->hqd",
                weights.astype(jnp.bfloat16),
                shard_values,
                preferred_element_type=jnp.float32,
            )
            new_out = running_out * rescale[:, :, None] + mixture
            return (new_max, new_sum, new_out)

        def keep_state(state_in):
            return state_in

        return lax.cond(key_first <= last_row, attend, keep_state, carried_state)

    final_max, final_sum, final_out = lax.fori_loop(0, shards, one_shard, start_state)
    attn_heads = (final_out / final_sum[:, :, None]).astype(jnp.bfloat16)
    attn_rows = jnp.transpose(attn_heads, (1, 0, 2)).reshape(tok_rows, attn_width)
    conv_mine, attn_mine = (
        lax.all_to_all(conv_rows, "tp", split_axis=0, concat_axis=1, tiled=True),
        lax.all_to_all(attn_rows, "tp", split_axis=0, concat_axis=1, tiled=True),
    )
    projected = jnp.dot(conv_mine, w_out[:total_channels], preferred_element_type=jnp.float32)
    projected = projected + jnp.dot(
        attn_mine, w_out[total_channels:], preferred_element_type=jnp.float32
    )
    result = projected.astype(jnp.bfloat16)
    return result


def solution(mesh):
    in_specs = (
        P("sp", None),
        P(None, "tp"),
        P(None, "tp"),
        P(None, "tp"),
        P(None, "tp"),
        P(None, "tp"),
        P(None, "tp"),
        P("tp"),
        P("sp", "tp"),
        P(),
    )
    out_specs = P(("sp", "tp"), None)
    return jax.shard_map(
        on_device, mesh=mesh, in_specs=in_specs, out_specs=out_specs, check_vma=False
    )
```

profile of v0, /device:TPU:102, one launch (start us, length us, event | category | flops | bytes accessed | tf_op | source)
XLA Modules:
  0.0 225.7 jit_solution(10124119903688183234)
XLA Ops:
  27.5 4.5 %all-to-all-start = ((f32[8,1,2048]{2,1,0:T(1,128)}), f32[8,1,2048]{2,1,0:T(1,128)S(1)}, u32[]{:S(2)}, u32[]{:S(2)}) async-start(f32[8,1,2048]{2,1,0:T(1,128)} %broadcast_in_dim.19), calls=%async_computation | async-start | bytes 131072 | tf_op jit(solution)/shard_map/all_to_all | solution.py:22
  38.2 6.9 %all-to-all-start.2 = ((f32[16,1024,1]{1,2,0:T(1,128)}), f32[16,1024,1]{1,2,0:T(1,128)S(1)}, u32[]{:S(2)}, u32[]{:S(2)}) async-start(f32[16,1024,1]{1,2,0:T(1,128)} %broadcast_in_dim.44), calls=%async_computation.2 | async-start | bytes 131072 | tf_op jit(solution)/shard_map/all_to_all | solution.py:22
  45.2 38.9 %all-gather.2.cloned.1.call-done = bf16[16384,256]{0,1:T(8,128)(2,1)} async-done(((bf16[1024,256]{0,1:T(8,128)(2,1)}), bf16[16384,256]{0,1:T(8,128)(2,1)}) %all-gather.2.cloned.1.call-update) | async-done | bytes 8388624 | tf_op jit(solution)/shard_map/all_gather | solution.py:52
  84.1 5.8 %fusion.72 = (bf16[16384,128]{0,1:T(8,128)(2,1)}, bf16[16384,128]{0,1:T(8,128)(2,1)}) fusion(bf16[16384,256]{0,1:T(8,128)(2,1)} %all-gather.2.cloned.1.call-done), kind=kLoop, calls=%fused_computation.142 | loop fusion | bytes 16777216 | tf_op jit(solution)/shard_map/slice | solution.py:54
  89.9 6.4 %copy.31 = bf16[16384,128]{1,0:T(8,128)(2,1)} copy(bf16[16384,128]{0,1:T(8,128)(2,1)} %get-tuple-element.385) | data formatting | bytes 8388608
  96.3 6.4 %copy.32 = bf16[16384,128]{1,0:T(8,128)(2,1)} copy(bf16[16384,128]{0,1:T(8,128)(2,1)} %get-tuple-element.384) | data formatting | bytes 8388608
  102.8 88.8 %while.18 = (s32[]{:T(128)}, f32[1,1024]{1,0:T(1,128)S(1)}, f32[1,1024]{1,0:T(1,128)S(1)}, f32[1,1024,128]{2,1,0:T(8,128)S(1)}, s32[]{:T(128)}, /*index=5*/bf16[...) while((s32[]{:T(128)}, f32[1,1024]{1,0:T(1,128)S(1)}, ...), condition=%wide.region_8.9_spmd.clone, body=%wide.region_3.8_spmd.clone.sunk | while | flops 551817216 | bytes 14545253 | solution.py:157
  102.8 5.5 %conditional.3 = ((f32[1,1024]{1,0:T(1,128)S(1)}, f32[1,1024]{1,0:T(1,128)S(1)}, f32[1,1024,128]{2,1,0:T(8,128)S(1)})) conditional(s32[]{:T(128)} %convert_element_type.61, (f32[1,1024]{1,0:T(1,128)S(1)}, f32[1,1024]{1,0:T(1,128)S(1)}, f32[1,1024,128]{2,1,0:T(8,128)S(1)}) %tuple.84, (s32[]{:T(128)}, s32[1024]{0:T(1024)S(1)}, s32[]{:T(128)}, ...), branch_computations={%region_4.4_spmd, %region_5.7_spmd} | conditional | flops 551817216 | bytes 14540886 | solution.py:155
  108.4 5.5 %conditional.3 = ((f32[1,1024]{1,0:T(1,128)S(1)}, f32[1,1024]{1,0:T(1,128)S(1)}, f32[1,1024,128]{2,1,0:T(8,128)S(1)})) conditional(s32[]{:T(128)} %convert_element_type.61, (f32[1,1024]{1,0:T(1,128)S(1)}, f32[1,1024]{1,0:T(1,128)S(1)}, f32[1,1024,128]{2,1,0:T(8,128)S(1)}) %tuple.84, (s32[]{:T(128)}, s32[1024]{0:T(1024)S(1)}, s32[]{:T(128)}, ...), branch_computations={%region_4.4_spmd, %region_5.7_spmd} | conditional | flops 551817216 | bytes 14540886 | solution.py:155
  113.9 5.5 %conditional.3 = ((f32[1,1024]{1,0:T(1,128)S(1)}, f32[1,1024]{1,0:T(1,128)S(1)}, f32[1,1024,128]{2,1,0:T(8,128)S(1)})) conditional(s32[]{:T(128)} %convert_element_type.61, (f32[1,1024]{1,0:T(1,128)S(1)}, f32[1,1024]{1,0:T(1,128)S(1)}, f32[1,1024,128]{2,1,0:T(8,128)S(1)}) %tuple.84, (s32[]{:T(128)}, s32[1024]{0:T(1024)S(1)}, s32[]{:T(128)}, ...), branch_computations={%region_4.4_spmd, %region_5.7_spmd} | conditional | flops 551817216 | bytes 14540886 | solution.py:155
  119.5 5.5 %conditional.3 = ((f32[1,1024]{1,0:T(1,128)S(1)}, f32[1,1024]{1,0:T(1,128)S(1)}, f32[1,1024,128]{2,1,0:T(8,128)S(1)})) conditional(s32[]{:T(128)} %convert_element_type.61, (f32[1,1024]{1,0:T(1,128)S(1)}, f32[1,1024]{1,0:T(1,128)S(1)}, f32[1,1024,128]{2,1,0:T(8,128)S(1)}) %tuple.84, (s32[]{:T(128)}, s32[1024]{0:T(1024)S(1)}, s32[]{:T(128)}, ...), branch_computations={%region_4.4_spmd, %region_5.7_spmd} | conditional | flops 551817216 | bytes 14540886 | solution.py:155
  125.0 5.5 %conditional.3 = ((f32[1,1024]{1,0:T(1,128)S(1)}, f32[1,1024]{1,0:T(1,128)S(1)}, f32[1,1024,128]{2,1,0:T(8,128)S(1)})) conditional(s32[]{:T(128)} %convert_element_type.61, (f32[1,1024]{1,0:T(1,128)S(1)}, f32[1,1024]{1,0:T(1,128)S(1)}, f32[1,1024,128]{2,1,0:T(8,128)S(1)}) %tuple.84, (s32[]{:T(128)}, s32[1024]{0:T(1024)S(1)}, s32[]{:T(128)}, ...), branch_computations={%region_4.4_spmd, %region_5.7_spmd} | conditional | flops 551817216 | bytes 14540886 | solution.py:155
  130.6 5.5 %conditional.3 = ((f32[1,1024]{1,0:T(1,128)S(1)}, f32[1,1024]{1,0:T(1,128)S(1)}, f32[1,1024,128]{2,1,0:T(8,128)S(1)})) conditional(s32[]{:T(128)} %convert_element_type.61, (f32[1,1024]{1,0:T(1,128)S(1)}, f32[1,1024]{1,0:T(1,128)S(1)}, f32[1,1024,128]{2,1,0:T(8,128)S(1)}) %tuple.84, (s32[]{:T(128)}, s32[1024]{0:T(1024)S(1)}, s32[]{:T(128)}, ...), branch_computations={%region_4.4_spmd, %region_5.7_spmd} | conditional | flops 551817216 | bytes 14540886 | solution.py:155
  136.1 5.5 %conditional.3 = ((f32[1,1024]{1,0:T(1,128)S(1)}, f32[1,1024]{1,0:T(1,128)S(1)}, f32[1,1024,128]{2,1,0:T(8,128)S(1)})) conditional(s32[]{:T(128)} %convert_element_type.61, (f32[1,1024]{1,0:T(1,128)S(1)}, f32[1,1024]{1,0:T(1,128)S(1)}, f32[1,1024,128]{2,1,0:T(8,128)S(1)}) %tuple.84, (s32[]{:T(128)}, s32[1024]{0:T(1024)S(1)}, s32[]{:T(128)}, ...), branch_computations={%region_4.4_spmd, %region_5.7_spmd} | conditional | flops 551817216 | bytes 14540886 | solution.py:155
  141.7 5.5 %conditional.3 = ((f32[1,1024]{1,0:T(1,128)S(1)}, f32[1,1024]{1,0:T(1,128)S(1)}, f32[1,1024,128]{2,1,0:T(8,128)S(1)})) conditional(s32[]{:T(128)} %convert_element_type.61, (f32[1,1024]{1,0:T(1,128)S(1)}, f32[1,1024]{1,0:T(1,128)S(1)}, f32[1,1024,128]{2,1,0:T(8,128)S(1)}) %tuple.84, (s32[]{:T(128)}, s32[1024]{0:T(1024)S(1)}, s32[]{:T(128)}, ...), branch_computations={%region_4.4_spmd, %region_5.7_spmd} | conditional | flops 551817216 | bytes 14540886 | solution.py:155
  147.2 5.5 %conditional.3 = ((f32[1,1024]{1,0:T(1,128)S(1)}, f32[1,1024]{1,0:T(1,128)S(1)}, f32[1,1024,128]{2,1,0:T(8,128)S(1)})) conditional(s32[]{:T(128)} %convert_element_type.61, (f32[1,1024]{1,0:T(1,128)S(1)}, f32[1,1024]{1,0:T(1,128)S(1)}, f32[1,1024,128]{2,1,0:T(8,128)S(1)}) %tuple.84, (s32[]{:T(128)}, s32[1024]{0:T(1024)S(1)}, s32[]{:T(128)}, ...), branch_computations={%region_4.4_spmd, %region_5.7_spmd} | conditional | flops 551817216 | bytes 14540886 | solution.py:155
  152.8 5.5 %conditional.3 = ((f32[1,1024]{1,0:T(1,128)S(1)}, f32[1,1024]{1,0:T(1,128)S(1)}, f32[1,1024,128]{2,1,0:T(8,128)S(1)})) conditional(s32[]{:T(128)} %convert_element_type.61, (f32[1,1024]{1,0:T(1,128)S(1)}, f32[1,1024]{1,0:T(1,128)S(1)}, f32[1,1024,128]{2,1,0:T(8,128)S(1)}) %tuple.84, (s32[]{:T(128)}, s32[1024]{0:T(1024)S(1)}, s32[]{:T(128)}, ...), branch_computations={%region_4.4_spmd, %region_5.7_spmd} | conditional | flops 551817216 | bytes 14540886 | solution.py:155
  158.3 5.5 %conditional.3 = ((f32[1,1024]{1,0:T(1,128)S(1)}, f32[1,1024]{1,0:T(1,128)S(1)}, f32[1,1024,128]{2,1,0:T(8,128)S(1)})) conditional(s32[]{:T(128)} %convert_element_type.61, (f32[1,1024]{1,0:T(1,128)S(1)}, f32[1,1024]{1,0:T(1,128)S(1)}, f32[1,1024,128]{2,1,0:T(8,128)S(1)}) %tuple.84, (s32[]{:T(128)}, s32[1024]{0:T(1024)S(1)}, s32[]{:T(128)}, ...), branch_computations={%region_4.4_spmd, %region_5.7_spmd} | conditional | flops 551817216 | bytes 14540886 | solution.py:155
  163.8 5.5 %conditional.3 = ((f32[1,1024]{1,0:T(1,128)S(1)}, f32[1,1024]{1,0:T(1,128)S(1)}, f32[1,1024,128]{2,1,0:T(8,128)S(1)})) conditional(s32[]{:T(128)} %convert_element_type.61, (f32[1,1024]{1,0:T(1,128)S(1)}, f32[1,1024]{1,0:T(1,128)S(1)}, f32[1,1024,128]{2,1,0:T(8,128)S(1)}) %tuple.84, (s32[]{:T(128)}, s32[1024]{0:T(1024)S(1)}, s32[]{:T(128)}, ...), branch_computations={%region_4.4_spmd, %region_5.7_spmd} | conditional | flops 551817216 | bytes 14540886 | solution.py:155
  169.4 5.5 %conditional.3 = ((f32[1,1024]{1,0:T(1,128)S(1)}, f32[1,1024]{1,0:T(1,128)S(1)}, f32[1,1024,128]{2,1,0:T(8,128)S(1)})) conditional(s32[]{:T(128)} %convert_element_type.61, (f32[1,1024]{1,0:T(1,128)S(1)}, f32[1,1024]{1,0:T(1,128)S(1)}, f32[1,1024,128]{2,1,0:T(8,128)S(1)}) %tuple.84, (s32[]{:T(128)}, s32[1024]{0:T(1024)S(1)}, s32[]{:T(128)}, ...), branch_computations={%region_4.4_spmd, %region_5.7_spmd} | conditional | flops 551817216 | bytes 14540886 | solution.py:155
  174.9 5.5 %conditional.3 = ((f32[1,1024]{1,0:T(1,128)S(1)}, f32[1,1024]{1,0:T(1,128)S(1)}, f32[1,1024,128]{2,1,0:T(8,128)S(1)})) conditional(s32[]{:T(128)} %convert_element_type.61, (f32[1,1024]{1,0:T(1,128)S(1)}, f32[1,1024]{1,0:T(1,128)S(1)}, f32[1,1024,128]{2,1,0:T(8,128)S(1)}) %tuple.84, (s32[]{:T(128)}, s32[1024]{0:T(1024)S(1)}, s32[]{:T(128)}, ...), branch_computations={%region_4.4_spmd, %region_5.7_spmd} | conditional | flops 551817216 | bytes 14540886 | solution.py:155
  180.5 5.5 %conditional.3 = ((f32[1,1024]{1,0:T(1,128)S(1)}, f32[1,1024]{1,0:T(1,128)S(1)}, f32[1,1024,128]{2,1,0:T(8,128)S(1)})) conditional(s32[]{:T(128)} %convert_element_type.61, (f32[1,1024]{1,0:T(1,128)S(1)}, f32[1,1024]{1,0:T(1,128)S(1)}, f32[1,1024,128]{2,1,0:T(8,128)S(1)}) %tuple.84, (s32[]{:T(128)}, s32[1024]{0:T(1024)S(1)}, s32[]{:T(128)}, ...), branch_computations={%region_4.4_spmd, %region_5.7_spmd} | conditional | flops 551817216 | bytes 14540886 | solution.py:155
  186.0 5.5 %conditional.3 = ((f32[1,1024]{1,0:T(1,128)S(1)}, f32[1,1024]{1,0:T(1,128)S(1)}, f32[1,1024,128]{2,1,0:T(8,128)S(1)})) conditional(s32[]{:T(128)} %convert_element_type.61, (f32[1,1024]{1,0:T(1,128)S(1)}, f32[1,1024]{1,0:T(1,128)S(1)}, f32[1,1024,128]{2,1,0:T(8,128)S(1)}) %tuple.84, (s32[]{:T(128)}, s32[1024]{0:T(1024)S(1)}, s32[]{:T(128)}, ...), branch_computations={%region_4.4_spmd, %region_5.7_spmd} | conditional | flops 551817216 | bytes 14540886 | solution.py:155
  198.0 6.3 %all-to-all-done.3 = bf16[8,128,128]{2,1,0:T(8,128)(2,1)S(1)} async-done(((bf16[8,128,128]{2,1,0:T(8,128)(2,1)}), bf16[8,128,128]{2,1,0:T(8,128)(2,1)S(1)}, u32[]{:S(2)}, u32[]{:S(2)}) %all-to-all-start.3) | async-done | bytes 262176 | tf_op jit(solution)/shard_map/all_to_all | solution.py:162
  (198 shorter events, 135.1 us)
Async XLA Ops:
  6.5 1.0 copy-start
  6.5 4.9 %copy-start.3 = (bf16[2048,128]{1,0:T(8,128)(2,1)S(1)}, bf16[2048,128]{1,0:T(8,128)(2,1)}, u32[]{:S(2)}) copy-start(bf16[2048,128]{1,0:T(8,128)(2,1)} %param.16) | copy-start | bytes 1572868
  6.5 77.5 %all-gather.2.cloned.1.call-start = ((), (), s32[]{:S(2)}) async-start(), calls=%async_computation.4 | async-start | bytes 8912896 | tf_op jit(solution)/shard_map/all_gather | solution.py:52
  7.6 3.9 %copy-start.1 = (bf16[1024,2048]{1,0:T(8,128)(2,1)S(1)}, bf16[1024,2048]{1,0:T(8,128)(2,1)}, u32[]{:S(2)}) copy-start(bf16[1024,2048]{1,0:T(8,128)(2,1)} %param.14) | copy-start | bytes 12582916
  11.5 2.4 %copy-start.8 = (bf16[2048,128]{1,0:T(8,128)(2,1)S(1)}, bf16[2048,128]{1,0:T(8,128)(2,1)}, u32[]{:S(2)}) copy-start(bf16[2048,128]{1,0:T(8,128)(2,1)} %param.19) | copy-start | bytes 1572868
  13.9 3.6 %copy-start.2 = (bf16[1024,2048]{1,0:T(8,128)(2,1)S(1)}, bf16[1024,2048]{1,0:T(8,128)(2,1)}, u32[]{:S(2)}) copy-start(bf16[1024,2048]{1,0:T(8,128)(2,1)} %param.14) | copy-start | bytes 12582916
  13.9 3.6 %copy-start.4 = (bf16[2048,128]{1,0:T(8,128)(2,1)S(1)}, bf16[2048,128]{1,0:T(8,128)(2,1)}, u32[]{:S(2)}) copy-start(bf16[2048,128]{1,0:T(8,128)(2,1)} %param.18) | copy-start | bytes 1572868
  17.5 2.6 %copy-start.5 = (f32[31,128]{1,0:T(8,128)S(1)}, f32[31,128]{1,0:T(8,128)}, u32[]{:S(2)}) copy-start(f32[31,128]{1,0:T(8,128)} %param.20) | copy-start | bytes 47620
  18.8 5.5 %collective-permute-start = (bf16[30,128]{1,0:T(8,128)(2,1)S(1)}, bf16[30,128]{1,0:T(8,128)(2,1)S(1)}, u32[]{:S(2)}, u32[]{:S(2)}) collective-permute-start(bf16[30,128]{1,0:T(8,128)(2,1)S(1)} %slice.276), channel_id=1, source_target_pairs={{0,8},{8,16},{16,24},{24,32},{32,40},{40,48},{48,56},{56,64},{64,7... | collective-permute-start | bytes 23048 | tf_op jit(solution)/shard_map/ppermute | solution.py:17
  24.4 7.6 %copy-start.9 = (bf16[2048,128]{1,0:T(8,128)(2,1)S(1)}, bf16[2048,128]{1,0:T(8,128)(2,1)}, u32[]{:S(2)}) copy-start(bf16[2048,128]{1,0:T(8,128)(2,1)} %param.15) | copy-start | bytes 1572868
  26.8 10.8 %copy-start.6 = (f32[1024,1]{0,1:T(1,128)S(1)}, f32[1024,1]{0,1:T(1,128)}, u32[]{:S(2)}) copy-start(f32[1024,1]{0,1:T(1,128)} %param.22) | copy-start | bytes 12292
  27.5 10.1 %all-to-all-start = ((f32[8,1,2048]{2,1,0:T(1,128)}), f32[8,1,2048]{2,1,0:T(1,128)S(1)}, u32[]{:S(2)}, u32[]{:S(2)}) async-start(f32[8,1,2048]{2,1,0:T(1,128)} %broadcast_in_dim.19), calls=%async_computation | async-start | bytes 131072 | tf_op jit(solution)/shard_map/all_to_all | solution.py:22
  38.2 64.5 %all-to-all-start.2 = ((f32[16,1024,1]{1,2,0:T(1,128)}), f32[16,1024,1]{1,2,0:T(1,128)S(1)}, u32[]{:S(2)}, u32[]{:S(2)}) async-start(f32[16,1024,1]{1,2,0:T(1,128)} %broadcast_in_dim.44), calls=%async_computation.2 | async-start | bytes 131072 | tf_op jit(solution)/shard_map/all_to_all | solution.py:22
  102.7 94.0 %copy-start.7 = (f32[128]{0:T(128)S(1)}, f32[128]{0:T(128)}, u32[]{:S(2)}) copy-start(f32[128]{0:T(128)} %param.21) | copy-start | bytes 1540
  192.5 11.8 %all-to-all-start.3 = ((bf16[8,128,128]{2,1,0:T(8,128)(2,1)}), bf16[8,128,128]{2,1,0:T(8,128)(2,1)S(1)}, u32[]{:S(2)}, u32[]{:S(2)}) async-start(bf16[8,128,128]{2,1,0:T(8,128)(2,1)} %bitcast.47), calls=%async_computation.3 | async-start | bytes 524288 | tf_op jit(solution)/shard_map/all_to_all | solution.py:162
  204.3 10.8 %all-to-all-start.1 = ((bf16[8,128,128]{1,2,0:T(8,128)(2,1)}), bf16[8,128,128]{1,2,0:T(8,128)(2,1)S(1)}, u32[]{:S(2)}, u32[]{:S(2)}) async-start(bf16[8,128,128]{1,2,0:T(8,128)(2,1)} %copy.30), calls=%async_computation.1 | async-start | bytes 524288 | tf_op jit(solution)/shard_map/all_to_all | solution.py:161
Sparse Core Ops, SparseCore 0:
  14.0 70.0 all-gather.1
where the time goes:
time: 227 us; the launch traced here: 226 us
  matrix products  92.9 us (41%)
  waiting for transfers between devices  55.9 us (25%)
  local copies, waits for them, and re-layouts  22.3 us (10%)
  starting transfers between devices  20.4 us (9%)
  other arithmetic  18.8 us (8%)
  between operations  13.7 us (6%)
    all_gather x1, waiting for transfers between devices, in_one_piece(): lax.all_gather(both, axis, axis=dim, tiled=True)  38.9 us
    dot_general x16, matrix products, attend(): jnp.einsum('hqk,khd->hqd', weights.astype(jnp.bfloat16), shard_values, pr...  37.5 us
    dot_general x16, matrix products, attend(): jnp.einsum('qhd,khd->hqk', query_heads, shard_keys, preferred_element_typ...  35.1 us
    unnamed x22, local copies, waits for them, and re-layouts  13.9 us
    reduce_sum x16, other arithmetic, attend(): new_sum = running_sum * rescale + jnp.sum(weights, axis=2)  13.6 us
    all_to_all x2, starting transfers between devices, from_everyone(): lax.all_to_all(jnp.broadcast_to(shard[None], (length, *shard.shape)), axi...  11.4 us
    all_to_all x1, waiting for transfers between devices, on_device(): lax.all_to_all(attn_rows, 'tp', split_axis=0, concat_axis=1, tiled=True)  6.3 us
    slice x1, local copies, waits for them, and re-layouts, in_one_piece(): lax.slice_in_dim(result, at, at + a.shape[along], axis=along)  5.83 us
  transfers between devices with their start and end apart: 6, of which 5 were waited for; matrix products, arithmetic and copies ran while one was open for 16% of the time, Pallas kernels for 0%

commit v1 on v0

v1 whole, which is shorter than its diff:
```python
import functools

import jax
import jax.numpy as jnp
import numpy as np
from jax import lax
from jax.experimental import pallas as pl
from jax.experimental.pallas import tpu as pltpu
from jax.sharding import PartitionSpec as P


BF16, F32, I32 = jnp.bfloat16, jnp.float32, jnp.int32
SIDE = 4
HEAD = 128
TOK = 1024
HALF = 512
TAPS = 31
GATE_ROW = TOK
QUERY_ROW = TOK + 16
PACK_ROWS = QUERY_ROW + HALF // 2
BACK_ROWS = HALF + 16
TILES = 15
LOG2E = 1.4426950408889634
SCALE = HEAD**-0.5 * LOG2E
LOW = -1e30
TINY = 1e-37
EPS = 1e-05

VM = pl.BlockSpec(memory_space=pltpu.VMEM)
SM = pl.BlockSpec(memory_space=pltpu.SMEM)
ANY = pl.BlockSpec(memory_space=pl.ANY)


def dot(a, b):
    return jnp.dot(a, b, preferred_element_type=F32)


def params(mib):
    return pltpu.CompilerParams(vmem_limit_bytes=mib << 20)


def cost(flops, moved):
    return pl.CostEstimate(flops=flops, bytes_accessed=moved, transcendentals=0)


def moves(dx, dz):
    return [
        (z * SIDE + x, (z + dz) % SIDE * SIDE + (x + dx) % SIDE)
        for z in range(SIDE)
        for x in range(SIDE)
    ]


def eye():
    return lax.broadcasted_iota(I32, (128, 128), 0) == lax.broadcasted_iota(I32, (128, 128), 1)


def to_row(column):
    return jnp.sum(jnp.where(eye(), column, 0.0), axis=0, keepdims=True)


def to_column(row):
    return jnp.sum(jnp.where(eye(), row, 0.0), axis=1, keepdims=True)


def split3(value):
    top = value.astype(BF16)
    rest = value - top.astype(F32)
    mid = rest.astype(BF16)
    return top, mid, (rest - mid.astype(F32)).astype(BF16)


def work_table():
    table = np.zeros((SIDE * SIDE, 2, TILES + 1), np.int32)
    for z in range(SIDE):
        for x in range(SIDE):
            tiles = []
            for d in range(SIDE):
                for e in range(SIDE):
                    late = (d == 2) + (e == 2)
                    first_z = (z + e) % SIDE
                    if first_z < z or (e == 0 and x < (x + d) % SIDE):
                        tiles.append((late, d, 3 + e if e else 0))
                    second_z = (z + d) % SIDE
                    if second_z > z or (d == 0 and (x + e) % SIDE < x):
                        tiles.append((late, 4 + d, e))
            assert len(tiles) == TILES
            for n, (_, q, k) in enumerate(sorted(tiles)):
                table[z * SIDE + x, :, n] = q, k
    return table


def project_kernel(x_hbm, wq, wk, wv, gate, px, pz, x, w, sems):
    copies = [
        pltpu.make_async_copy(
            x_hbm.at[pl.ds(256 * i, 256)], x.at[pl.ds(256 * i, 256)], sems.at[i]
        )
        for i in range(4)
    ]
    for c in copies:
        c.start()
    w[:, 0:128] = wk[...]
    w[:, 128:256] = wv[...]
    w[:, 256:384] = wq[...]
    zero = jnp.zeros((8, 128), BF16)
    scaled = jnp.concatenate(
        [to_row(gate[128 * r : 128 * r + 128, :] * (-LOG2E)) for r in range(8)], axis=0
    )
    top, mid, low = split3(scaled)
    gates = jnp.concatenate(
        [jnp.concatenate([top, mid], axis=1), jnp.concatenate([low, zero], axis=1)], axis=0
    )
    px[GATE_ROW : GATE_ROW + 16, :] = gates
    pz[GATE_ROW : GATE_ROW + 16, :] = gates
    for i in range(4):
        copies[i].wait()
        out = dot(x[256 * i : 256 * i + 256, :], w[...]).astype(BF16)
        px[256 * i : 256 * i + 256, :] = out[:, :256]
        pz[256 * i : 256 * i + 256, :] = out[:, :256]
        dest = px if i < 2 else pz
        lane = 128 * (i % 2)
        dest[QUERY_ROW:PACK_ROWS, lane : lane + 128] = out[:, 256:]


def project(x, wq, wk, wv, gate):
    pack = jax.ShapeDtypeStruct((PACK_ROWS, 256), BF16)
    return pl.pallas_call(
        project_kernel,
        out_shape=(pack, pack),
        in_specs=[ANY, VM, VM, VM, VM],
        out_specs=(VM, VM),
        scratch_shapes=[
            pltpu.VMEM((TOK, 2048), BF16),
            pltpu.VMEM((2048, 384), BF16),
            pltpu.SemaphoreType.DMA((4,)),
        ],
        compiler_params=params(32),
        cost_estimate=cost(2 * TOK * 2048 * 512, 8 << 20),
        name="project",
    )(x, wq, wk, wv, gate)


def glu_kernel(x_hbm, wu, wg, out, x, w, sems):
    copies = [
        pltpu.make_async_copy(
            x_hbm.at[pl.ds(256 * i, 256)], x.at[pl.ds(256 * i, 256)], sems.at[i]
        )
        for i in range(4)
    ]
    for c in copies:
        c.start()
    w[:, 0:128] = wu[...]
    w[:, 128:256] = wg[...]
    for i in range(4):
        copies[i].wait()
        both = dot(x[256 * i : 256 * i + 256, :], w[...])
        out[256 * i : 256 * i + 256, :] = (both[:, :128] * jax.nn.sigmoid(both[:, 128:])).astype(
            BF16
        )


def glu(x, wu, wg):
    return pl.pallas_call(
        glu_kernel,
        out_shape=jax.ShapeDtypeStruct((TOK, 128), BF16),
        in_specs=[ANY, VM, VM],
        out_specs=VM,
        scratch_shapes=[
            pltpu.VMEM((TOK, 2048), BF16),
            pltpu.VMEM((2048, 256), BF16),
            pltpu.SemaphoreType.DMA((4,)),
        ],
        compiler_params=params(32),
        cost_estimate=cost(2 * TOK * 2048 * 256, 6 << 20),
        name="glu",
    )(x, wu, wg)


def conv_kernel(gated, halo, taps, gain, out, padded):
    padded[0:32, :] = halo[...].astype(F32)
    padded[32 : 32 + TOK, :] = gated[...].astype(F32)
    padded[32 + TOK :, :] = jnp.zeros((8, 128), F32)
    for block in range(8):
        start = 128 * block
        total = None
        for r in range(8):
            part = None
            for q in range(5):
                j = 8 * q + r - 2
                if 0 <= j < TAPS:
                    term = taps[j : j + 1, :] * padded[start + 8 * q : start + 8 * q + 136, :]
                    part = term if part is None else part + term
            part = part[r : r + 128, :]
            total = part if total is None else total + part
        out[block, 0:128, :] = total
        out[block, 128:136, :] = jnp.broadcast_to(gain[...], (8, 128))


def convolve(gated, halo, taps, gain):
    return pl.pallas_call(
        conv_kernel,
        out_shape=jax.ShapeDtypeStruct((8, 136, 128), F32),
        in_specs=[VM] * 4,
        out_specs=VM,
        scratch_shapes=[pltpu.VMEM((TOK + 40, 128), F32)],
        compiler_params=params(8),
        cost_estimate=cost(2 * TOK * 128 * 31 * 64, 1 << 20),
        name="convolve",
    )(gated, halo, taps, gain)


def diagonal_kernel(px, pz, m_out, l_out, acc_out):
    top = px[GATE_ROW : GATE_ROW + 8, :].astype(F32)
    low = px[GATE_ROW + 8 : GATE_ROW + 16, :].astype(F32)
    gates = top[:, :128] + top[:, 128:] + low[:, :128]
    for half, pack in ((0, px), (1, pz)):
        keys = HALF * (half + 1)
        query = jnp.concatenate(
            [pack[QUERY_ROW:PACK_ROWS, :128], pack[QUERY_ROW:PACK_ROWS, 128:]], axis=0
        )
        scores = lax.dot_general(
            query, px[:keys, :128], (((1,), (1,)), ((), ())), preferred_element_type=F32
        )
        row = lax.broadcasted_iota(I32, (HALF, 128), 0) + HALF * half
        lane = lax.broadcasted_iota(I32, (HALF, 128), 1)
        parts = []
        for c in range(keys // 128):
            t = scores[:, 128 * c : 128 * c + 128] * SCALE + gates[c : c + 1, :]
            parts.append(jnp.where(lane + 128 * c <= row, t, LOW))
        most = functools.reduce(jnp.maximum, parts)
        most = jnp.broadcast_to(jnp.max(most, axis=1, keepdims=True), (HALF, 128))
        weights = [jnp.exp2(t - most) for t in parts]
        m_out[half] = most
        l_out[half] = functools.reduce(jnp.add, weights)
        acc_out[half] = dot(
            jnp.concatenate([w.astype(BF16) for w in weights], axis=1), px[:keys, 128:]
        )


def diagonal(px, pz):
    state = jax.ShapeDtypeStruct((2, HALF, 128), F32)
    return pl.pallas_call(
        diagonal_kernel,
        out_shape=(state, state, state),
        in_specs=[VM, VM],
        out_specs=(VM, VM, VM),
        compiler_params=params(32),
        cost_estimate=cost(2 * HALF * 2048 * 512, 4 << 20),
        name="diagonal",
    )(px, pz)


def attend_kernel(
    table, own, px, x1, x2, x3, pz, z1, z2, z3, m_in, l_in, acc_in,
    o_own, lse_own, a1, a2, a3, b1, b2, b3,
    packs, query, gates, sa, sb, ma, mb, aa, ab, m, l, acc, sems,
):
    sources = (px, x1, x2, x3, z1, z2, z3)
    copies = [
        pltpu.make_async_copy(source, packs.at[n], sems.at[n]) for n, source in enumerate(sources)
    ]
    copies.append(pltpu.make_async_copy(pz, packs.at[7], sems.at[7]))
    for c in copies:
        c.start()
    m[...] = jnp.full_like(m, LOW)
    l[...] = jnp.zeros_like(l)
    acc[...] = jnp.zeros_like(acc)
    for half in range(2):
        m[4 * half] = m_in[half]
        l[4 * half] = l_in[half]
        acc[4 * half] = acc_in[half]
    for c in copies:
        c.wait()
    for n, slot in enumerate((0, 1, 2, 3, 7, 4, 5, 6)):
        for side in range(2):
            query[n, 256 * side : 256 * side + 256, :] = packs[
                slot, QUERY_ROW:PACK_ROWS, 128 * side : 128 * side + 128
            ]
    for n in range(7):
        top = packs[n, GATE_ROW : GATE_ROW + 8, :].astype(F32)
        low = packs[n, GATE_ROW + 8 : GATE_ROW + 16, :].astype(F32)
        gates[n] = top[:, :128] + top[:, 128:] + low[:, :128]
    row = own[0]

    def scores_of(n, s, most, shrink):
        q, k = table[row, 0, n], table[row, 1, n]
        raw = lax.dot_general(
            query[q], packs[k, :TOK, :128], (((1,), (1,)), ((), ())), preferred_element_type=F32
        )
        best = None
        for c in range(8):
            t = raw[:, 128 * c : 128 * c + 128] * SCALE + gates[k, c : c + 1, :]
            s[:, 128 * c : 128 * c + 128] = t
            best = t if best is None else jnp.maximum(best, t)
        old = m[q]
        new = jnp.maximum(old, jnp.max(best, axis=1, keepdims=True))
        shrink[...] = jnp.exp2(old - new)
        m[q] = new
        most[...] = new

    def weigh(n, s, most, shrink):
        q, k = table[row, 0, n], table[row, 1, n]
        top = most[...]
        by = shrink[...]
        w = [jnp.exp2(s[:, 128 * c : 128 * c + 128] - top) for c in range(8)]
        total = ((w[0] + w[1]) + (w[2] + w[3])) + ((w[4] + w[5]) + (w[6] + w[7]))
        rounded = jnp.concatenate([v.astype(BF16) for v in w], axis=1)
        l[q] = l[q] * by + total
        acc[q] = acc[q] * by + dot(rounded, packs[k, :TOK, 128:])

    first, second = (sa, ma, aa), (sb, mb, ab)
    scores_of(0, *first)

    def two_tiles(i, carry):
        scores_of(2 * i + 1, *second)
        weigh(2 * i, *first)
        scores_of(2 * i + 2, *first)
        weigh(2 * i + 1, *second)
        return carry

    lax.fori_loop(0, (TILES - 1) // 2, two_tiles, 0)
    weigh(TILES - 1, *first)
    for n, out in enumerate((None, a1, a2, a3, None, b1, b2, b3)):
        total = jnp.maximum(jnp.sum(l[n], axis=1, keepdims=True), TINY)
        mixed = acc[n] / total
        lse = m[n] + jnp.log2(total)
        if out is None:
            o_own[n // 4] = mixed
            lse_own[n // 4] = lse
        else:
            out[0:HALF, :] = mixed.astype(BF16)
            rows = [to_row(lse[128 * b : 128 * b + 128, :]) for b in range(4)]
            parts = split3(jnp.concatenate(rows + rows, axis=0))
            out[HALF : HALF + 16, :] = jnp.concatenate(
                [parts[0][:4], parts[1][:4], parts[2]], axis=0
            )


def attend(table, own, packs, state):
    back = jax.ShapeDtypeStruct((BACK_ROWS, 128), BF16)
    kept = jax.ShapeDtypeStruct((2, HALF, 128), F32)
    per_tile = [pltpu.VMEM((HALF, 128), F32)] * 4
    return pl.pallas_call(
        attend_kernel,
        out_shape=(kept, kept) + (back,) * 6,
        in_specs=[SM, SM] + [ANY] * 8 + [VM] * 3,
        out_specs=(VM,) * 8,
        scratch_shapes=[
            pltpu.VMEM((8, PACK_ROWS, 256), BF16),
            pltpu.VMEM((8, HALF, 128), BF16),
            pltpu.VMEM((7, 8, 128), F32),
            pltpu.VMEM((HALF, TOK), F32),
            pltpu.VMEM((HALF, TOK), F32),
            *per_tile,
            *[pltpu.VMEM((8, HALF, 128), F32)] * 3,
            pltpu.SemaphoreType.DMA((8,)),
        ],
        compiler_params=params(40),
        cost_estimate=cost(TILES * 4 * HALF * TOK * 256, 8 << 20),
        name="attend",
    )(table, own, *packs, *state)


def combine_kernel(o_own, lse_own, a1, a2, a3, b1, b2, b3, out):
    for half, backs in ((0, (a1, a2, a3)), (1, (b1, b2, b3))):
        lses = []
        for back in backs:
            tail = back[HALF : HALF + 16, :].astype(F32)
            lses.append(tail[0:4] + tail[4:8] + tail[8:12])
        for b in range(4):
            rows = slice(128 * b, 128 * b + 128)
            columns = [lse_own[half, rows, :]]
            columns += [jnp.broadcast_to(to_column(v[b : b + 1, :]), (128, 128)) for v in lses]
            most = functools.reduce(jnp.maximum, columns)
            shares = [jnp.exp2(c - most) for c in columns]
            mixed = shares[0] * o_own[half, rows, :]
            for share, back in zip(shares[1:], backs):
                mixed = mixed + share * back[rows, :].astype(F32)
            out[4 * half + b] = (mixed / functools.reduce(jnp.add, shares)).astype(BF16)


def combine(o_own, lse_own, backs):
    return pl.pallas_call(
        combine_kernel,
        out_shape=jax.ShapeDtypeStruct((8, 128, 128), BF16),
        in_specs=[VM] * 8,
        out_specs=VM,
        compiler_params=params(16),
        cost_estimate=cost(1 << 29, 2 << 20),
        name="combine",
    )(o_own, lse_own, *backs)


def conv_out_kernel(parts, w, out, rows):
    @pl.when(pl.program_id(0) == 0)
    def _():
        total = functools.reduce(jnp.add, [parts[c, :128, :] for c in range(8)])
        mean = jnp.sum(total, axis=1, keepdims=True) * (1.0 / 1024)
        far = [parts[c, :128, :] - mean for c in range(8)]
        spread = functools.reduce(jnp.add, [v * v for v in far])
        spread = jnp.sum(spread, axis=1, keepdims=True) * (1.0 / 1024)
        inverse = lax.rsqrt(spread + EPS)
        for c in range(8):
            v = far[c] * inverse * parts[c, 128:129, :]
            rows[:, 128 * c : 128 * c + 128] = (v * jax.nn.sigmoid(v)).astype(BF16)

    out[...] = dot(rows[...], w[...])


def conv_out(parts, w):
    return pl.pallas_call(
        conv_out_kernel,
        grid=(4,),
        out_shape=jax.ShapeDtypeStruct((128, 2048), F32),
        in_specs=[
            pl.BlockSpec((8, 136, 128), lambda j: (0, 0, 0)),
            pl.BlockSpec((1024, 512), lambda j: (0, j)),
        ],
        out_specs=pl.BlockSpec((128, 512), lambda j: (0, j)),
        scratch_shapes=[pltpu.VMEM((128, 1024), BF16)],
        compiler_params=params(16),
        cost_estimate=cost(2 * 128 * 1024 * 2048 * 4, 6 << 20),
        name="conv_out",
    )(parts, w)


def attn_out_kernel(parts, conv, w, out, rows):
    @pl.when(pl.program_id(0) == 0)
    def _():
        for c in range(8):
            rows[:, 128 * c : 128 * c + 128] = parts[c]

    out[...] = (dot(rows[...], w[...]) + conv[...]).astype(BF16)


def attn_out(parts, conv, w):
    return pl.pallas_call(
        attn_out_kernel,
        grid=(4,),
        out_shape=jax.ShapeDtypeStruct((128, 2048), BF16),
        in_specs=[
            pl.BlockSpec((8, 128, 128), lambda j: (0, 0, 0)),
            pl.BlockSpec((128, 512), lambda j: (0, j)),
            pl.BlockSpec((1024, 512), lambda j: (1, j)),
        ],
        out_specs=pl.BlockSpec((128, 512), lambda j: (0, j)),
        scratch_shapes=[pltpu.VMEM((128, 1024), BF16)],
        compiler_params=params(16),
        cost_estimate=cost(2 * 128 * 1024 * 2048 * 4, 6 << 20),
        name="attn_out",
    )(parts, conv, w)


def on_device(x, wq, wk, wv, wu, wg, taps, gain, gate, w_out):
    own = lax.axis_index("sp").astype(I32).reshape(1)
    table = jnp.asarray(work_table())
    px, pz = project(x, wq, wk, wv, gate)
    xs, zs = [None] * 4, [None] * 4
    for d in (1, 3, 2):
        xs[d] = lax.ppermute(px, "sp", moves(-d, 0))
        zs[d] = lax.ppermute(pz, "sp", moves(0, -d))
    gated = glu(x, wu, wg)
    halo = lax.ppermute(gated[TOK - 32 :], "sp", [(i, i + 1) for i in range(15)])
    state = diagonal(px, pz)
    conv = convolve(gated, halo, taps, gain.reshape(1, 128))
    conv_parts = lax.all_to_all(conv, "tp", 0, 0, tiled=True)
    conv_mixed = conv_out(conv_parts, w_out)
    packs = (px, *xs[1:], pz, *zs[1:])
    o_own, lse_own, *sent = attend(table, own, packs, state)
    backs = [lax.ppermute(sent[d - 1], "sp", moves(d, 0)) for d in (1, 2, 3)]
    backs += [lax.ppermute(sent[d + 2], "sp", moves(0, d)) for d in (1, 2, 3)]
    mixed = combine(o_own, lse_own, backs)
    attn_parts = lax.all_to_all(mixed, "tp", 0, 0, tiled=True)
    return attn_out(attn_parts, conv_mixed, w_out)


def solution(mesh):
    in_specs = (
        P("sp", None),
        P(None, "tp"),
        P(None, "tp"),
        P(None, "tp"),
        P(None, "tp"),
        P(None, "tp"),
        P(None, "tp"),
        P("tp"),
        P("sp", "tp"),
        P(),
    )
    out_specs = P(("sp", "tp"), None)
    return jax.shard_map(
        on_device, mesh=mesh, in_specs=in_specs, out_specs=out_specs, check_vma=False
    )
```

time: 227 us -> 115 us (0.51)
  the two profiles are of different devices: /device:TPU:102 before, /device:TPU:2 now
where the time goes in v1:
time: 115 us; the launch traced here: 114 us
  starting transfers between devices  36.5 us (32%)
  Pallas kernels  34 us (30%)
  waiting for transfers between devices  24.6 us (21%)
  local copies, waits for them, and re-layouts  18.9 us (16%)
    unnamed x35, local copies, waits for them, and re-layouts  18.9 us
    pallas_call x1, Pallas kernels, attend(): pl.pallas_call(attend_kernel, out_shape=(kept, kept) + (back,) * 6, in_sp...  17.1 us
    ppermute x3, waiting for transfers between devices, on_device(): xs[d] = lax.ppermute(px, 'sp', moves(-d, 0))  11.5 us
    ppermute x3, starting transfers between devices, on_device(): backs = [lax.ppermute(sent[d - 1], 'sp', moves(d, 0)) for d in (1, 2, 3)]  8.56 us
    ppermute x3, waiting for transfers between devices, on_device(): zs[d] = lax.ppermute(pz, 'sp', moves(0, -d))  6.16 us
    ppermute x3, starting transfers between devices, on_device(): zs[d] = lax.ppermute(pz, 'sp', moves(0, -d))  5.68 us
    ppermute x3, starting transfers between devices, on_device(): xs[d] = lax.ppermute(px, 'sp', moves(-d, 0))  5.27 us
    ppermute x3, starting transfers between devices, on_device(): backs += [lax.ppermute(sent[d + 2], 'sp', moves(0, d)) for d in (1, 2, 3)]  4.52 us
  transfers between devices with their start and end apart: 15, of which 7 were waited for; matrix products, arithmetic and copies ran while one was open for 0% of the time, Pallas kernels for 24%

profile of v1, /device:TPU:2, one launch (start us, length us, event | category | flops | bytes accessed | tf_op | source)
XLA Modules:
  0.0 114.1 jit_solution(7068723353837103003)
XLA Ops:
  1.0 2.2 %copy-done.2 = bf16[1024,2048]{1,0:T(8,128)(2,1)S(1)} copy-done((bf16[1024,2048]{1,0:T(8,128)(2,1)S(1)}, bf16[1024,2048]{1,0:T(8,128)(2,1)}, u32[]{:S(2)}) %copy-start.2) | copy-done | bytes 4194328
  6.3 3.6 %project.1 = (bf16[1296,256]{1,0:T(8,128)(2,1)S(1)}, bf16[1296,256]{1,0:T(8,128)(2,1)S(1)}) custom-call(bf16[1024,2048]{1,0:T(8,128)(2,1)S(1)} %copy-done.2, bf16[2048,128]{1,0:T(8,128)(2,1)S(1)} %copy-done.7, bf16[2048,128]{1,0:T(8,128)(2,1)S(1)} %copy-done.8, bf16[2048,128]{1,0:T(8,128)(2,1)S(1)} %copy-done.9, f32[1024,1]{1,0:T(8,128)S(1)} %copy.12.gate), custom_call_target="tpu_custom_call" | custom-call | flops 2147483648 | bytes 8388608 | tf_op jit(solution)/shard_map/project/pallas_call | solution.py:127
  11.4 3.3 %glu.1.gated = bf16[1024,128]{1,0:T(8,128)(2,1)S(1)} custom-call(bf16[1024,2048]{1,0:T(8,128)(2,1)S(1)} %copy-done.2, bf16[2048,128]{1,0:T(8,128)(2,1)S(1)} %copy-done.3, bf16[2048,128]{1,0:T(8,128)(2,1)S(1)} %copy-done.4), custom_call_target="tpu_custom_call" | custom-call | flops 1073741824 | bytes 6291456 | tf_op jit(solution)/shard_map/glu/pallas_call | solution.py:163
  14.7 3.5 %collective-permute-start.12 = (bf16[32,128]{1,0:T(8,128)(2,1)S(1)}, bf16[32,128]{1,0:T(8,128)(2,1)S(1)}, u32[]{:S(2)}, u32[]{:S(2)}) collective-permute-start(bf16[32,128]{1,0:T(8,128)(2,1)S(1)} %slice.4), channel_id=1, source_target_pairs={{0,8},{8,16},{16,24},{24,32},{32,40},{40,48},{48,56},{56,64},{64,7... | collective-permute-start | bytes 24584 | tf_op jit(solution)/shard_map/ppermute | solution.py:463
  18.2 4.8 %collective-permute-start.1 = (bf16[1296,256]{1,0:T(8,128)(2,1)S(1)}, bf16[1296,256]{1,0:T(8,128)(2,1)S(1)}, u32[]{:S(2)}, u32[]{:S(2)}) collective-permute-start(bf16[1296,256]{1,0:T(8,128)(2,1)S(1)} %get-tuple-element.18.px), channel_id=1, source_target_pairs={{0,16},{8,24},{16,0},{24,8},{32,48},{40,56},{48,32},{56,40},{64,80... | collective-permute-start | bytes 1990664 | tf_op jit(solution)/shard_map/ppermute | solution.py:460
  23.0 2.1 %collective-permute-start.3 = (bf16[1296,256]{1,0:T(8,128)(2,1)S(1)}, bf16[1296,256]{1,0:T(8,128)(2,1)}, u32[]{:S(2)}, u32[]{:S(2)}) collective-permute-start(bf16[1296,256]{1,0:T(8,128)(2,1)S(1)} %get-tuple-element.19.pz), channel_id=1, source_target_pairs={{0,96},{8,104},{16,112},{24,120},{32,0},{40,8},{48,16},{56,24},{64... | collective-permute-start | bytes 1990664 | tf_op jit(solution)/shard_map/ppermute | solution.py:461
  25.1 1.9 %collective-permute-start.4 = (bf16[1296,256]{1,0:T(8,128)(2,1)S(1)}, bf16[1296,256]{1,0:T(8,128)(2,1)}, u32[]{:S(2)}, u32[]{:S(2)}) collective-permute-start(bf16[1296,256]{1,0:T(8,128)(2,1)S(1)} %get-tuple-element.19.pz), channel_id=1, source_target_pairs={{0,64},{8,72},{16,80},{24,88},{32,96},{40,104},{48,112},{56,120},{... | collective-permute-start | bytes 1990664 | tf_op jit(solution)/shard_map/ppermute | solution.py:461
  32.1 2.2 %convolve.1 = f32[8,136,128]{2,1,0:T(8,128)} custom-call(bf16[1024,128]{1,0:T(8,128)(2,1)S(1)} %glu.1.gated, bf16[32,128]{1,0:T(8,128)(2,1)S(1)} %collective-permute-done.12.halo, f32[31,128]{1,0:T(8,128)S(1)} %copy-done.10, f32[1,128]{1,0:T(1,128)S(1)} %bitcast.2), custom_call_target="tpu_custom_call" | custom-call | flops 520093696 | bytes 1048576 | tf_op jit(solution)/shard_map/convolve/pallas_call | solution.py:200
  34.3 4.5 %all-to-all-start.1 = ((f32[8,136,128]{2,1,0:T(8,128)}), f32[8,136,128]{2,1,0:T(8,128)S(1)}, u32[]{:S(2)}, u32[]{:S(2)}) async-start(f32[8,136,128]{2,1,0:T(8,128)} %convolve.1), calls=%async_computation.1 | async-start | bytes 1114112 | tf_op jit(solution)/shard_map/all_to_all | solution.py:466
  38.8 2.9 %collective-permute-done.1.x2 = bf16[1296,256]{1,0:T(8,128)(2,1)S(1)} collective-permute-done((bf16[1296,256]{1,0:T(8,128)(2,1)S(1)}, bf16[1296,256]{1,0:T(8,128)(2,1)S(1)}, u32[]{:S(2)}, u32[]{:S(2)}) %collective-permute-start.1) | collective-permute-done | bytes 663584 | tf_op jit(solution)/shard_map/ppermute | solution.py:460
  41.8 8.6 %collective-permute-done.2.x3 = bf16[1296,256]{1,0:T(8,128)(2,1)} collective-permute-done((bf16[1296,256]{1,0:T(8,128)(2,1)S(1)}, bf16[1296,256]{1,0:T(8,128)(2,1)}, u32[]{:S(2)}, u32[]{:S(2)}) %collective-permute-start.2) | collective-permute-done | bytes 663584 | tf_op jit(solution)/shard_map/ppermute | solution.py:460
  50.3 2.4 %collective-permute-done.3.z1 = bf16[1296,256]{1,0:T(8,128)(2,1)} collective-permute-done((bf16[1296,256]{1,0:T(8,128)(2,1)S(1)}, bf16[1296,256]{1,0:T(8,128)(2,1)}, u32[]{:S(2)}, u32[]{:S(2)}) %collective-permute-start.3) | collective-permute-done | bytes 663584 | tf_op jit(solution)/shard_map/ppermute | solution.py:461
  52.7 3.8 %collective-permute-done.5.z3 = bf16[1296,256]{1,0:T(8,128)(2,1)} collective-permute-done((bf16[1296,256]{1,0:T(8,128)(2,1)S(1)}, bf16[1296,256]{1,0:T(8,128)(2,1)}, u32[]{:S(2)}, u32[]{:S(2)}) %collective-permute-start.5) | collective-permute-done | bytes 663584 | tf_op jit(solution)/shard_map/ppermute | solution.py:461
  59.7 17.1 %attend.1 = (f32[2,512,128]{2,1,0:T(8,128)S(1)}, f32[2,512,128]{2,1,0:T(8,128)S(1)}, bf16[528,128]{1,0:T(8,128)(2,1)S(1)}, bf16[528,128]{1,0:T(8,128)(2,1)S(1)},...) custom-call(s32[16,2,16]{2,1,0:T(2,128)S(1)} %copy-done.12, ...), custom_call_target="tpu_custom_call" | custom-call | flops 8053063680 | bytes 8388608 | tf_op jit(solution)/shard_map/attend/pallas_call | solution.py:343
  76.8 2.0 %collective-permute-start.10 = (bf16[528,128]{1,0:T(8,128)(2,1)S(1)}, bf16[528,128]{1,0:T(8,128)(2,1)S(1)}, u32[]{:S(2)}, u32[]{:S(2)}) collective-permute-start(bf16[528,128]{1,0:T(8,128)(2,1)S(1)} %get-tuple-element.29), channel_id=1, source_target_pairs={{0,64},{8,72},{16,80},{24,88},{32,96},{40,104},{48,112},{56,120},{... | collective-permute-start | bytes 405512 | tf_op jit(solution)/shard_map/ppermute | solution.py:471
  80.6 5.3 %collective-permute-start.7 = (bf16[528,128]{1,0:T(8,128)(2,1)S(1)}, bf16[528,128]{1,0:T(8,128)(2,1)S(1)}, u32[]{:S(2)}, u32[]{:S(2)}) collective-permute-start(bf16[528,128]{1,0:T(8,128)(2,1)S(1)} %get-tuple-element.26), channel_id=1, source_target_pairs={{0,16},{8,24},{16,0},{24,8},{32,48},{40,56},{48,32},{56,40},{64,80... | collective-permute-start | bytes 405512 | tf_op jit(solution)/shard_map/ppermute | solution.py:470
  85.9 2.6 %collective-permute-start.8 = (bf16[528,128]{1,0:T(8,128)(2,1)S(1)}, bf16[528,128]{1,0:T(8,128)(2,1)S(1)}, u32[]{:S(2)}, u32[]{:S(2)}) collective-permute-start(bf16[528,128]{1,0:T(8,128)(2,1)S(1)} %get-tuple-element.27), channel_id=1, source_target_pairs={{0,24},{8,0},{16,8},{24,16},{32,56},{40,32},{48,40},{56,48},{64,88... | collective-permute-start | bytes 405512 | tf_op jit(solution)/shard_map/ppermute | solution.py:470
  91.1 3.7 %collective-permute-done.9.b1 = bf16[528,128]{1,0:T(8,128)(2,1)S(1)} collective-permute-done((bf16[528,128]{1,0:T(8,128)(2,1)S(1)}, bf16[528,128]{1,0:T(8,128)(2,1)S(1)}, u32[]{:S(2)}, u32[]{:S(2)}) %collective-permute-start.9) | collective-permute-done | bytes 135200 | tf_op jit(solution)/shard_map/ppermute | solution.py:471
  96.1 4.5 %all-to-all-start = ((bf16[8,128,128]{2,1,0:T(8,128)(2,1)}), bf16[8,128,128]{2,1,0:T(8,128)(2,1)S(1)}, u32[]{:S(2)}, u32[]{:S(2)}) async-start(bf16[8,128,128]{2,1,0:T(8,128)(2,1)} %combine.1), calls=%async_computation | async-start | bytes 524288 | tf_op jit(solution)/shard_map/all_to_all | solution.py:473
  100.6 3.4 %copy-done = bf16[2048,2048]{1,0:T(8,128)(2,1)S(1)} copy-done((bf16[2048,2048]{1,0:T(8,128)(2,1)S(1)}, bf16[2048,2048]{1,0:T(8,128)(2,1)}, u32[]{:S(2)}) %copy-start) | copy-done | bytes 8388632
  104.0 2.0 %conv_out.1.conv = f32[128,2048]{1,0:T(8,128)S(1)} custom-call(f32[8,136,128]{2,1,0:T(8,128)S(1)} %all-to-all-done.1.parts, bf16[2048,2048]{1,0:T(8,128)(2,1)S(1)} %copy-done), custom_call_target="tpu_custom_call" | custom-call | flops 2147483648 | bytes 6291456 | tf_op jit(solution)/shard_map/conv_out/pallas_call | solution.py:411
  106.0 2.1 %all-to-all-done.parts = bf16[8,128,128]{2,1,0:T(8,128)(2,1)S(1)} async-done(((bf16[8,128,128]{2,1,0:T(8,128)(2,1)}), bf16[8,128,128]{2,1,0:T(8,128)(2,1)S(1)}, u32[]{:S(2)}, u32[]{:S(2)}) %all-to-all-start) | async-done | bytes 262176 | tf_op jit(solution)/shard_map/all_to_all | solution.py:473
  108.1 3.4 %copy-done.1 = bf16[2048,2048]{1,0:T(8,128)(2,1)S(1)} copy-done((bf16[2048,2048]{1,0:T(8,128)(2,1)S(1)}, bf16[2048,2048]{1,0:T(8,128)(2,1)}, u32[]{:S(2)}) %copy-start.1) | copy-done | bytes 8388632
  111.5 2.7 %attn_out.1 = bf16[128,2048]{1,0:T(8,128)(2,1)} custom-call(bf16[8,128,128]{2,1,0:T(8,128)(2,1)S(1)} %all-to-all-done.parts, f32[128,2048]{1,0:T(8,128)S(1)} %conv_out.1.conv, bf16[2048,2048]{1,0:T(8,128)(2,1)S(1)} %copy-done.1), custom_call_target="tpu_custom_call" | custom-call | flops 2147483648 | bytes 6291456 | tf_op jit(solution)/shard_map/attn_out/pallas_call | solution.py:437
  (50 shorter events, 19.6 us)
Async XLA Ops:
  0.0 10.4 %copy-start.3 = (bf16[2048,128]{1,0:T(8,128)(2,1)S(1)}, bf16[2048,128]{1,0:T(8,128)(2,1)}, u32[]{:S(2)}) copy-start(bf16[2048,128]{1,0:T(8,128)(2,1)} %wu.1) | copy-start | bytes 1572868
  1.0 2.2 %copy-start.2 = (bf16[1024,2048]{1,0:T(8,128)(2,1)S(1)}, bf16[1024,2048]{1,0:T(8,128)(2,1)}, u32[]{:S(2)}) copy-start(bf16[1024,2048]{1,0:T(8,128)(2,1)} %x_hbm.3) | copy-start | bytes 12582916
  6.3 25.8 %copy-start.10 = (f32[31,128]{1,0:T(8,128)S(1)}, f32[31,128]{1,0:T(8,128)}, u32[]{:S(2)}) copy-start(f32[31,128]{1,0:T(8,128)} %taps.1) | copy-start | bytes 47620
  6.3 25.8 %copy-start.11 = (f32[128]{0:T(128)S(1)}, f32[128]{0:T(128)}, u32[]{:S(2)}) copy-start(f32[128]{0:T(128)} %param.18) | copy-start | bytes 1540
  6.3 50.2 %copy-start.12 = (s32[16,2,16]{2,1,0:T(2,128)S(1)}, s32[16,2,16]{2,1,0:T(2,128)}, u32[]{:S(2)}) copy-start(s32[16,2,16]{2,1,0:T(2,128)} %constant.8.clone.table) | copy-start | bytes 6148
  9.9 17.1 %collective-permute-start = (bf16[1296,256]{1,0:T(8,128)(2,1)S(1)}, bf16[1296,256]{1,0:T(8,128)(2,1)S(1)}, u32[]{:S(2)}, u32[]{:S(2)}) collective-permute-start(bf16[1296,256]{1,0:T(8,128)(2,1)S(1)} %get-tuple-element.18.px), channel_id=1, source_target_pairs={{0,24},{8,0},{16,8},{24,16},{32,56},{40,32},{48,40},{56,48},{64,88... | collective-permute-start | bytes 1990664 | tf_op jit(solution)/shard_map/ppermute | solution.py:460
  14.7 10.4 %collective-permute-start.12 = (bf16[32,128]{1,0:T(8,128)(2,1)S(1)}, bf16[32,128]{1,0:T(8,128)(2,1)S(1)}, u32[]{:S(2)}, u32[]{:S(2)}) collective-permute-start(bf16[32,128]{1,0:T(8,128)(2,1)S(1)} %slice.4), channel_id=1, source_target_pairs={{0,8},{8,16},{16,24},{24,32},{32,40},{40,48},{48,56},{56,64},{64,7... | collective-permute-start | bytes 24584 | tf_op jit(solution)/shard_map/ppermute | solution.py:463
  18.2 23.5 %collective-permute-start.1 = (bf16[1296,256]{1,0:T(8,128)(2,1)S(1)}, bf16[1296,256]{1,0:T(8,128)(2,1)S(1)}, u32[]{:S(2)}, u32[]{:S(2)}) collective-permute-start(bf16[1296,256]{1,0:T(8,128)(2,1)S(1)} %get-tuple-element.18.px), channel_id=1, source_target_pairs={{0,16},{8,24},{16,0},{24,8},{32,48},{40,56},{48,32},{56,40},{64,80... | collective-permute-start | bytes 1990664 | tf_op jit(solution)/shard_map/ppermute | solution.py:460
  23.0 27.3 %collective-permute-start.2 = (bf16[1296,256]{1,0:T(8,128)(2,1)S(1)}, bf16[1296,256]{1,0:T(8,128)(2,1)}, u32[]{:S(2)}, u32[]{:S(2)}) collective-permute-start(bf16[1296,256]{1,0:T(8,128)(2,1)S(1)} %get-tuple-element.18.px), channel_id=1, source_target_pairs={{0,8},{8,16},{16,24},{24,0},{32,40},{40,48},{48,56},{56,32},{64,72... | collective-permute-start | bytes 1990664 | tf_op jit(solution)/shard_map/ppermute | solution.py:460
  23.0 29.7 %collective-permute-start.3 = (bf16[1296,256]{1,0:T(8,128)(2,1)S(1)}, bf16[1296,256]{1,0:T(8,128)(2,1)}, u32[]{:S(2)}, u32[]{:S(2)}) collective-permute-start(bf16[1296,256]{1,0:T(8,128)(2,1)S(1)} %get-tuple-element.19.pz), channel_id=1, source_target_pairs={{0,96},{8,104},{16,112},{24,120},{32,0},{40,8},{48,16},{56,24},{64... | collective-permute-start | bytes 1990664 | tf_op jit(solution)/shard_map/ppermute | solution.py:461
  25.1 27.6 %collective-permute-start.4 = (bf16[1296,256]{1,0:T(8,128)(2,1)S(1)}, bf16[1296,256]{1,0:T(8,128)(2,1)}, u32[]{:S(2)}, u32[]{:S(2)}) collective-permute-start(bf16[1296,256]{1,0:T(8,128)(2,1)S(1)} %get-tuple-element.19.pz), channel_id=1, source_target_pairs={{0,64},{8,72},{16,80},{24,88},{32,96},{40,104},{48,112},{56,120},{... | collective-permute-start | bytes 1990664 | tf_op jit(solution)/shard_map/ppermute | solution.py:461
  27.9 28.6 %collective-permute-start.5 = (bf16[1296,256]{1,0:T(8,128)(2,1)S(1)}, bf16[1296,256]{1,0:T(8,128)(2,1)}, u32[]{:S(2)}, u32[]{:S(2)}) collective-permute-start(bf16[1296,256]{1,0:T(8,128)(2,1)S(1)} %get-tuple-element.19.pz), channel_id=1, source_target_pairs={{0,32},{8,40},{16,48},{24,56},{32,64},{40,72},{48,80},{56,88},{64,... | collective-permute-start | bytes 1990664 | tf_op jit(solution)/shard_map/ppermute | solution.py:461
  32.1 2.2 %copy-start.13 = (f32[2,512,128]{2,1,0:T(8,128)}, f32[2,512,128]{2,1,0:T(8,128)S(1)}, u32[]{:S(2)}) copy-start(f32[2,512,128]{2,1,0:T(8,128)S(1)} %get-tuple-element.21.l_in) | copy-start | bytes 1572868
  34.3 61.8 %all-to-all-start.1 = ((f32[8,136,128]{2,1,0:T(8,128)}), f32[8,136,128]{2,1,0:T(8,128)S(1)}, u32[]{:S(2)}, u32[]{:S(2)}) async-start(f32[8,136,128]{2,1,0:T(8,128)} %convolve.1), calls=%async_computation.1 | async-start | bytes 1114112 | tf_op jit(solution)/shard_map/all_to_all | solution.py:466
  56.5 1.1 copy-start.6
  76.8 11.7 %collective-permute-start.10 = (bf16[528,128]{1,0:T(8,128)(2,1)S(1)}, bf16[528,128]{1,0:T(8,128)(2,1)S(1)}, u32[]{:S(2)}, u32[]{:S(2)}) collective-permute-start(bf16[528,128]{1,0:T(8,128)(2,1)S(1)} %get-tuple-element.29), channel_id=1, source_target_pairs={{0,64},{8,72},{16,80},{24,88},{32,96},{40,104},{48,112},{56,120},{... | collective-permute-start | bytes 405512 | tf_op jit(solution)/shard_map/ppermute | solution.py:471
  78.8 11.1 %collective-permute-start.11 = (bf16[528,128]{1,0:T(8,128)(2,1)S(1)}, bf16[528,128]{1,0:T(8,128)(2,1)S(1)}, u32[]{:S(2)}, u32[]{:S(2)}) collective-permute-start(bf16[528,128]{1,0:T(8,128)(2,1)S(1)} %get-tuple-element.30), channel_id=1, source_target_pairs={{0,96},{8,104},{16,112},{24,120},{32,0},{40,8},{48,16},{56,24},{64... | collective-permute-start | bytes 405512 | tf_op jit(solution)/shard_map/ppermute | solution.py:471
  79.9 9.9 %collective-permute-start.6 = (bf16[528,128]{1,0:T(8,128)(2,1)S(1)}, bf16[528,128]{1,0:T(8,128)(2,1)S(1)}, u32[]{:S(2)}, u32[]{:S(2)}) collective-permute-start(bf16[528,128]{1,0:T(8,128)(2,1)S(1)} %get-tuple-element.25), channel_id=1, source_target_pairs={{0,8},{8,16},{16,24},{24,0},{32,40},{40,48},{48,56},{56,32},{64,72... | collective-permute-start | bytes 405512 | tf_op jit(solution)/shard_map/ppermute | solution.py:470
  80.6 9.3 %collective-permute-start.7 = (bf16[528,128]{1,0:T(8,128)(2,1)S(1)}, bf16[528,128]{1,0:T(8,128)(2,1)S(1)}, u32[]{:S(2)}, u32[]{:S(2)}) collective-permute-start(bf16[528,128]{1,0:T(8,128)(2,1)S(1)} %get-tuple-element.26), channel_id=1, source_target_pairs={{0,16},{8,24},{16,0},{24,8},{32,48},{40,56},{48,32},{56,40},{64,80... | collective-permute-start | bytes 405512 | tf_op jit(solution)/shard_map/ppermute | solution.py:470
  85.9 5.2 %collective-permute-start.8 = (bf16[528,128]{1,0:T(8,128)(2,1)S(1)}, bf16[528,128]{1,0:T(8,128)(2,1)S(1)}, u32[]{:S(2)}, u32[]{:S(2)}) collective-permute-start(bf16[528,128]{1,0:T(8,128)(2,1)S(1)} %get-tuple-element.27), channel_id=1, source_target_pairs={{0,24},{8,0},{16,8},{24,16},{32,56},{40,32},{48,40},{56,48},{64,88... | collective-permute-start | bytes 405512 | tf_op jit(solution)/shard_map/ppermute | solution.py:470
  88.5 6.2 %collective-permute-start.9 = (bf16[528,128]{1,0:T(8,128)(2,1)S(1)}, bf16[528,128]{1,0:T(8,128)(2,1)S(1)}, u32[]{:S(2)}, u32[]{:S(2)}) collective-permute-start(bf16[528,128]{1,0:T(8,128)(2,1)S(1)} %get-tuple-element.28), channel_id=1, source_target_pairs={{0,32},{8,40},{16,48},{24,56},{32,64},{40,72},{48,80},{56,88},{64,... | collective-permute-start | bytes 405512 | tf_op jit(solution)/shard_map/ppermute | solution.py:471
  96.1 12.0 %all-to-all-start = ((bf16[8,128,128]{2,1,0:T(8,128)(2,1)}), bf16[8,128,128]{2,1,0:T(8,128)(2,1)S(1)}, u32[]{:S(2)}, u32[]{:S(2)}) async-start(bf16[8,128,128]{2,1,0:T(8,128)(2,1)} %combine.1), calls=%async_computation | async-start | bytes 524288 | tf_op jit(solution)/shard_map/all_to_all | solution.py:473
  100.6 3.4 %copy-start = (bf16[2048,2048]{1,0:T(8,128)(2,1)S(1)}, bf16[2048,2048]{1,0:T(8,128)(2,1)}, u32[]{:S(2)}) copy-start(bf16[2048,2048]{1,0:T(8,128)(2,1)} %w.3) | copy-start | bytes 25165828
  108.1 3.4 %copy-start.1 = (bf16[2048,2048]{1,0:T(8,128)(2,1)S(1)}, bf16[2048,2048]{1,0:T(8,128)(2,1)}, u32[]{:S(2)}) copy-start(bf16[2048,2048]{1,0:T(8,128)(2,1)} %w.3) | copy-start | bytes 25165828
  (8 other events, 7.9 us)

commit v2 on v1

--- a/solution.py
+++ b/solution.py
@@ -29,6 +29,7 @@
 VM = pl.BlockSpec(memory_space=pltpu.VMEM)
 SM = pl.BlockSpec(memory_space=pltpu.SMEM)
 ANY = pl.BlockSpec(memory_space=pl.ANY)
+HBM = pl.BlockSpec(memory_space=pltpu.HBM)
 
 
 def dot(a, b):
@@ -90,30 +91,32 @@
     return table
 
 
-def project_kernel(x_hbm, wq, wk, wv, gate, px, pz, x, w, sems):
-    copies = [
-        pltpu.make_async_copy(
-            x_hbm.at[pl.ds(256 * i, 256)], x.at[pl.ds(256 * i, 256)], sems.at[i]
-        )
-        for i in range(4)
-    ]
+def start_copies(x_hbm, weights, x, w, sems):
+    copies = []
+    for n, source in enumerate(weights):
+        dest = w.at[:, pl.ds(128 * n, 128)]
+        copies.append(pltpu.make_async_copy(source, dest, sems.at[4 + n]))
+    for i in range(4):
+        rows = pl.ds(256 * i, 256)
+        copies.append(pltpu.make_async_copy(x_hbm.at[rows], x.at[rows], sems.at[i]))
     for c in copies:
         c.start()
-    w[:, 0:128] = wk[...]
-    w[:, 128:256] = wv[...]
-    w[:, 256:384] = wq[...]
+    for c in copies[:-4]:
+        c.wait()
+    return copies[-4:]
+
+
+def project_kernel(x_hbm, wq, wk, wv, gate, px, pz, x, w, sems):
+    arrivals = start_copies(x_hbm, (wk, wv, wq), x, w, sems)
     zero = jnp.zeros((8, 128), BF16)
-    scaled = jnp.concatenate(
-        [to_row(gate[128 * r : 128 * r + 128, :] * (-LOG2E)) for r in range(8)], axis=0
-    )
-    top, mid, low = split3(scaled)
+    top, mid, low = split3(gate[...] * (-LOG2E))
     gates = jnp.concatenate(
         [jnp.concatenate([top, mid], axis=1), jnp.concatenate([low, zero], axis=1)], axis=0
     )
     px[GATE_ROW : GATE_ROW + 16, :] = gates
     pz[GATE_ROW : GATE_ROW + 16, :] = gates
     for i in range(4):
-        copies[i].wait()
+        arrivals[i].wait()
         out = dot(x[256 * i : 256 * i + 256, :], w[...]).astype(BF16)
         px[256 * i : 256 * i + 256, :] = out[:, :256]
         pz[256 * i : 256 * i + 256, :] = out[:, :256]
@@ -127,53 +130,44 @@
     return pl.pallas_call(
         project_kernel,
         out_shape=(pack, pack),
-        in_specs=[ANY, VM, VM, VM, VM],
+        in_specs=[HBM, HBM, HBM, HBM, VM],
         out_specs=(VM, VM),
         scratch_shapes=[
             pltpu.VMEM((TOK, 2048), BF16),
             pltpu.VMEM((2048, 384), BF16),
-            pltpu.SemaphoreType.DMA((4,)),
+            pltpu.SemaphoreType.DMA((7,)),
         ],
-        compiler_params=params(32),
+        compiler_params=params(12),
         cost_estimate=cost(2 * TOK * 2048 * 512, 8 << 20),
         name="project",
     )(x, wq, wk, wv, gate)
 
 
-def glu_kernel(x_hbm, wu, wg, out, x, w, sems):
-    copies = [
-        pltpu.make_async_copy(
-            x_hbm.at[pl.ds(256 * i, 256)], x.at[pl.ds(256 * i, 256)], sems.at[i]
-        )
-        for i in range(4)
-    ]
-    for c in copies:
-        c.start()
-    w[:, 0:128] = wu[...]
-    w[:, 128:256] = wg[...]
+def glu_kernel(x_hbm, wu, wg, after, out, x, w, sems):
+    arrivals = start_copies(x_hbm, (wu, wg), x, w, sems)
     for i in range(4):
-        copies[i].wait()
+        arrivals[i].wait()
         both = dot(x[256 * i : 256 * i + 256, :], w[...])
         out[256 * i : 256 * i + 256, :] = (both[:, :128] * jax.nn.sigmoid(both[:, 128:])).astype(
             BF16
         )
 
 
-def glu(x, wu, wg):
+def glu(x, wu, wg, after):
     return pl.pallas_call(
         glu_kernel,
         out_shape=jax.ShapeDtypeStruct((TOK, 128), BF16),
-        in_specs=[ANY, VM, VM],
+        in_specs=[HBM, HBM, HBM, ANY],
         out_specs=VM,
         scratch_shapes=[
             pltpu.VMEM((TOK, 2048), BF16),
             pltpu.VMEM((2048, 256), BF16),
-            pltpu.SemaphoreType.DMA((4,)),
+            pltpu.SemaphoreType.DMA((6,)),
         ],
-        compiler_params=params(32),
+        compiler_params=params(10),
         cost_estimate=cost(2 * TOK * 2048 * 256, 6 << 20),
         name="glu",
-    )(x, wu, wg)
+    )(x, wu, wg, after)
 
 
 def conv_kernel(gated, halo, taps, gain, out, padded):
@@ -209,7 +203,7 @@
     )(gated, halo, taps, gain)
 
 
-def diagonal_kernel(px, pz, m_out, l_out, acc_out):
+def diagonal_kernel(px, pz, after, m_out, l_out, acc_out):
     top = px[GATE_ROW : GATE_ROW + 8, :].astype(F32)
     low = px[GATE_ROW + 8 : GATE_ROW + 16, :].astype(F32)
     gates = top[:, :128] + top[:, 128:] + low[:, :128]
@@ -237,17 +231,17 @@
         )
 
 
-def diagonal(px, pz):
+def diagonal(px, pz, after):
     state = jax.ShapeDtypeStruct((2, HALF, 128), F32)
     return pl.pallas_call(
         diagonal_kernel,
         out_shape=(state, state, state),
-        in_specs=[VM, VM],
+        in_specs=[VM, VM, ANY],
         out_specs=(VM, VM, VM),
-        compiler_params=params(32),
+        compiler_params=params(16),
         cost_estimate=cost(2 * HALF * 2048 * 512, 4 << 20),
         name="diagonal",
-    )(px, pz)
+    )(px, pz, after)
 
 
 def attend_kernel(
@@ -355,7 +349,7 @@
             *[pltpu.VMEM((8, HALF, 128), F32)] * 3,
             pltpu.SemaphoreType.DMA((8,)),
         ],
-        compiler_params=params(40),
+        compiler_params=params(28),
         cost_estimate=cost(TILES * 4 * HALF * TOK * 256, 8 << 20),
         name="attend",
     )(table, own, *packs, *state)
@@ -391,87 +385,96 @@
     )(o_own, lse_own, *backs)
 
 
-def conv_out_kernel(parts, w, out, rows):
-    @pl.when(pl.program_id(0) == 0)
-    def _():
-        total = functools.reduce(jnp.add, [parts[c, :128, :] for c in range(8)])
-        mean = jnp.sum(total, axis=1, keepdims=True) * (1.0 / 1024)
-        far = [parts[c, :128, :] - mean for c in range(8)]
-        spread = functools.reduce(jnp.add, [v * v for v in far])
-        spread = jnp.sum(spread, axis=1, keepdims=True) * (1.0 / 1024)
-        inverse = lax.rsqrt(spread + EPS)
-        for c in range(8):
-            v = far[c] * inverse * parts[c, 128:129, :]
-            rows[:, 128 * c : 128 * c + 128] = (v * jax.nn.sigmoid(v)).astype(BF16)
-
-    out[...] = dot(rows[...], w[...])
+def conv_out_kernel(parts, w_hbm, out, later, rows, w, sems):
+    copies = []
+    for j in range(4):
+        cols = pl.ds(512 * j, 512)
+        copies.append(
+            pltpu.make_async_copy(w_hbm.at[pl.ds(0, 1024), cols], w.at[:, cols], sems.at[j])
+        )
+    copies.append(pltpu.make_async_copy(w_hbm.at[pl.ds(1024, 1024)], later, sems.at[4]))
+    for c in copies:
+        c.start()
+    total = functools.reduce(jnp.add, [parts[c, :128, :] for c in range(8)])
+    mean = jnp.sum(total, axis=1, keepdims=True) * (1.0 / 1024)
+    far = [parts[c, :128, :] - mean for c in range(8)]
+    spread = functools.reduce(jnp.add, [v * v for v in far])
+    spread = jnp.sum(spread, axis=1, keepdims=True) * (1.0 / 1024)
+    inverse = lax.rsqrt(spread + EPS)
+    for c in range(8):
+        v = far[c] * inverse * parts[c, 128:129, :]
+        rows[:, 128 * c : 128 * c + 128] = (v * jax.nn.sigmoid(v)).astype(BF16)
+    for j in range(4):
+        copies[j].wait()
+        out[:, 512 * j : 512 * j + 512] = dot(rows[...], w[:, 512 * j : 512 * j + 512])
+    copies[4].wait()
 
 
 def conv_out(parts, w):
     return pl.pallas_call(
         conv_out_kernel,
-        grid=(4,),
-        out_shape=jax.ShapeDtypeStruct((128, 2048), F32),
-        in_specs=[
-            pl.BlockSpec((8, 136, 128), lambda j: (0, 0, 0)),
-            pl.BlockSpec((1024, 512), lambda j: (0, j)),
+        out_shape=(
+            jax.ShapeDtypeStruct((128, 2048), F32),
+            jax.ShapeDtypeStruct((1024, 2048), BF16),
+        ),
+        in_specs=[VM, HBM],
+        out_specs=(VM, VM),
+        scratch_shapes=[
+            pltpu.VMEM((128, 1024), BF16),
+            pltpu.VMEM((1024, 2048), BF16),
+            pltpu.SemaphoreType.DMA((5,)),
         ],
-        out_specs=pl.BlockSpec((128, 512), lambda j: (0, j)),
-        scratch_shapes=[pltpu.VMEM((128, 1024), BF16)],
-        compiler_params=params(16),
+        compiler_params=params(14),
         cost_estimate=cost(2 * 128 * 1024 * 2048 * 4, 6 << 20),
         name="conv_out",
     )(parts, w)
 
 
 def attn_out_kernel(parts, conv, w, out, rows):
-    @pl.when(pl.program_id(0) == 0)
-    def _():
-        for c in range(8):
-            rows[:, 128 * c : 128 * c + 128] = parts[c]
-
-    out[...] = (dot(rows[...], w[...]) + conv[...]).astype(BF16)
+    for c in range(8):
+        rows[:, 128 * c : 128 * c + 128] = parts[c]
+    for j in range(4):
+        cols = slice(512 * j, 512 * j + 512)
+        out[:, cols] = (dot(rows[...], w[:, cols]) + conv[:, cols]).astype(BF16)
 
 
 def attn_out(parts, conv, w):
     return pl.pallas_call(
         attn_out_kernel,
-        grid=(4,),
         out_shape=jax.ShapeDtypeStruct((128, 2048), BF16),
-        in_specs=[
-            pl.BlockSpec((8, 128, 128), lambda j: (0, 0, 0)),
-            pl.BlockSpec((128, 512), lambda j: (0, j)),
-            pl.BlockSpec((1024, 512), lambda j: (1, j)),
-        ],
-        out_specs=pl.BlockSpec((128, 512), lambda j: (0, j)),
+        in_specs=[VM, VM, VM],
+        out_specs=VM,
         scratch_shapes=[pltpu.VMEM((128, 1024), BF16)],
-        compiler_params=params(16),
+        compiler_params=params(10),
         cost_estimate=cost(2 * 128 * 1024 * 2048 * 4, 6 << 20),
         name="attn_out",
     )(parts, conv, w)
 
 
-def on_device(x, wq, wk, wv, wu, wg, taps, gain, gate, w_out):
+def layer(x, wq, wk, wv, wu, wg, taps, gain, gate, w_out):
+    x, wq, wk, wv, wu, wg, w_out = (
+        pltpu.with_memory_space_constraint(v, pltpu.HBM) for v in (x, wq, wk, wv, wu, wg, w_out)
+    )
     own = lax.axis_index("sp").astype(I32).reshape(1)
     table = jnp.asarray(work_table())
-    px, pz = project(x, wq, wk, wv, gate)
+    px, pz = project(x, wq, wk, wv, gate.reshape(8, 128))
     xs, zs = [None] * 4, [None] * 4
     for d in (1, 3, 2):
         xs[d] = lax.ppermute(px, "sp", moves(-d, 0))
         zs[d] = lax.ppermute(pz, "sp", moves(0, -d))
-    gated = glu(x, wu, wg)
+    gated = glu(x, wu, wg, px)
     halo = lax.ppermute(gated[TOK - 32 :], "sp", [(i, i + 1) for i in range(15)])
-    state = diagonal(px, pz)
     conv = convolve(gated, halo, taps, gain.reshape(1, 128))
     conv_parts = lax.all_to_all(conv, "tp", 0, 0, tiled=True)
-    conv_mixed = conv_out(conv_parts, w_out)
+    conv_mixed, w_attn = conv_out(conv_parts, w_out)
+    state = diagonal(px, pz, conv_mixed)
     packs = (px, *xs[1:], pz, *zs[1:])
     o_own, lse_own, *sent = attend(table, own, packs, state)
     backs = [lax.ppermute(sent[d - 1], "sp", moves(d, 0)) for d in (1, 2, 3)]
     backs += [lax.ppermute(sent[d + 2], "sp", moves(0, d)) for d in (1, 2, 3)]
     mixed = combine(o_own, lse_own, backs)
     attn_parts = lax.all_to_all(mixed, "tp", 0, 0, tiled=True)
-    return attn_out(attn_parts, conv_mixed, w_out)
+    return attn_out(attn_parts, conv_mixed, w_attn)
 
 
 def solution(mesh):
@@ -488,6 +491,4 @@
         P(),
     )
     out_specs = P(("sp", "tp"), None)
-    return jax.shard_map(
-        on_device, mesh=mesh, in_specs=in_specs, out_specs=out_specs, check_vma=False
-    )
+    return jax.shard_map(layer, mesh=mesh, in_specs=in_specs, out_specs=out_specs, check_vma=False)

time: 115 us -> 108 us (0.939)
  the two profiles are of different devices: /device:TPU:2 before, /device:TPU:1 now
where the time goes in v2:
time: 108 us
  Pallas kernels  35.4 us (33%)
  waiting for transfers between devices  29.8 us (28%)
  starting transfers between devices  29 us (27%)
  blocking collectives  12.9 us (12%)
    ppermute x3, waiting for transfers between devices, layer(): zs[d] = lax.ppermute(pz, 'sp', moves(0, -d))  19.8 us
    pallas_call x1, Pallas kernels, attend(): pl.pallas_call(attend_kernel, out_shape=(kept, kept) + (back,) * 6, in_sp...  16.6 us
    all_to_all x1, blocking collectives, layer(): attn_parts = lax.all_to_all(mixed, 'tp', 0, 0, tiled=True)  12.9 us
    ppermute x3, starting transfers between devices, layer(): zs[d] = lax.ppermute(pz, 'sp', moves(0, -d))  9.57 us
    all_to_all x1, starting transfers between devices, layer(): conv_parts = lax.all_to_all(conv, 'tp', 0, 0, tiled=True)  6.27 us
    pallas_call x1, Pallas kernels, project(): pl.pallas_call(project_kernel, out_shape=(pack, pack), in_specs=[HBM, HBM...  4.62 us
    pallas_call x1, Pallas kernels, glu(): pl.pallas_call(glu_kernel, out_shape=jax.ShapeDtypeStruct((TOK, 128), BF1...  4.39 us
    ppermute x3, starting transfers between devices, layer(): backs = [lax.ppermute(sent[d - 1], 'sp', moves(d, 0)) for d in (1, 2, 3)]  4.22 us
  transfers between devices with their start and end apart: 14, of which 9 were waited for; matrix products, arithmetic and copies ran while one was open for 0% of the time, Pallas kernels for 11%

profile of v2, /device:TPU:1, one launch (start us, length us, event | category | flops | bytes accessed | tf_op | source)
XLA Modules:
  0.0 108.0 jit_solution(15117474995876571352)
XLA Ops:
  0.7 4.6 %project.1 = (bf16[1296,256]{1,0:T(8,128)(2,1)S(1)}, bf16[1296,256]{1,0:T(8,128)(2,1)S(1)}) custom-call(bf16[1024,2048]{1,0:T(8,128)(2,1)} %x_hbm.3, bf16[2048,128]{1,0:T(8,128)(2,1)} %wq.1, bf16[2048,128]{1,0:T(8,128)(2,1)} %wk.1, bf16[2048,128]{1,0:T(8,128)(2,1)} %wv.1, f32[8,128]{1,0:T(8,128)S(1)} %bitcast.3), custom_call_target="tpu_custom_call" | custom-call | flops 2147483648 | bytes 8388608 | tf_op jit(solution)/shard_map/project/pallas_call | solution.py:130
  5.3 2.5 %collective-permute-start.5 = (bf16[1296,256]{1,0:T(8,128)(2,1)S(1)}, bf16[1296,256]{1,0:T(8,128)(2,1)S(1)}, u32[]{:S(2)}, u32[]{:S(2)}) collective-permute-start(bf16[1296,256]{1,0:T(8,128)(2,1)S(1)} %get-tuple-element.21.pz), channel_id=1, source_target_pairs={{0,32},{8,40},{16,48},{24,56},{32,64},{40,72},{48,80},{56,88},{64,... | collective-permute-start | bytes 1990664 | tf_op jit(solution)/shard_map/ppermute | solution.py:464
  7.9 4.4 %glu.1.gated = bf16[1024,128]{1,0:T(8,128)(2,1)S(1)} custom-call(bf16[1024,2048]{1,0:T(8,128)(2,1)} %x_hbm.3, bf16[2048,128]{1,0:T(8,128)(2,1)} %wu.1, bf16[2048,128]{1,0:T(8,128)(2,1)} %wg.1, bf16[1296,256]{1,0:T(8,128)(2,1)S(1)} %get-tuple-element.20.after.px), custom_call_target="tpu_custom_call" | custom-call | flops 1073741824 | bytes 6291456 | tf_op jit(solution)/shard_map/glu/pallas_call | solution.py:157
  12.3 3.1 %collective-permute-start.6 = (bf16[32,128]{1,0:T(8,128)(2,1)S(1)}, bf16[32,128]{1,0:T(8,128)(2,1)S(1)}, u32[]{:S(2)}, u32[]{:S(2)}) collective-permute-start(bf16[32,128]{1,0:T(8,128)(2,1)S(1)} %slice.4), channel_id=1, source_target_pairs={{0,8},{8,16},{16,24},{24,32},{32,40},{40,48},{48,56},{56,64},{64,7... | collective-permute-start | bytes 24584 | tf_op jit(solution)/shard_map/ppermute | solution.py:466
  15.4 0.8 collective-permute-done.6.halo
  16.2 2.2 %convolve.1 = f32[8,136,128]{2,1,0:T(8,128)} custom-call(bf16[1024,128]{1,0:T(8,128)(2,1)S(1)} %glu.1.gated, bf16[32,128]{1,0:T(8,128)(2,1)S(1)} %collective-permute-done.6.halo, f32[31,128]{1,0:T(8,128)S(1)} %copy-done, f32[1,128]{1,0:T(1,128)S(1)} %bitcast.4), custom_call_target="tpu_custom_call" | custom-call | flops 520093696 | bytes 1048576 | tf_op jit(solution)/shard_map/convolve/pallas_call | solution.py:194
  18.4 6.3 %all-to-all-start = ((f32[8,136,128]{2,1,0:T(8,128)}), f32[8,136,128]{2,1,0:T(8,128)S(1)}, u32[]{:S(2)}, u32[]{:S(2)}) async-start(f32[8,136,128]{2,1,0:T(8,128)} %convolve.1), calls=%async_computation | async-start | bytes 1114112 | tf_op jit(solution)/shard_map/all_to_all | solution.py:468
  24.7 6.3 %collective-permute-start.4 = (bf16[1296,256]{1,0:T(8,128)(2,1)S(1)}, bf16[1296,256]{1,0:T(8,128)(2,1)S(1)}, u32[]{:S(2)}, u32[]{:S(2)}) collective-permute-start(bf16[1296,256]{1,0:T(8,128)(2,1)S(1)} %get-tuple-element.21.pz), channel_id=1, source_target_pairs={{0,64},{8,72},{16,80},{24,88},{32,96},{40,104},{48,112},{56,120},{... | collective-permute-start | bytes 1990664 | tf_op jit(solution)/shard_map/ppermute | solution.py:464
  31.7 1.4 %collective-permute-start.1 = (bf16[1296,256]{1,0:T(8,128)(2,1)S(1)}, bf16[1296,256]{1,0:T(8,128)(2,1)}, u32[]{:S(2)}, u32[]{:S(2)}) collective-permute-start(bf16[1296,256]{1,0:T(8,128)(2,1)S(1)} %get-tuple-element.20.after.px), channel_id=1, source_target_pairs={{0,16},{8,24},{16,0},{24,8},{32,48},{40,56},{48,32},{56,40},{64,80... | collective-permute-start | bytes 1990664 | tf_op jit(solution)/shard_map/ppermute | solution.py:463
  33.2 1.2 %collective-permute-start = (bf16[1296,256]{1,0:T(8,128)(2,1)S(1)}, bf16[1296,256]{1,0:T(8,128)(2,1)}, u32[]{:S(2)}, u32[]{:S(2)}) collective-permute-start(bf16[1296,256]{1,0:T(8,128)(2,1)S(1)} %get-tuple-element.20.after.px), channel_id=1, source_target_pairs={{0,24},{8,0},{16,8},{24,16},{32,56},{40,32},{48,40},{56,48},{64,88... | collective-permute-start | bytes 1990664 | tf_op jit(solution)/shard_map/ppermute | solution.py:463
  34.4 3.6 %conv_out.1 = (f32[128,2048]{1,0:T(8,128)S(1)}, bf16[1024,2048]{1,0:T(8,128)(2,1)S(1)}) custom-call(f32[8,136,128]{2,1,0:T(8,128)S(1)} %all-to-all-done.parts, bf16[2048,2048]{1,0:T(8,128)(2,1)} %w_hbm.1), custom_call_target="tpu_custom_call" | custom-call | flops 2147483648 | bytes 6291456 | tf_op jit(solution)/shard_map/conv_out/pallas_call | solution.py:414
  38.0 1.8 %diagonal.1 = (f32[2,512,128]{2,1,0:T(8,128)S(1)}, f32[2,512,128]{2,1,0:T(8,128)S(1)}, f32[2,512,128]{2,1,0:T(8,128)S(1)}) custom-call(bf16[1296,256]{1,0:T(8,128)(2,1)S(1)} %get-tuple-element.20.after.px, bf16[1296,256]{1,0:T(8,128)(2,1)S(1)} %get-tuple-element.21.pz, f32[128,2048]{1,0:T(8,128)S(1)} %get-tuple-element.22.after.conv), custom_call_target="tpu_custom_call" | custom-call | flops 1073741824 | bytes 4194304 | tf_op jit(solution)/shard_map/diagonal/pallas_call | solution.py:236
  39.8 6.5 %collective-permute-done.4.z2 = bf16[1296,256]{1,0:T(8,128)(2,1)S(1)} collective-permute-done((bf16[1296,256]{1,0:T(8,128)(2,1)S(1)}, bf16[1296,256]{1,0:T(8,128)(2,1)S(1)}, u32[]{:S(2)}, u32[]{:S(2)}) %collective-permute-start.4) | collective-permute-done | bytes 663584 | tf_op jit(solution)/shard_map/ppermute | solution.py:464
  46.3 13.3 %collective-permute-done.3.z1 = bf16[1296,256]{1,0:T(8,128)(2,1)} collective-permute-done((bf16[1296,256]{1,0:T(8,128)(2,1)S(1)}, bf16[1296,256]{1,0:T(8,128)(2,1)}, u32[]{:S(2)}, u32[]{:S(2)}) %collective-permute-start.3) | collective-permute-done | bytes 663584 | tf_op jit(solution)/shard_map/ppermute | solution.py:464
  59.6 3.6 %collective-permute-done.2.x3 = bf16[1296,256]{1,0:T(8,128)(2,1)} collective-permute-done((bf16[1296,256]{1,0:T(8,128)(2,1)S(1)}, bf16[1296,256]{1,0:T(8,128)(2,1)}, u32[]{:S(2)}, u32[]{:S(2)}) %collective-permute-start.2) | collective-permute-done | bytes 663584 | tf_op jit(solution)/shard_map/ppermute | solution.py:463
  63.6 16.6 %attend.1 = (f32[2,512,128]{2,1,0:T(8,128)S(1)}, f32[2,512,128]{2,1,0:T(8,128)S(1)}, bf16[528,128]{1,0:T(8,128)(2,1)S(1)}, bf16[528,128]{1,0:T(8,128)(2,1)S(1)},...) custom-call(s32[16,2,16]{2,1,0:T(2,128)S(1)} %copy-done.3, ...), custom_call_target="tpu_custom_call" | custom-call | flops 8053063680 | bytes 8388608 | tf_op jit(solution)/shard_map/attend/pallas_call | solution.py:337
  80.2 1.2 %collective-permute-start.7 = (bf16[528,128]{1,0:T(8,128)(2,1)S(1)}, bf16[528,128]{1,0:T(8,128)(2,1)S(1)}, u32[]{:S(2)}, u32[]{:S(2)}) collective-permute-start(bf16[528,128]{1,0:T(8,128)(2,1)S(1)} %get-tuple-element.28), channel_id=1, source_target_pairs={{0,8},{8,16},{16,24},{24,0},{32,40},{40,48},{48,56},{56,32},{64,72... | collective-permute-start | bytes 405512 | tf_op jit(solution)/shard_map/ppermute | solution.py:473
  81.4 3.0 %collective-permute-start.8 = (bf16[528,128]{1,0:T(8,128)(2,1)S(1)}, bf16[528,128]{1,0:T(8,128)(2,1)S(1)}, u32[]{:S(2)}, u32[]{:S(2)}) collective-permute-start(bf16[528,128]{1,0:T(8,128)(2,1)S(1)} %get-tuple-element.29), channel_id=1, source_target_pairs={{0,16},{8,24},{16,0},{24,8},{32,48},{40,56},{48,32},{56,40},{64,80... | collective-permute-start | bytes 405512 | tf_op jit(solution)/shard_map/ppermute | solution.py:473
  85.6 1.9 %collective-permute-start.12 = (bf16[528,128]{1,0:T(8,128)(2,1)S(1)}, bf16[528,128]{1,0:T(8,128)(2,1)S(1)}, u32[]{:S(2)}, u32[]{:S(2)}) collective-permute-start(bf16[528,128]{1,0:T(8,128)(2,1)S(1)} %get-tuple-element.33), channel_id=1, source_target_pairs={{0,96},{8,104},{16,112},{24,120},{32,0},{40,8},{48,16},{56,24},{64... | collective-permute-start | bytes 405512 | tf_op jit(solution)/shard_map/ppermute | solution.py:474
  87.5 2.7 %collective-permute-done.8.a2 = bf16[528,128]{1,0:T(8,128)(2,1)S(1)} collective-permute-done((bf16[528,128]{1,0:T(8,128)(2,1)S(1)}, bf16[528,128]{1,0:T(8,128)(2,1)S(1)}, u32[]{:S(2)}, u32[]{:S(2)}) %collective-permute-start.8) | collective-permute-done | bytes 135200 | tf_op jit(solution)/shard_map/ppermute | solution.py:473
  90.2 1.4 %collective-permute-done.11.b2 = bf16[528,128]{1,0:T(8,128)(2,1)S(1)} collective-permute-done((bf16[528,128]{1,0:T(8,128)(2,1)S(1)}, bf16[528,128]{1,0:T(8,128)(2,1)S(1)}, u32[]{:S(2)}, u32[]{:S(2)}) %collective-permute-start.11) | collective-permute-done | bytes 135200 | tf_op jit(solution)/shard_map/ppermute | solution.py:474
  91.7 1.2 %collective-permute-done.12.b3 = bf16[528,128]{1,0:T(8,128)(2,1)S(1)} collective-permute-done((bf16[528,128]{1,0:T(8,128)(2,1)S(1)}, bf16[528,128]{1,0:T(8,128)(2,1)S(1)}, u32[]{:S(2)}, u32[]{:S(2)}) %collective-permute-start.12) | collective-permute-done | bytes 135200 | tf_op jit(solution)/shard_map/ppermute | solution.py:474
  93.5 12.9 %all_to_all.10.parts = bf16[8,128,128]{2,1,0:T(8,128)(2,1)S(1)} all-to-all(bf16[8,128,128]{2,1,0:T(8,128)(2,1)S(1)} %combine.1), channel_id=1, replica_groups=mesh['sp'=16,'tp'=8] {'tp'}, dimensions={0} | all-to-all | bytes 524288 | tf_op jit(solution)/shard_map/all_to_all | solution.py:476
  106.4 1.6 %attn_out.1 = bf16[128,2048]{1,0:T(8,128)(2,1)} custom-call(bf16[8,128,128]{2,1,0:T(8,128)(2,1)S(1)} %all_to_all.10.parts, f32[128,2048]{1,0:T(8,128)S(1)} %get-tuple-element.22.after.conv, bf16[1024,2048]{1,0:T(8,128)(2,1)S(1)} %get-tuple-element.34.w), custom_call_target="tpu_custom_call" | custom-call | flops 2147483648 | bytes 6291456 | tf_op jit(solution)/shard_map/attn_out/pallas_call | solution.py:442
  (22 shorter events, 3.8 us)
Async XLA Ops:
  0.0 0.7 copy-start.1
  5.3 10.9 %copy-start = (f32[31,128]{1,0:T(8,128)S(1)}, f32[31,128]{1,0:T(8,128)}, u32[]{:S(2)}) copy-start(f32[31,128]{1,0:T(8,128)} %taps.1) | copy-start | bytes 47620
  5.3 10.8 %copy-start.2 = (f32[128]{0:T(128)S(1)}, f32[128]{0:T(128)}, u32[]{:S(2)}) copy-start(f32[128]{0:T(128)} %param.18) | copy-start | bytes 1540
  5.3 27.8 %collective-permute-start.5 = (bf16[1296,256]{1,0:T(8,128)(2,1)S(1)}, bf16[1296,256]{1,0:T(8,128)(2,1)S(1)}, u32[]{:S(2)}, u32[]{:S(2)}) collective-permute-start(bf16[1296,256]{1,0:T(8,128)(2,1)S(1)} %get-tuple-element.21.pz), channel_id=1, source_target_pairs={{0,32},{8,40},{16,48},{24,56},{32,64},{40,72},{48,80},{56,88},{64,... | collective-permute-start | bytes 1990664 | tf_op jit(solution)/shard_map/ppermute | solution.py:464
  12.3 3.9 %collective-permute-start.6 = (bf16[32,128]{1,0:T(8,128)(2,1)S(1)}, bf16[32,128]{1,0:T(8,128)(2,1)S(1)}, u32[]{:S(2)}, u32[]{:S(2)}) collective-permute-start(bf16[32,128]{1,0:T(8,128)(2,1)S(1)} %slice.4), channel_id=1, source_target_pairs={{0,8},{8,16},{16,24},{24,32},{32,40},{40,48},{48,56},{56,64},{64,7... | collective-permute-start | bytes 24584 | tf_op jit(solution)/shard_map/ppermute | solution.py:466
  18.4 16.0 %all-to-all-start = ((f32[8,136,128]{2,1,0:T(8,128)}), f32[8,136,128]{2,1,0:T(8,128)S(1)}, u32[]{:S(2)}, u32[]{:S(2)}) async-start(f32[8,136,128]{2,1,0:T(8,128)} %convolve.1), calls=%async_computation | async-start | bytes 1114112 | tf_op jit(solution)/shard_map/all_to_all | solution.py:468
  24.7 21.6 %collective-permute-start.4 = (bf16[1296,256]{1,0:T(8,128)(2,1)S(1)}, bf16[1296,256]{1,0:T(8,128)(2,1)S(1)}, u32[]{:S(2)}, u32[]{:S(2)}) collective-permute-start(bf16[1296,256]{1,0:T(8,128)(2,1)S(1)} %get-tuple-element.21.pz), channel_id=1, source_target_pairs={{0,64},{8,72},{16,80},{24,88},{32,96},{40,104},{48,112},{56,120},{... | collective-permute-start | bytes 1990664 | tf_op jit(solution)/shard_map/ppermute | solution.py:464
  31.0 28.6 %collective-permute-start.3 = (bf16[1296,256]{1,0:T(8,128)(2,1)S(1)}, bf16[1296,256]{1,0:T(8,128)(2,1)}, u32[]{:S(2)}, u32[]{:S(2)}) collective-permute-start(bf16[1296,256]{1,0:T(8,128)(2,1)S(1)} %get-tuple-element.21.pz), channel_id=1, source_target_pairs={{0,96},{8,104},{16,112},{24,120},{32,0},{40,8},{48,16},{56,24},{64... | collective-permute-start | bytes 1990664 | tf_op jit(solution)/shard_map/ppermute | solution.py:464
  31.7 31.4 %collective-permute-start.2 = (bf16[1296,256]{1,0:T(8,128)(2,1)S(1)}, bf16[1296,256]{1,0:T(8,128)(2,1)}, u32[]{:S(2)}, u32[]{:S(2)}) collective-permute-start(bf16[1296,256]{1,0:T(8,128)(2,1)S(1)} %get-tuple-element.20.after.px), channel_id=1, source_target_pairs={{0,8},{8,16},{16,24},{24,0},{32,40},{40,48},{48,56},{56,32},{64,72... | collective-permute-start | bytes 1990664 | tf_op jit(solution)/shard_map/ppermute | solution.py:463
  31.7 31.4 %collective-permute-start.1 = (bf16[1296,256]{1,0:T(8,128)(2,1)S(1)}, bf16[1296,256]{1,0:T(8,128)(2,1)}, u32[]{:S(2)}, u32[]{:S(2)}) collective-permute-start(bf16[1296,256]{1,0:T(8,128)(2,1)S(1)} %get-tuple-element.20.after.px), channel_id=1, source_target_pairs={{0,16},{8,24},{16,0},{24,8},{32,48},{40,56},{48,32},{56,40},{64,80... | collective-permute-start | bytes 1990664 | tf_op jit(solution)/shard_map/ppermute | solution.py:463
  33.2 30.4 %collective-permute-start = (bf16[1296,256]{1,0:T(8,128)(2,1)S(1)}, bf16[1296,256]{1,0:T(8,128)(2,1)}, u32[]{:S(2)}, u32[]{:S(2)}) collective-permute-start(bf16[1296,256]{1,0:T(8,128)(2,1)S(1)} %get-tuple-element.20.after.px), channel_id=1, source_target_pairs={{0,24},{8,0},{16,8},{24,16},{32,56},{40,32},{48,40},{56,48},{64,88... | collective-permute-start | bytes 1990664 | tf_op jit(solution)/shard_map/ppermute | solution.py:463
  34.4 29.1 %copy-start.3 = (s32[16,2,16]{2,1,0:T(2,128)S(1)}, s32[16,2,16]{2,1,0:T(2,128)}, u32[]{:S(2)}) copy-start(s32[16,2,16]{2,1,0:T(2,128)} %constant.8.clone.table) | copy-start | bytes 6148
  80.2 5.4 %collective-permute-start.7 = (bf16[528,128]{1,0:T(8,128)(2,1)S(1)}, bf16[528,128]{1,0:T(8,128)(2,1)S(1)}, u32[]{:S(2)}, u32[]{:S(2)}) collective-permute-start(bf16[528,128]{1,0:T(8,128)(2,1)S(1)} %get-tuple-element.28), channel_id=1, source_target_pairs={{0,8},{8,16},{16,24},{24,0},{32,40},{40,48},{48,56},{56,32},{64,72... | collective-permute-start | bytes 405512 | tf_op jit(solution)/shard_map/ppermute | solution.py:473
  81.4 8.8 %collective-permute-start.8 = (bf16[528,128]{1,0:T(8,128)(2,1)S(1)}, bf16[528,128]{1,0:T(8,128)(2,1)S(1)}, u32[]{:S(2)}, u32[]{:S(2)}) collective-permute-start(bf16[528,128]{1,0:T(8,128)(2,1)S(1)} %get-tuple-element.29), channel_id=1, source_target_pairs={{0,16},{8,24},{16,0},{24,8},{32,48},{40,56},{48,32},{56,40},{64,80... | collective-permute-start | bytes 405512 | tf_op jit(solution)/shard_map/ppermute | solution.py:473
  84.4 5.8 %collective-permute-start.9 = (bf16[528,128]{1,0:T(8,128)(2,1)S(1)}, bf16[528,128]{1,0:T(8,128)(2,1)S(1)}, u32[]{:S(2)}, u32[]{:S(2)}) collective-permute-start(bf16[528,128]{1,0:T(8,128)(2,1)S(1)} %get-tuple-element.30), channel_id=1, source_target_pairs={{0,24},{8,0},{16,8},{24,16},{32,56},{40,32},{48,40},{56,48},{64,88... | collective-permute-start | bytes 405512 | tf_op jit(solution)/shard_map/ppermute | solution.py:473
  84.4 5.9 %collective-permute-start.10 = (bf16[528,128]{1,0:T(8,128)(2,1)S(1)}, bf16[528,128]{1,0:T(8,128)(2,1)S(1)}, u32[]{:S(2)}, u32[]{:S(2)}) collective-permute-start(bf16[528,128]{1,0:T(8,128)(2,1)S(1)} %get-tuple-element.31), channel_id=1, source_target_pairs={{0,32},{8,40},{16,48},{24,56},{32,64},{40,72},{48,80},{56,88},{64,... | collective-permute-start | bytes 405512 | tf_op jit(solution)/shard_map/ppermute | solution.py:474
  85.1 6.5 %collective-permute-start.11 = (bf16[528,128]{1,0:T(8,128)(2,1)S(1)}, bf16[528,128]{1,0:T(8,128)(2,1)S(1)}, u32[]{:S(2)}, u32[]{:S(2)}) collective-permute-start(bf16[528,128]{1,0:T(8,128)(2,1)S(1)} %get-tuple-element.32), channel_id=1, source_target_pairs={{0,64},{8,72},{16,80},{24,88},{32,96},{40,104},{48,112},{56,120},{... | collective-permute-start | bytes 405512 | tf_op jit(solution)/shard_map/ppermute | solution.py:474
  85.6 7.2 %collective-permute-start.12 = (bf16[528,128]{1,0:T(8,128)(2,1)S(1)}, bf16[528,128]{1,0:T(8,128)(2,1)S(1)}, u32[]{:S(2)}, u32[]{:S(2)}) collective-permute-start(bf16[528,128]{1,0:T(8,128)(2,1)S(1)} %get-tuple-element.33), channel_id=1, source_target_pairs={{0,96},{8,104},{16,112},{24,120},{32,0},{40,8},{48,16},{56,24},{64... | collective-permute-start | bytes 405512 | tf_op jit(solution)/shard_map/ppermute | solution.py:474

commit v3 on v2

--- a/solution.py
+++ b/solution.py
@@ -78,14 +78,14 @@
             tiles = []
             for d in range(SIDE):
                 for e in range(SIDE):
-                    late = (d == 2) + (e == 2)
+                    late = d == 2 or e == 2
                     first_z = (z + e) % SIDE
                     if first_z < z or (e == 0 and x < (x + d) % SIDE):
-                        tiles.append((late, d, 3 + e if e else 0))
+                        tiles.append((late, d, 4 + e if e else 0))
                     second_z = (z + d) % SIDE
                     if second_z > z or (d == 0 and (x + e) % SIDE < x):
                         tiles.append((late, 4 + d, e))
-            assert len(tiles) == TILES
+            assert len(tiles) == TILES and sum(not t[0] for t in tiles) == 8
             for n, (_, q, k) in enumerate(sorted(tiles)):
                 table[z * SIDE + x, :, n] = q, k
     return table
@@ -106,8 +106,12 @@
     return copies[-4:]
 
 
-def project_kernel(x_hbm, wq, wk, wv, gate, px, pz, x, w, sems):
-    arrivals = start_copies(x_hbm, (wk, wv, wq), x, w, sems)
+def gate_rows(both):
+    return (both[:, :128] * jax.nn.sigmoid(both[:, 128:])).astype(BF16)
+
+
+def project_kernel(x_hbm, wq, wk, wv, wu, wg, gate, px, pz, tail, x, w, sems):
+    arrivals = start_copies(x_hbm, (wk, wv, wq, wu, wg), x, w, sems)
     zero = jnp.zeros((8, 128), BF16)
     top, mid, low = split3(gate[...] * (-LOG2E))
     gates = jnp.concatenate(
@@ -117,40 +121,38 @@
     pz[GATE_ROW : GATE_ROW + 16, :] = gates
     for i in range(4):
         arrivals[i].wait()
-        out = dot(x[256 * i : 256 * i + 256, :], w[...]).astype(BF16)
+        out = dot(x[256 * i : 256 * i + 256, :], w[:, :384]).astype(BF16)
         px[256 * i : 256 * i + 256, :] = out[:, :256]
         pz[256 * i : 256 * i + 256, :] = out[:, :256]
         dest = px if i < 2 else pz
         lane = 128 * (i % 2)
         dest[QUERY_ROW:PACK_ROWS, lane : lane + 128] = out[:, 256:]
-
-
-def project(x, wq, wk, wv, gate):
+    tail[...] = gate_rows(dot(x[TOK - 32 :, :], w[:, 384:]))
+
+
+def project(x, wq, wk, wv, wu, wg, gate):
     pack = jax.ShapeDtypeStruct((PACK_ROWS, 256), BF16)
     return pl.pallas_call(
         project_kernel,
-        out_shape=(pack, pack),
-        in_specs=[HBM, HBM, HBM, HBM, VM],
-        out_specs=(VM, VM),
+        out_shape=(pack, pack, jax.ShapeDtypeStruct((32, 128), BF16)),
+        in_specs=[HBM] * 6 + [VM],
+        out_specs=(VM, VM, VM),
         scratch_shapes=[
             pltpu.VMEM((TOK, 2048), BF16),
-            pltpu.VMEM((2048, 384), BF16),
-            pltpu.SemaphoreType.DMA((7,)),
+            pltpu.VMEM((2048, 640), BF16),
+            pltpu.SemaphoreType.DMA((9,)),
         ],
         compiler_params=params(12),
         cost_estimate=cost(2 * TOK * 2048 * 512, 8 << 20),
         name="project",
-    )(x, wq, wk, wv, gate)
+    )(x, wq, wk, wv, wu, wg, gate)
 
 
 def glu_kernel(x_hbm, wu, wg, after, out, x, w, sems):
     arrivals = start_copies(x_hbm, (wu, wg), x, w, sems)
     for i in range(4):
         arrivals[i].wait()
-        both = dot(x[256 * i : 256 * i + 256, :], w[...])
-        out[256 * i : 256 * i + 256, :] = (both[:, :128] * jax.nn.sigmoid(both[:, 128:])).astype(
-            BF16
-        )
+        out[256 * i : 256 * i + 256, :] = gate_rows(dot(x[256 * i : 256 * i + 256, :], w[...]))
 
 
 def glu(x, wu, wg, after):
@@ -203,7 +205,7 @@
     )(gated, halo, taps, gain)
 
 
-def diagonal_kernel(px, pz, after, m_out, l_out, acc_out):
+def diagonal_kernel(px, pz, m_out, l_out, acc_out):
     top = px[GATE_ROW : GATE_ROW + 8, :].astype(F32)
     low = px[GATE_ROW + 8 : GATE_ROW + 16, :].astype(F32)
     gates = top[:, :128] + top[:, 128:] + low[:, :128]
@@ -231,50 +233,43 @@
         )
 
 
-def diagonal(px, pz, after):
+def diagonal(px, pz):
     state = jax.ShapeDtypeStruct((2, HALF, 128), F32)
     return pl.pallas_call(
         diagonal_kernel,
         out_shape=(state, state, state),
-        in_specs=[VM, VM, ANY],
+        in_specs=[VM, VM],
         out_specs=(VM, VM, VM),
         compiler_params=params(16),
         cost_estimate=cost(2 * HALF * 2048 * 512, 4 << 20),
         name="diagonal",
-    )(px, pz, after)
-
-
-def attend_kernel(
-    table, own, px, x1, x2, x3, pz, z1, z2, z3, m_in, l_in, acc_in,
-    o_own, lse_own, a1, a2, a3, b1, b2, b3,
-    packs, query, gates, sa, sb, ma, mb, aa, ab, m, l, acc, sems,
-):
-    sources = (px, x1, x2, x3, z1, z2, z3)
-    copies = [
-        pltpu.make_async_copy(source, packs.at[n], sems.at[n]) for n, source in enumerate(sources)
-    ]
-    copies.append(pltpu.make_async_copy(pz, packs.at[7], sems.at[7]))
+    )(px, pz)
+
+
+PACKS = 8
+NEAR, FAR = 8, 7
+
+
+def load_packs(sources, packs, query, gates, sems):
+    copies = [pltpu.make_async_copy(src, packs.at[n], sems.at[n]) for n, src in sources]
     for c in copies:
         c.start()
-    m[...] = jnp.full_like(m, LOW)
-    l[...] = jnp.zeros_like(l)
-    acc[...] = jnp.zeros_like(acc)
-    for half in range(2):
-        m[4 * half] = m_in[half]
-        l[4 * half] = l_in[half]
-        acc[4 * half] = acc_in[half]
     for c in copies:
         c.wait()
-    for n, slot in enumerate((0, 1, 2, 3, 7, 4, 5, 6)):
+    for slot, _ in sources:
         for side in range(2):
-            query[n, 256 * side : 256 * side + 256, :] = packs[
+            query[slot, 256 * side : 256 * side + 256, :] = packs[
                 slot, QUERY_ROW:PACK_ROWS, 128 * side : 128 * side + 128
             ]
-    for n in range(7):
-        top = packs[n, GATE_ROW : GATE_ROW + 8, :].astype(F32)
-        low = packs[n, GATE_ROW + 8 : GATE_ROW + 16, :].astype(F32)
-        gates[n] = top[:, :128] + top[:, 128:] + low[:, :128]
+        top = packs[slot, GATE_ROW : GATE_ROW + 8, :].astype(F32)
+        low = packs[slot, GATE_ROW + 8 : GATE_ROW + 16, :].astype(F32)
+        gates[slot] = top[:, :128] + top[:, 128:] + low[:, :128]
+
+
+def run_tiles(table, own, start, count, packs, query, gates, per_tile, m, l, acc):
+    sa, sb, ma, mb, aa, ab = per_tile
     row = own[0]
+    first, second = (sa, ma, aa), (sb, mb, ab)
 
     def scores_of(n, s, most, shrink):
         q, k = table[row, 0, n], table[row, 1, n]
@@ -302,18 +297,59 @@
         l[q] = l[q] * by + total
         acc[q] = acc[q] * by + dot(rounded, packs[k, :TOK, 128:])
 
-    first, second = (sa, ma, aa), (sb, mb, ab)
-    scores_of(0, *first)
+
+    scores_of(start, *first)
 
     def two_tiles(i, carry):
-        scores_of(2 * i + 1, *second)
-        weigh(2 * i, *first)
-        scores_of(2 * i + 2, *first)
-        weigh(2 * i + 1, *second)
+        n = start + 2 * i
+        scores_of(n + 1, *second)
+        weigh(n, *first)
+        scores_of(n + 2, *first)
+        weigh(n + 1, *second)
         return carry
 
-    lax.fori_loop(0, (TILES - 1) // 2, two_tiles, 0)
-    weigh(TILES - 1, *first)
+    lax.fori_loop(0, (count - 1) // 2, two_tiles, 0)
+    if count % 2 == 0:
+        scores_of(start + count - 1, *second)
+        weigh(start + count - 2, *first)
+        weigh(start + count - 1, *second)
+    else:
+        weigh(start + count - 1, *first)
+
+
+def near_kernel(
+    table, own, px, x1, x3, pz, z1, z3, m_in, l_in, acc_in, after, m, l, acc,
+    packs, query, gates, sems, *per_tile,
+):
+    sources = ((0, px), (1, x1), (3, x3), (4, pz), (5, z1), (7, z3))
+    for half in range(2):
+        m[4 * half] = m_in[half]
+        l[4 * half] = l_in[half]
+        acc[4 * half] = acc_in[half]
+    for n in (1, 3, 5, 7):
+        m[n] = jnp.full((HALF, 128), LOW, F32)
+        l[n] = jnp.zeros((HALF, 128), F32)
+        acc[n] = jnp.zeros((HALF, 128), F32)
+    load_packs(sources, packs, query, gates, sems)
+    run_tiles(table, own, 0, NEAR, packs, query, gates, per_tile, m, l, acc)
+
+
+def far_kernel(
+    table, own, px, x1, x2, x3, pz, z1, z2, z3, m_in, l_in, acc_in,
+    o_own, lse_own, a1, a2, a3, b1, b2, b3,
+    packs, query, gates, sems, m, l, acc, *per_tile,
+):
+    sources = ((0, px), (1, x1), (2, x2), (3, x3), (4, pz), (5, z1), (6, z2), (7, z3))
+    for n in (0, 1, 3, 4, 5, 7):
+        m[n] = m_in[n]
+        l[n] = l_in[n]
+        acc[n] = acc_in[n]
+    for n in (2, 6):
+        m[n] = jnp.full((HALF, 128), LOW, F32)
+        l[n] = jnp.zeros((HALF, 128), F32)
+        acc[n] = jnp.zeros((HALF, 128), F32)
+    load_packs(sources, packs, query, gates, sems)
+    run_tiles(table, own, NEAR, FAR, packs, query, gates, per_tile, m, l, acc)
     for n, out in enumerate((None, a1, a2, a3, None, b1, b2, b3)):
         total = jnp.maximum(jnp.sum(l[n], axis=1, keepdims=True), TINY)
         mixed = acc[n] / total
@@ -330,28 +366,42 @@
             )
 
 
-def attend(table, own, packs, state):
+SLOT_SCRATCH = [
+    pltpu.VMEM((PACKS, PACK_ROWS, 256), BF16),
+    pltpu.VMEM((PACKS, HALF, 128), BF16),
+    pltpu.VMEM((PACKS, 8, 128), F32),
+    pltpu.SemaphoreType.DMA((PACKS,)),
+]
+TILE_SCRATCH = [pltpu.VMEM((HALF, TOK), F32)] * 2 + [pltpu.VMEM((HALF, 128), F32)] * 4
+STATE_SCRATCH = [pltpu.VMEM((PACKS, HALF, 128), F32)] * 3
+
+
+def attend_near(table, own, packs, state, after):
+    kept = jax.ShapeDtypeStruct((PACKS, HALF, 128), F32)
+    return pl.pallas_call(
+        near_kernel,
+        out_shape=(kept, kept, kept),
+        in_specs=[SM, SM] + [ANY] * 6 + [VM] * 3 + [ANY],
+        out_specs=(VM,) * 3,
+        scratch_shapes=SLOT_SCRATCH + TILE_SCRATCH,
+        compiler_params=params(24),
+        cost_estimate=cost(NEAR * 4 * HALF * TOK * 256, 8 << 20),
+        name="attend_near",
+    )(table, own, *packs, *state, after)
+
+
+def attend_far(table, own, packs, state):
     back = jax.ShapeDtypeStruct((BACK_ROWS, 128), BF16)
     kept = jax.ShapeDtypeStruct((2, HALF, 128), F32)
-    per_tile = [pltpu.VMEM((HALF, 128), F32)] * 4
-    return pl.pallas_call(
-        attend_kernel,
+    return pl.pallas_call(
+        far_kernel,
         out_shape=(kept, kept) + (back,) * 6,
         in_specs=[SM, SM] + [ANY] * 8 + [VM] * 3,
         out_specs=(VM,) * 8,
-        scratch_shapes=[
-            pltpu.VMEM((8, PACK_ROWS, 256), BF16),
-            pltpu.VMEM((8, HALF, 128), BF16),
-            pltpu.VMEM((7, 8, 128), F32),
-            pltpu.VMEM((HALF, TOK), F32),
-            pltpu.VMEM((HALF, TOK), F32),
-            *per_tile,
-            *[pltpu.VMEM((8, HALF, 128), F32)] * 3,
-            pltpu.SemaphoreType.DMA((8,)),
-        ],
-        compiler_params=params(28),
-        cost_estimate=cost(TILES * 4 * HALF * TOK * 256, 8 << 20),
-        name="attend",
+        scratch_shapes=SLOT_SCRATCH + STATE_SCRATCH + TILE_SCRATCH,
+        compiler_params=params(30),
+        cost_estimate=cost(FAR * 4 * HALF * TOK * 256, 8 << 20),
+        name="attend_far",
     )(table, own, *packs, *state)
 
 
@@ -457,19 +507,21 @@
     )
     own = lax.axis_index("sp").astype(I32).reshape(1)
     table = jnp.asarray(work_table())
-    px, pz = project(x, wq, wk, wv, gate.reshape(8, 128))
+    px, pz, tail = project(x, wq, wk, wv, wu, wg, gate.reshape(8, 128))
+    halo = lax.ppermute(tail, "sp", [(i, i + 1) for i in range(15)])
     xs, zs = [None] * 4, [None] * 4
     for d in (1, 3, 2):
         xs[d] = lax.ppermute(px, "sp", moves(-d, 0))
         zs[d] = lax.ppermute(pz, "sp", moves(0, -d))
     gated = glu(x, wu, wg, px)
-    halo = lax.ppermute(gated[TOK - 32 :], "sp", [(i, i + 1) for i in range(15)])
     conv = convolve(gated, halo, taps, gain.reshape(1, 128))
     conv_parts = lax.all_to_all(conv, "tp", 0, 0, tiled=True)
     conv_mixed, w_attn = conv_out(conv_parts, w_out)
-    state = diagonal(px, pz, conv_mixed)
+    state = diagonal(px, pz)
+    near = (px, xs[1], xs[3], pz, zs[1], zs[3])
+    state = attend_near(table, own, near, state, conv_mixed)
     packs = (px, *xs[1:], pz, *zs[1:])
-    o_own, lse_own, *sent = attend(table, own, packs, state)
+    o_own, lse_own, *sent = attend_far(table, own, packs, state)
     backs = [lax.ppermute(sent[d - 1], "sp", moves(d, 0)) for d in (1, 2, 3)]
     backs += [lax.ppermute(sent[d + 2], "sp", moves(0, d)) for d in (1, 2, 3)]
     mixed = combine(o_own, lse_own, backs)
@@ -491,4 +543,6 @@
         P(),
     )
     out_specs = P(("sp", "tp"), None)
-    return jax.shard_map(layer, mesh=mesh, in_specs=in_specs, out_specs=out_specs, check_vma=False)
+    return jax.shard_map(
+        layer, mesh=mesh, in_specs=in_specs, out_specs=out_specs, check_vma=False
+    )

time: 108 us -> 105 us (0.972)
  the two profiles are of different devices: /device:TPU:1 before, /device:TPU:2 now
where the time goes in v3:
time: 105 us
  Pallas kernels  39.7 us (38%)
  starting transfers between devices  27.9 us (27%)
  waiting for transfers between devices  22.5 us (21%)
  blocking collectives  11.7 us (11%)
  local copies, waits for them, and re-layouts  3.1 us (3%)
    ppermute x3, waiting for transfers between devices, layer(): zs[d] = lax.ppermute(pz, 'sp', moves(0, -d))  15.2 us
    all_to_all x1, blocking collectives, layer(): attn_parts = lax.all_to_all(mixed, 'tp', 0, 0, tiled=True)  11.7 us
    pallas_call x1, Pallas kernels, attend_far(): pl.pallas_call(far_kernel, out_shape=(kept, kept) + (back,) * 6, in_specs...  10.1 us
    pallas_call x1, Pallas kernels, attend_near(): pl.pallas_call(near_kernel, out_shape=(kept, kept, kept), in_specs=[SM, S...  9.99 us
    ppermute x3, starting transfers between devices, layer(): zs[d] = lax.ppermute(pz, 'sp', moves(0, -d))  5.97 us
    ppermute x3, starting transfers between devices, layer(): backs = [lax.ppermute(sent[d - 1], 'sp', moves(d, 0)) for d in (1, 2, 3)]  5.33 us
    pallas_call x1, Pallas kernels, project(): pl.pallas_call(project_kernel, out_shape=(pack, pack, jax.ShapeDtypeStruc...  5.3 us
    ppermute x3, starting transfers between devices, layer(): backs += [lax.ppermute(sent[d + 2], 'sp', moves(0, d)) for d in (1, 2, 3)]  4.5 us
  transfers between devices with their start and end apart: 14, of which 5 were waited for; matrix products, arithmetic and copies ran while one was open for 0% of the time, Pallas kernels for 21%

profile of v3, /device:TPU:2, one launch (start us, length us, event | category | flops | bytes accessed | tf_op | source)
XLA Modules:
  0.0 105.0 jit_solution(9638562347494868554)
XLA Ops:
  0.7 5.3 %project.1 = (bf16[1296,256]{1,0:T(8,128)(2,1)S(1)}, bf16[1296,256]{1,0:T(8,128)(2,1)S(1)}, bf16[32,128]{1,0:T(8,128)(2,1)S(1)}) custom-call(bf16[1024,2048]{1,0:T(8,128)(2,1)} %x_hbm.3, bf16[2048,128]{1,0:T(8,128)(2,1)} %wq.1, bf16[2048,128]{1,0:T(8,128)(2,1)} %wk.1, bf16[2048,128]{1,0:T(8,128)(2,1)} %wv.1, bf16[2048,128]{1,0:T(8,128)(2,1)} %wu.3, ...), custom_call_target="tpu_custom_call" | custom-call | flops 2147483648 | bytes 8388608 | tf_op jit(solution)/shard_map/project/pallas_call | solution.py:135
  6.0 2.0 %collective-permute-start.5 = (bf16[1296,256]{1,0:T(8,128)(2,1)S(1)}, bf16[1296,256]{1,0:T(8,128)(2,1)S(1)}, u32[]{:S(2)}, u32[]{:S(2)}) collective-permute-start(bf16[1296,256]{1,0:T(8,128)(2,1)S(1)} %get-tuple-element.25.pz), channel_id=1, source_target_pairs={{0,32},{8,40},{16,48},{24,56},{32,64},{40,72},{48,80},{56,88},{64,... | collective-permute-start | bytes 1990664 | tf_op jit(solution)/shard_map/ppermute | solution.py:515
  8.0 3.4 %collective-permute-start.6 = (bf16[32,128]{1,0:T(8,128)(2,1)S(1)}, bf16[32,128]{1,0:T(8,128)(2,1)S(1)}, u32[]{:S(2)}, u32[]{:S(2)}) collective-permute-start(bf16[32,128]{1,0:T(8,128)(2,1)S(1)} %get-tuple-element.29), channel_id=1, source_target_pairs={{0,8},{8,16},{16,24},{24,32},{32,40},{40,48},{48,56},{56,64},{64,7... | collective-permute-start | bytes 24584 | tf_op jit(solution)/shard_map/ppermute | solution.py:511
  11.4 4.4 %glu.1.gated = bf16[1024,128]{1,0:T(8,128)(2,1)S(1)} custom-call(bf16[1024,2048]{1,0:T(8,128)(2,1)} %x_hbm.3, bf16[2048,128]{1,0:T(8,128)(2,1)} %wu.3, bf16[2048,128]{1,0:T(8,128)(2,1)} %wg.3, bf16[1296,256]{1,0:T(8,128)(2,1)S(1)} %get-tuple-element.24.px.after), custom_call_target="tpu_custom_call" | custom-call | flops 1073741824 | bytes 6291456 | tf_op jit(solution)/shard_map/glu/pallas_call | solution.py:159
  15.8 2.2 %convolve.1 = f32[8,136,128]{2,1,0:T(8,128)} custom-call(bf16[1024,128]{1,0:T(8,128)(2,1)S(1)} %glu.1.gated, bf16[32,128]{1,0:T(8,128)(2,1)S(1)} %collective-permute-done.6.halo, f32[31,128]{1,0:T(8,128)S(1)} %copy-done, f32[1,128]{1,0:T(1,128)S(1)} %bitcast.4), custom_call_target="tpu_custom_call" | custom-call | flops 520093696 | bytes 1048576 | tf_op jit(solution)/shard_map/convolve/pallas_call | solution.py:196
  18.1 4.5 %all-to-all-start = ((f32[8,136,128]{2,1,0:T(8,128)}), f32[8,136,128]{2,1,0:T(8,128)S(1)}, u32[]{:S(2)}, u32[]{:S(2)}) async-start(f32[8,136,128]{2,1,0:T(8,128)} %convolve.1), calls=%async_computation | async-start | bytes 1114112 | tf_op jit(solution)/shard_map/all_to_all | solution.py:518
  22.5 2.1 %collective-permute-start.3 = (bf16[1296,256]{1,0:T(8,128)(2,1)S(1)}, bf16[1296,256]{1,0:T(8,128)(2,1)S(1)}, u32[]{:S(2)}, u32[]{:S(2)}) collective-permute-start(bf16[1296,256]{1,0:T(8,128)(2,1)S(1)} %get-tuple-element.25.pz), channel_id=1, source_target_pairs={{0,96},{8,104},{16,112},{24,120},{32,0},{40,8},{48,16},{56,24},{64... | collective-permute-start | bytes 1990664 | tf_op jit(solution)/shard_map/ppermute | solution.py:515
  24.7 1.2 %collective-permute-start.2 = (bf16[1296,256]{1,0:T(8,128)(2,1)S(1)}, bf16[1296,256]{1,0:T(8,128)(2,1)}, u32[]{:S(2)}, u32[]{:S(2)}) collective-permute-start(bf16[1296,256]{1,0:T(8,128)(2,1)S(1)} %get-tuple-element.24.px.after), channel_id=1, source_target_pairs={{0,8},{8,16},{16,24},{24,0},{32,40},{40,48},{48,56},{56,32},{64,72... | collective-permute-start | bytes 1990664 | tf_op jit(solution)/shard_map/ppermute | solution.py:514
  26.7 1.8 %collective-permute-start.4 = (bf16[1296,256]{1,0:T(8,128)(2,1)S(1)}, bf16[1296,256]{1,0:T(8,128)(2,1)}, u32[]{:S(2)}, u32[]{:S(2)}) collective-permute-start(bf16[1296,256]{1,0:T(8,128)(2,1)S(1)} %get-tuple-element.25.pz), channel_id=1, source_target_pairs={{0,64},{8,72},{16,80},{24,88},{32,96},{40,104},{48,112},{56,120},{... | collective-permute-start | bytes 1990664 | tf_op jit(solution)/shard_map/ppermute | solution.py:515
  28.5 2.2 %collective-permute-start.1 = (bf16[1296,256]{1,0:T(8,128)(2,1)S(1)}, bf16[1296,256]{1,0:T(8,128)(2,1)}, u32[]{:S(2)}, u32[]{:S(2)}) collective-permute-start(bf16[1296,256]{1,0:T(8,128)(2,1)S(1)} %get-tuple-element.24.px.after), channel_id=1, source_target_pairs={{0,16},{8,24},{16,0},{24,8},{32,48},{40,56},{48,32},{56,40},{64,80... | collective-permute-start | bytes 1990664 | tf_op jit(solution)/shard_map/ppermute | solution.py:514
  30.7 1.8 %diagonal.1 = (f32[2,512,128]{2,1,0:T(8,128)S(1)}, f32[2,512,128]{2,1,0:T(8,128)S(1)}, f32[2,512,128]{2,1,0:T(8,128)S(1)}) custom-call(bf16[1296,256]{1,0:T(8,128)(2,1)S(1)} %get-tuple-element.24.px.after, bf16[1296,256]{1,0:T(8,128)(2,1)S(1)} %get-tuple-element.25.pz), custom_call_target="tpu_custom_call" | custom-call | flops 1073741824 | bytes 4194304 | tf_op jit(solution)/shard_map/diagonal/pallas_call | solution.py:238
  34.9 3.7 %conv_out.1 = (f32[128,2048]{1,0:T(8,128)S(1)}, bf16[1024,2048]{1,0:T(8,128)(2,1)S(1)}) custom-call(f32[8,136,128]{2,1,0:T(8,128)S(1)} %all-to-all-done.parts, bf16[2048,2048]{1,0:T(8,128)(2,1)} %w_hbm.1), custom_call_target="tpu_custom_call" | custom-call | flops 2147483648 | bytes 6291456 | tf_op jit(solution)/shard_map/conv_out/pallas_call | solution.py:464
  38.6 15.2 %collective-permute-done.3.z1 = bf16[1296,256]{1,0:T(8,128)(2,1)S(1)} collective-permute-done((bf16[1296,256]{1,0:T(8,128)(2,1)S(1)}, bf16[1296,256]{1,0:T(8,128)(2,1)S(1)}, u32[]{:S(2)}, u32[]{:S(2)}) %collective-permute-start.3) | collective-permute-done | bytes 663584 | tf_op jit(solution)/shard_map/ppermute | solution.py:515
  53.8 3.2 %collective-permute-done.x1 = bf16[1296,256]{1,0:T(8,128)(2,1)} collective-permute-done((bf16[1296,256]{1,0:T(8,128)(2,1)S(1)}, bf16[1296,256]{1,0:T(8,128)(2,1)}, u32[]{:S(2)}, u32[]{:S(2)}) %collective-permute-start) | collective-permute-done | bytes 663584 | tf_op jit(solution)/shard_map/ppermute | solution.py:514
  57.0 10.0 %attend_near.1 = (f32[8,512,128]{2,1,0:T(8,128)S(1)}, f32[8,512,128]{2,1,0:T(8,128)S(1)}, f32[8,512,128]{2,1,0:T(8,128)S(1)}) custom-call(s32[16,2,16]{2,1,0:T(2,128)S(1)} %copy-done.3, s32[1]{0:T(128)} %bitcast.own, bf16[1296,256]{1,0:T(8,128)(2,1)S(1)} %get-tuple-element.24.px.after, bf16[1296,256]{1,0:T(8,128)(2,1)} %collective-permute-done.x1, ...), custom_call_target="tpu_custom_call" | custom-call | flops 4294967296 | bytes 8388608 | tf_op jit(solution)/shard_map/attend_near/pallas_call | solution.py:381
  67.0 10.1 %attend_far.1 = (f32[2,512,128]{2,1,0:T(8,128)S(1)}, f32[2,512,128]{2,1,0:T(8,128)S(1)}, bf16[528,128]{1,0:T(8,128)(2,1)S(1)}, bf16[528,128]{1,0:T(8,128)(2,1)S(...) custom-call(s32[16,2,16]{2,1,0:T(2,128)S(1)} %copy-done.3, ...), custom_call_target="tpu_custom_call" | custom-call | flops 3758096384 | bytes 8388608 | tf_op jit(solution)/shard_map/attend_far/pallas_call | solution.py:396
  77.2 2.9 %collective-permute-start.8 = (bf16[528,128]{1,0:T(8,128)(2,1)S(1)}, bf16[528,128]{1,0:T(8,128)(2,1)S(1)}, u32[]{:S(2)}, u32[]{:S(2)}) collective-permute-start(bf16[528,128]{1,0:T(8,128)(2,1)S(1)} %get-tuple-element.37), channel_id=1, source_target_pairs={{0,16},{8,24},{16,0},{24,8},{32,48},{40,56},{48,32},{56,40},{64,80... | collective-permute-start | bytes 405512 | tf_op jit(solution)/shard_map/ppermute | solution.py:525
  80.0 2.4 %collective-permute-start.9 = (bf16[528,128]{1,0:T(8,128)(2,1)S(1)}, bf16[528,128]{1,0:T(8,128)(2,1)S(1)}, u32[]{:S(2)}, u32[]{:S(2)}) collective-permute-start(bf16[528,128]{1,0:T(8,128)(2,1)S(1)} %get-tuple-element.38), channel_id=1, source_target_pairs={{0,24},{8,0},{16,8},{24,16},{32,56},{40,32},{48,40},{56,48},{64,88... | collective-permute-start | bytes 405512 | tf_op jit(solution)/shard_map/ppermute | solution.py:525
  82.6 3.4 %collective-permute-start.11 = (bf16[528,128]{1,0:T(8,128)(2,1)S(1)}, bf16[528,128]{1,0:T(8,128)(2,1)S(1)}, u32[]{:S(2)}, u32[]{:S(2)}) collective-permute-start(bf16[528,128]{1,0:T(8,128)(2,1)S(1)} %get-tuple-element.40), channel_id=1, source_target_pairs={{0,64},{8,72},{16,80},{24,88},{32,96},{40,104},{48,112},{56,120},{... | collective-permute-start | bytes 405512 | tf_op jit(solution)/shard_map/ppermute | solution.py:526
  86.0 0.9 collective-permute-start.12
  86.9 1.7 %collective-permute-done.10.b1 = bf16[528,128]{1,0:T(8,128)(2,1)S(1)} collective-permute-done((bf16[528,128]{1,0:T(8,128)(2,1)S(1)}, bf16[528,128]{1,0:T(8,128)(2,1)S(1)}, u32[]{:S(2)}, u32[]{:S(2)}) %collective-permute-start.10) | collective-permute-done | bytes 135200 | tf_op jit(solution)/shard_map/ppermute | solution.py:526
  88.6 1.8 %collective-permute-done.11.b2 = bf16[528,128]{1,0:T(8,128)(2,1)S(1)} collective-permute-done((bf16[528,128]{1,0:T(8,128)(2,1)S(1)}, bf16[528,128]{1,0:T(8,128)(2,1)S(1)}, u32[]{:S(2)}, u32[]{:S(2)}) %collective-permute-start.11) | collective-permute-done | bytes 135200 | tf_op jit(solution)/shard_map/ppermute | solution.py:526
  91.7 11.7 %all_to_all.10.parts = bf16[8,128,128]{2,1,0:T(8,128)(2,1)S(1)} all-to-all(bf16[8,128,128]{2,1,0:T(8,128)(2,1)S(1)} %combine.1), channel_id=1, replica_groups=mesh['sp'=16,'tp'=8] {'tp'}, dimensions={0} | all-to-all | bytes 524288 | tf_op jit(solution)/shard_map/all_to_all | solution.py:528
  103.5 1.6 %attn_out.1 = bf16[128,2048]{1,0:T(8,128)(2,1)} custom-call(bf16[8,128,128]{2,1,0:T(8,128)(2,1)S(1)} %all_to_all.10.parts, f32[128,2048]{1,0:T(8,128)S(1)} %get-tuple-element.30.after.conv, bf16[1024,2048]{1,0:T(8,128)(2,1)S(1)} %get-tuple-element.42.w), custom_call_target="tpu_custom_call" | custom-call | flops 2147483648 | bytes 6291456 | tf_op jit(solution)/shard_map/attn_out/pallas_call | solution.py:492
  (34 shorter events, 5.5 us)
Async XLA Ops:
  0.0 0.7 copy-start.1
  6.0 9.8 %copy-start = (f32[31,128]{1,0:T(8,128)S(1)}, f32[31,128]{1,0:T(8,128)}, u32[]{:S(2)}) copy-start(f32[31,128]{1,0:T(8,128)} %taps.1) | copy-start | bytes 47620
  6.0 9.8 %copy-start.2 = (f32[128]{0:T(128)S(1)}, f32[128]{0:T(128)}, u32[]{:S(2)}) copy-start(f32[128]{0:T(128)} %param.18) | copy-start | bytes 1540
  6.0 22.5 %collective-permute-start.5 = (bf16[1296,256]{1,0:T(8,128)(2,1)S(1)}, bf16[1296,256]{1,0:T(8,128)(2,1)S(1)}, u32[]{:S(2)}, u32[]{:S(2)}) collective-permute-start(bf16[1296,256]{1,0:T(8,128)(2,1)S(1)} %get-tuple-element.25.pz), channel_id=1, source_target_pairs={{0,32},{8,40},{16,48},{24,56},{32,64},{40,72},{48,80},{56,88},{64,... | collective-permute-start | bytes 1990664 | tf_op jit(solution)/shard_map/ppermute | solution.py:515
  8.0 7.8 %collective-permute-start.6 = (bf16[32,128]{1,0:T(8,128)(2,1)S(1)}, bf16[32,128]{1,0:T(8,128)(2,1)S(1)}, u32[]{:S(2)}, u32[]{:S(2)}) collective-permute-start(bf16[32,128]{1,0:T(8,128)(2,1)S(1)} %get-tuple-element.29), channel_id=1, source_target_pairs={{0,8},{8,16},{16,24},{24,32},{32,40},{40,48},{48,56},{56,64},{64,7... | collective-permute-start | bytes 24584 | tf_op jit(solution)/shard_map/ppermute | solution.py:511
  18.1 16.8 %all-to-all-start = ((f32[8,136,128]{2,1,0:T(8,128)}), f32[8,136,128]{2,1,0:T(8,128)S(1)}, u32[]{:S(2)}, u32[]{:S(2)}) async-start(f32[8,136,128]{2,1,0:T(8,128)} %convolve.1), calls=%async_computation | async-start | bytes 1114112 | tf_op jit(solution)/shard_map/all_to_all | solution.py:518
  22.5 31.2 %collective-permute-start.3 = (bf16[1296,256]{1,0:T(8,128)(2,1)S(1)}, bf16[1296,256]{1,0:T(8,128)(2,1)S(1)}, u32[]{:S(2)}, u32[]{:S(2)}) collective-permute-start(bf16[1296,256]{1,0:T(8,128)(2,1)S(1)} %get-tuple-element.25.pz), channel_id=1, source_target_pairs={{0,96},{8,104},{16,112},{24,120},{32,0},{40,8},{48,16},{56,24},{64... | collective-permute-start | bytes 1990664 | tf_op jit(solution)/shard_map/ppermute | solution.py:515
  24.7 29.1 %collective-permute-start.2 = (bf16[1296,256]{1,0:T(8,128)(2,1)S(1)}, bf16[1296,256]{1,0:T(8,128)(2,1)}, u32[]{:S(2)}, u32[]{:S(2)}) collective-permute-start(bf16[1296,256]{1,0:T(8,128)(2,1)S(1)} %get-tuple-element.24.px.after), channel_id=1, source_target_pairs={{0,8},{8,16},{16,24},{24,0},{32,40},{40,48},{48,56},{56,32},{64,72... | collective-permute-start | bytes 1990664 | tf_op jit(solution)/shard_map/ppermute | solution.py:514
  25.9 31.1 %collective-permute-start = (bf16[1296,256]{1,0:T(8,128)(2,1)S(1)}, bf16[1296,256]{1,0:T(8,128)(2,1)}, u32[]{:S(2)}, u32[]{:S(2)}) collective-permute-start(bf16[1296,256]{1,0:T(8,128)(2,1)S(1)} %get-tuple-element.24.px.after), channel_id=1, source_target_pairs={{0,24},{8,0},{16,8},{24,16},{32,56},{40,32},{48,40},{56,48},{64,88... | collective-permute-start | bytes 1990664 | tf_op jit(solution)/shard_map/ppermute | solution.py:514
  26.7 40.3 %collective-permute-start.4 = (bf16[1296,256]{1,0:T(8,128)(2,1)S(1)}, bf16[1296,256]{1,0:T(8,128)(2,1)}, u32[]{:S(2)}, u32[]{:S(2)}) collective-permute-start(bf16[1296,256]{1,0:T(8,128)(2,1)S(1)} %get-tuple-element.25.pz), channel_id=1, source_target_pairs={{0,64},{8,72},{16,80},{24,88},{32,96},{40,104},{48,112},{56,120},{... | collective-permute-start | bytes 1990664 | tf_op jit(solution)/shard_map/ppermute | solution.py:515
  28.5 38.4 %collective-permute-start.1 = (bf16[1296,256]{1,0:T(8,128)(2,1)S(1)}, bf16[1296,256]{1,0:T(8,128)(2,1)}, u32[]{:S(2)}, u32[]{:S(2)}) collective-permute-start(bf16[1296,256]{1,0:T(8,128)(2,1)S(1)} %get-tuple-element.24.px.after), channel_id=1, source_target_pairs={{0,16},{8,24},{16,0},{24,8},{32,48},{40,56},{48,32},{56,40},{64,80... | collective-permute-start | bytes 1990664 | tf_op jit(solution)/shard_map/ppermute | solution.py:514
  32.5 0.8 copy-start.4
  33.3 0.8 copy-start.6
  34.1 0.8 copy-start.8
  34.9 22.1 %copy-start.3 = (s32[16,2,16]{2,1,0:T(2,128)S(1)}, s32[16,2,16]{2,1,0:T(2,128)}, u32[]{:S(2)}) copy-start(s32[16,2,16]{2,1,0:T(2,128)} %constant.8.clone.table) | copy-start | bytes 6148
  34.9 22.1 %copy-start.5 = (f32[2,512,128]{2,1,0:T(8,128)S(1)}, f32[2,512,128]{2,1,0:T(8,128)}, u32[]{:S(2)}) copy-start(f32[2,512,128]{2,1,0:T(8,128)} %copy-done.4) | copy-start | bytes 1572868
  34.9 22.1 %copy-start.7 = (f32[2,512,128]{2,1,0:T(8,128)S(1)}, f32[2,512,128]{2,1,0:T(8,128)}, u32[]{:S(2)}) copy-start(f32[2,512,128]{2,1,0:T(8,128)} %copy-done.6) | copy-start | bytes 1572868
  34.9 22.1 %copy-start.9 = (f32[2,512,128]{2,1,0:T(8,128)S(1)}, f32[2,512,128]{2,1,0:T(8,128)}, u32[]{:S(2)}) copy-start(f32[2,512,128]{2,1,0:T(8,128)} %copy-done.8) | copy-start | bytes 1572868
  77.1 8.9 %collective-permute-start.7 = (bf16[528,128]{1,0:T(8,128)(2,1)S(1)}, bf16[528,128]{1,0:T(8,128)(2,1)S(1)}, u32[]{:S(2)}, u32[]{:S(2)}) collective-permute-start(bf16[528,128]{1,0:T(8,128)(2,1)S(1)} %get-tuple-element.36), channel_id=1, source_target_pairs={{0,8},{8,16},{16,24},{24,0},{32,40},{40,48},{48,56},{56,32},{64,72... | collective-permute-start | bytes 405512 | tf_op jit(solution)/shard_map/ppermute | solution.py:525
  77.2 9.8 %collective-permute-start.8 = (bf16[528,128]{1,0:T(8,128)(2,1)S(1)}, bf16[528,128]{1,0:T(8,128)(2,1)S(1)}, u32[]{:S(2)}, u32[]{:S(2)}) collective-permute-start(bf16[528,128]{1,0:T(8,128)(2,1)S(1)} %get-tuple-element.37), channel_id=1, source_target_pairs={{0,16},{8,24},{16,0},{24,8},{32,48},{40,56},{48,32},{56,40},{64,80... | collective-permute-start | bytes 405512 | tf_op jit(solution)/shard_map/ppermute | solution.py:525
  80.0 6.9 %collective-permute-start.9 = (bf16[528,128]{1,0:T(8,128)(2,1)S(1)}, bf16[528,128]{1,0:T(8,128)(2,1)S(1)}, u32[]{:S(2)}, u32[]{:S(2)}) collective-permute-start(bf16[528,128]{1,0:T(8,128)(2,1)S(1)} %get-tuple-element.38), channel_id=1, source_target_pairs={{0,24},{8,0},{16,8},{24,16},{32,56},{40,32},{48,40},{56,48},{64,88... | collective-permute-start | bytes 405512 | tf_op jit(solution)/shard_map/ppermute | solution.py:525
  82.4 6.2 %collective-permute-start.10 = (bf16[528,128]{1,0:T(8,128)(2,1)S(1)}, bf16[528,128]{1,0:T(8,128)(2,1)S(1)}, u32[]{:S(2)}, u32[]{:S(2)}) collective-permute-start(bf16[528,128]{1,0:T(8,128)(2,1)S(1)} %get-tuple-element.39), channel_id=1, source_target_pairs={{0,32},{8,40},{16,48},{24,56},{32,64},{40,72},{48,80},{56,88},{64,... | collective-permute-start | bytes 405512 | tf_op jit(solution)/shard_map/ppermute | solution.py:526
  82.6 7.9 %collective-permute-start.11 = (bf16[528,128]{1,0:T(8,128)(2,1)S(1)}, bf16[528,128]{1,0:T(8,128)(2,1)S(1)}, u32[]{:S(2)}, u32[]{:S(2)}) collective-permute-start(bf16[528,128]{1,0:T(8,128)(2,1)S(1)} %get-tuple-element.40), channel_id=1, source_target_pairs={{0,64},{8,72},{16,80},{24,88},{32,96},{40,104},{48,112},{56,120},{... | collective-permute-start | bytes 405512 | tf_op jit(solution)/shard_map/ppermute | solution.py:526
  86.0 5.0 %collective-permute-start.12 = (bf16[528,128]{1,0:T(8,128)(2,1)S(1)}, bf16[528,128]{1,0:T(8,128)(2,1)S(1)}, u32[]{:S(2)}, u32[]{:S(2)}) collective-permute-start(bf16[528,128]{1,0:T(8,128)(2,1)S(1)} %get-tuple-element.41), channel_id=1, source_target_pairs={{0,96},{8,104},{16,112},{24,120},{32,0},{40,8},{48,16},{56,24},{64... | collective-permute-start | bytes 405512 | tf_op jit(solution)/shard_map/ppermute | solution.py:526

commit v4 on v3

--- a/solution.py
+++ b/solution.py
@@ -91,27 +91,23 @@
     return table
 
 
-def start_copies(x_hbm, weights, x, w, sems):
-    copies = []
-    for n, source in enumerate(weights):
-        dest = w.at[:, pl.ds(128 * n, 128)]
-        copies.append(pltpu.make_async_copy(source, dest, sems.at[4 + n]))
-    for i in range(4):
-        rows = pl.ds(256 * i, 256)
-        copies.append(pltpu.make_async_copy(x_hbm.at[rows], x.at[rows], sems.at[i]))
-    for c in copies:
-        c.start()
-    for c in copies[:-4]:
-        c.wait()
-    return copies[-4:]
-
-
 def gate_rows(both):
     return (both[:, :128] * jax.nn.sigmoid(both[:, 128:])).astype(BF16)
 
 
-def project_kernel(x_hbm, wq, wk, wv, wu, wg, gate, px, pz, tail, x, w, sems):
-    arrivals = start_copies(x_hbm, (wk, wv, wq, wu, wg), x, w, sems)
+def project_kernel(x_hbm, wq, wk, wv, wu, wg, gate, px, pz, gated, tail, x, w, sems):
+    arrivals = [
+        pltpu.make_async_copy(
+            x_hbm.at[pl.ds(256 * i, 256)], x.at[pl.ds(256 * i, 256)], sems.at[i]
+        )
+        for i in range(4)
+    ]
+    loads = [
+        pltpu.make_async_copy(source, w.at[:, pl.ds(128 * n, 128)], sems.at[4 + n])
+        for n, source in enumerate((wk, wv, wq, wu, wg))
+    ]
+    for c in (*loads[:3], *arrivals, *loads[3:]):
+        c.start()
     zero = jnp.zeros((8, 128), BF16)
     top, mid, low = split3(gate[...] * (-LOG2E))
     gates = jnp.concatenate(
@@ -119,57 +115,46 @@
     )
     px[GATE_ROW : GATE_ROW + 16, :] = gates
     pz[GATE_ROW : GATE_ROW + 16, :] = gates
+    for c in loads[:3]:
+        c.wait()
     for i in range(4):
         arrivals[i].wait()
-        out = dot(x[256 * i : 256 * i + 256, :], w[:, :384]).astype(BF16)
-        px[256 * i : 256 * i + 256, :] = out[:, :256]
-        pz[256 * i : 256 * i + 256, :] = out[:, :256]
+        out = dot(x[256 * i : 256 * i + 256, :], w[:, :384])
+        both = out[:, :256].astype(BF16)
+        px[256 * i : 256 * i + 256, :] = both
+        pz[256 * i : 256 * i + 256, :] = both
         dest = px if i < 2 else pz
         lane = 128 * (i % 2)
-        dest[QUERY_ROW:PACK_ROWS, lane : lane + 128] = out[:, 256:]
-    tail[...] = gate_rows(dot(x[TOK - 32 :, :], w[:, 384:]))
+        dest[QUERY_ROW:PACK_ROWS, lane : lane + 128] = (out[:, 256:] * SCALE).astype(BF16)
+    for c in loads[3:]:
+        c.wait()
+    for i in range(4):
+        rows = gate_rows(dot(x[256 * i : 256 * i + 256, :], w[:, 384:]))
+        gated[256 * i : 256 * i + 256, :] = rows
+    tail[...] = rows[224:, :]
 
 
 def project(x, wq, wk, wv, wu, wg, gate):
     pack = jax.ShapeDtypeStruct((PACK_ROWS, 256), BF16)
     return pl.pallas_call(
         project_kernel,
-        out_shape=(pack, pack, jax.ShapeDtypeStruct((32, 128), BF16)),
+        out_shape=(
+            pack,
+            pack,
+            jax.ShapeDtypeStruct((TOK, 128), BF16),
+            jax.ShapeDtypeStruct((32, 128), BF16),
+        ),
         in_specs=[HBM] * 6 + [VM],
-        out_specs=(VM, VM, VM),
+        out_specs=(VM,) * 4,
         scratch_shapes=[
             pltpu.VMEM((TOK, 2048), BF16),
             pltpu.VMEM((2048, 640), BF16),
             pltpu.SemaphoreType.DMA((9,)),
         ],
         compiler_params=params(12),
-        cost_estimate=cost(2 * TOK * 2048 * 512, 8 << 20),
+        cost_estimate=cost(2 * TOK * 2048 * 640, 8 << 20),
         name="project",
     )(x, wq, wk, wv, wu, wg, gate)
-
-
-def glu_kernel(x_hbm, wu, wg, after, out, x, w, sems):
-    arrivals = start_copies(x_hbm, (wu, wg), x, w, sems)
-    for i in range(4):
-        arrivals[i].wait()
-        out[256 * i : 256 * i + 256, :] = gate_rows(dot(x[256 * i : 256 * i + 256, :], w[...]))
-
-
-def glu(x, wu, wg, after):
-    return pl.pallas_call(
-        glu_kernel,
-        out_shape=jax.ShapeDtypeStruct((TOK, 128), BF16),
-        in_specs=[HBM, HBM, HBM, ANY],
-        out_specs=VM,
-        scratch_shapes=[
-            pltpu.VMEM((TOK, 2048), BF16),
-            pltpu.VMEM((2048, 256), BF16),
-            pltpu.SemaphoreType.DMA((6,)),
-        ],
-        compiler_params=params(10),
-        cost_estimate=cost(2 * TOK * 2048 * 256, 6 << 20),
-        name="glu",
-    )(x, wu, wg, after)
 
 
 def conv_kernel(gated, halo, taps, gain, out, padded):
@@ -205,7 +190,7 @@
     )(gated, halo, taps, gain)
 
 
-def diagonal_kernel(px, pz, m_out, l_out, acc_out):
+def diagonal(px, pz, m, l, acc):
     top = px[GATE_ROW : GATE_ROW + 8, :].astype(F32)
     low = px[GATE_ROW + 8 : GATE_ROW + 16, :].astype(F32)
     gates = top[:, :128] + top[:, 128:] + low[:, :128]
@@ -221,39 +206,38 @@
         lane = lax.broadcasted_iota(I32, (HALF, 128), 1)
         parts = []
         for c in range(keys // 128):
-            t = scores[:, 128 * c : 128 * c + 128] * SCALE + gates[c : c + 1, :]
+            t = scores[:, 128 * c : 128 * c + 128] + gates[c : c + 1, :]
             parts.append(jnp.where(lane + 128 * c <= row, t, LOW))
         most = functools.reduce(jnp.maximum, parts)
         most = jnp.broadcast_to(jnp.max(most, axis=1, keepdims=True), (HALF, 128))
         weights = [jnp.exp2(t - most) for t in parts]
-        m_out[half] = most
-        l_out[half] = functools.reduce(jnp.add, weights)
-        acc_out[half] = dot(
-            jnp.concatenate([w.astype(BF16) for w in weights], axis=1), px[:keys, 128:]
-        )
-
-
-def diagonal(px, pz):
-    state = jax.ShapeDtypeStruct((2, HALF, 128), F32)
-    return pl.pallas_call(
-        diagonal_kernel,
-        out_shape=(state, state, state),
-        in_specs=[VM, VM],
-        out_specs=(VM, VM, VM),
-        compiler_params=params(16),
-        cost_estimate=cost(2 * HALF * 2048 * 512, 4 << 20),
-        name="diagonal",
-    )(px, pz)
+        m[4 * half] = most
+        rounded = jnp.concatenate([w.astype(BF16) for w in weights], axis=1)
+        ones = jnp.ones((keys, 128), BF16)
+        out = dot(rounded, jnp.concatenate([px[:keys, 128:], ones], axis=1))
+        acc[4 * half] = out[:, :128]
+        l[4 * half] = out[:, 128:]
 
 
 PACKS = 8
 NEAR, FAR = 8, 7
 
 
-def load_packs(sources, packs, query, gates, sems):
-    copies = [pltpu.make_async_copy(src, packs.at[n], sems.at[n]) for n, src in sources]
+def start_packs(sources, packs, sems):
+    rows = PACK_ROWS // 3
+    copies = [
+        pltpu.make_async_copy(
+            src.at[pl.ds(rows * i, rows)], packs.at[n, pl.ds(rows * i, rows)], sems.at[3 * n + i]
+        )
+        for n, src in sources
+        for i in range(3)
+    ]
     for c in copies:
         c.start()
+    return copies
+
+
+def finish_packs(copies, sources, packs, query, gates):
     for c in copies:
         c.wait()
     for slot, _ in sources:
@@ -278,7 +262,7 @@
         )
         best = None
         for c in range(8):
-            t = raw[:, 128 * c : 128 * c + 128] * SCALE + gates[k, c : c + 1, :]
+            t = raw[:, 128 * c : 128 * c + 128] + gates[k, c : c + 1, :]
             s[:, 128 * c : 128 * c + 128] = t
             best = t if best is None else jnp.maximum(best, t)
         old = m[q]
@@ -292,10 +276,11 @@
         top = most[...]
         by = shrink[...]
         w = [jnp.exp2(s[:, 128 * c : 128 * c + 128] - top) for c in range(8)]
-        total = ((w[0] + w[1]) + (w[2] + w[3])) + ((w[4] + w[5]) + (w[6] + w[7]))
         rounded = jnp.concatenate([v.astype(BF16) for v in w], axis=1)
-        l[q] = l[q] * by + total
-        acc[q] = acc[q] * by + dot(rounded, packs[k, :TOK, 128:])
+        ones = jnp.ones((TOK, 128), BF16)
+        out = dot(rounded, jnp.concatenate([packs[k, :TOK, 128:], ones], axis=1))
+        acc[q] = acc[q] * by + out[:, :128]
+        l[q] = l[q] * by + out[:, 128:]
 
 
     scores_of(start, *first)
@@ -318,29 +303,31 @@
 
 
 def near_kernel(
-    table, own, px, x1, x3, pz, z1, z3, m_in, l_in, acc_in, after, m, l, acc,
-    packs, query, gates, sems, *per_tile,
+    table, own, px, x1, x3, pz, z1, z3, m, l, acc, packs, query, gates, sems, *per_tile
 ):
     sources = ((0, px), (1, x1), (3, x3), (4, pz), (5, z1), (7, z3))
-    for half in range(2):
-        m[4 * half] = m_in[half]
-        l[4 * half] = l_in[half]
-        acc[4 * half] = acc_in[half]
+    copies = start_packs(sources, packs, sems)
     for n in (1, 3, 5, 7):
         m[n] = jnp.full((HALF, 128), LOW, F32)
         l[n] = jnp.zeros((HALF, 128), F32)
         acc[n] = jnp.zeros((HALF, 128), F32)
-    load_packs(sources, packs, query, gates, sems)
+    diagonal(px, pz, m, l, acc)
+    finish_packs(copies, sources, packs, query, gates)
     run_tiles(table, own, 0, NEAR, packs, query, gates, per_tile, m, l, acc)
 
 
 def far_kernel(
-    table, own, px, x1, x2, x3, pz, z1, z2, z3, m_in, l_in, acc_in,
+    table, own, x2, z2, m_in, l_in, acc_in, packs_in, query_in, gates_in,
     o_own, lse_own, a1, a2, a3, b1, b2, b3,
     packs, query, gates, sems, m, l, acc, *per_tile,
 ):
-    sources = ((0, px), (1, x1), (2, x2), (3, x3), (4, pz), (5, z1), (6, z2), (7, z3))
+    sources = ((2, x2), (6, z2))
+    copies = start_packs(sources, packs, sems)
     for n in (0, 1, 3, 4, 5, 7):
+        if n != 4:
+            packs[n, :TOK, :] = packs_in[n, :TOK, :]
+        query[n] = query_in[n]
+        gates[n] = gates_in[n]
         m[n] = m_in[n]
         l[n] = l_in[n]
         acc[n] = acc_in[n]
@@ -348,10 +335,10 @@
         m[n] = jnp.full((HALF, 128), LOW, F32)
         l[n] = jnp.zeros((HALF, 128), F32)
         acc[n] = jnp.zeros((HALF, 128), F32)
-    load_packs(sources, packs, query, gates, sems)
+    finish_packs(copies, sources, packs, query, gates)
     run_tiles(table, own, NEAR, FAR, packs, query, gates, per_tile, m, l, acc)
     for n, out in enumerate((None, a1, a2, a3, None, b1, b2, b3)):
-        total = jnp.maximum(jnp.sum(l[n], axis=1, keepdims=True), TINY)
+        total = jnp.maximum(l[n], TINY)
         mixed = acc[n] / total
         lse = m[n] + jnp.log2(total)
         if out is None:
@@ -366,43 +353,49 @@
             )
 
 
-SLOT_SCRATCH = [
-    pltpu.VMEM((PACKS, PACK_ROWS, 256), BF16),
-    pltpu.VMEM((PACKS, HALF, 128), BF16),
-    pltpu.VMEM((PACKS, 8, 128), F32),
-    pltpu.SemaphoreType.DMA((PACKS,)),
+SEMS = [pltpu.SemaphoreType.DMA((3 * PACKS,))]
+SLOTS = [
+    ((PACKS, PACK_ROWS, 256), BF16),
+    ((PACKS, HALF, 128), BF16),
+    ((PACKS, 8, 128), F32),
 ]
-TILE_SCRATCH = [pltpu.VMEM((HALF, TOK), F32)] * 2 + [pltpu.VMEM((HALF, 128), F32)] * 4
-STATE_SCRATCH = [pltpu.VMEM((PACKS, HALF, 128), F32)] * 3
-
-
-def attend_near(table, own, packs, state, after):
-    kept = jax.ShapeDtypeStruct((PACKS, HALF, 128), F32)
+STATE = [((PACKS, HALF, 128), F32)] * 3
+TILE = [((HALF, TOK), F32)] * 2 + [((HALF, 128), F32)] * 4
+
+
+def arrays(shapes):
+    return tuple(jax.ShapeDtypeStruct(*v) for v in shapes)
+
+
+def scratch(shapes):
+    return [pltpu.VMEM(*v) for v in shapes]
+
+
+def attend_near(table, own, packs):
     return pl.pallas_call(
         near_kernel,
-        out_shape=(kept, kept, kept),
-        in_specs=[SM, SM] + [ANY] * 6 + [VM] * 3 + [ANY],
-        out_specs=(VM,) * 3,
-        scratch_shapes=SLOT_SCRATCH + TILE_SCRATCH,
+        out_shape=arrays(STATE + SLOTS),
+        in_specs=[SM, SM, VM, ANY, ANY, VM, ANY, ANY],
+        out_specs=(VM,) * 6,
+        scratch_shapes=SEMS + scratch(TILE),
         compiler_params=params(24),
         cost_estimate=cost(NEAR * 4 * HALF * TOK * 256, 8 << 20),
         name="attend_near",
-    )(table, own, *packs, *state, after)
-
-
-def attend_far(table, own, packs, state):
-    back = jax.ShapeDtypeStruct((BACK_ROWS, 128), BF16)
-    kept = jax.ShapeDtypeStruct((2, HALF, 128), F32)
+    )(table, own, *packs)
+
+
+def attend_far(table, own, x2, z2, state):
+    outs = [((2, HALF, 128), F32)] * 2 + [((BACK_ROWS, 128), BF16)] * 6
     return pl.pallas_call(
         far_kernel,
-        out_shape=(kept, kept) + (back,) * 6,
-        in_specs=[SM, SM] + [ANY] * 8 + [VM] * 3,
+        out_shape=arrays(outs),
+        in_specs=[SM, SM, ANY, ANY] + [VM] * 6,
         out_specs=(VM,) * 8,
-        scratch_shapes=SLOT_SCRATCH + STATE_SCRATCH + TILE_SCRATCH,
+        scratch_shapes=scratch(SLOTS) + SEMS + scratch(STATE + TILE),
         compiler_params=params(30),
         cost_estimate=cost(FAR * 4 * HALF * TOK * 256, 8 << 20),
         name="attend_far",
-    )(table, own, *packs, *state)
+    )(table, own, x2, z2, *state)
 
 
 def combine_kernel(o_own, lse_own, a1, a2, a3, b1, b2, b3, out):
@@ -507,23 +500,22 @@
     )
     own = lax.axis_index("sp").astype(I32).reshape(1)
     table = jnp.asarray(work_table())
-    px, pz, tail = project(x, wq, wk, wv, wu, wg, gate.reshape(8, 128))
+    px, pz, gated, tail = project(x, wq, wk, wv, wu, wg, gate.reshape(8, 128))
     halo = lax.ppermute(tail, "sp", [(i, i + 1) for i in range(15)])
     xs, zs = [None] * 4, [None] * 4
     for d in (1, 3, 2):
         xs[d] = lax.ppermute(px, "sp", moves(-d, 0))
         zs[d] = lax.ppermute(pz, "sp", moves(0, -d))
-    gated = glu(x, wu, wg, px)
     conv = convolve(gated, halo, taps, gain.reshape(1, 128))
     conv_parts = lax.all_to_all(conv, "tp", 0, 0, tiled=True)
+    near = (px, xs[1], xs[3], pz, zs[1], zs[3])
+    state = attend_near(table, own, near)
+    o_own, lse_own, *sent = attend_far(table, own, xs[2], zs[2], state)
+    backs = [
+        lax.ppermute(sent[n], "sp", moves(*move))
+        for n, move in enumerate(((1, 0), (2, 0), (3, 0), (0, 1), (0, 2), (0, 3)))
+    ]
     conv_mixed, w_attn = conv_out(conv_parts, w_out)
-    state = diagonal(px, pz)
-    near = (px, xs[1], xs[3], pz, zs[1], zs[3])
-    state = attend_near(table, own, near, state, conv_mixed)
-    packs = (px, *xs[1:], pz, *zs[1:])
-    o_own, lse_own, *sent = attend_far(table, own, packs, state)
-    backs = [lax.ppermute(sent[d - 1], "sp", moves(d, 0)) for d in (1, 2, 3)]
-    backs += [lax.ppermute(sent[d + 2], "sp", moves(0, d)) for d in (1, 2, 3)]
     mixed = combine(o_own, lse_own, backs)
     attn_parts = lax.all_to_all(mixed, "tp", 0, 0, tiled=True)
     return attn_out(attn_parts, conv_mixed, w_attn)

time: 105 us -> 107 us (1.019)
  the two profiles are of different devices: /device:TPU:2 before, /device:TPU:1 now
where the time goes in v4:
time: 107 us
  starting transfers between devices  49.9 us (47%)
  Pallas kernels  36.5 us (34%)
  waiting for transfers between devices  13.4 us (13%)
  local copies, waits for them, and re-layouts  6.76 us (6%)
    ppermute x6, starting transfers between devices, layer(): lax.ppermute(sent[n], 'sp', moves(*move))  20.7 us
    pallas_call x1, Pallas kernels, attend_near(): pl.pallas_call(near_kernel, out_shape=arrays(STATE + SLOTS), in_specs=[SM...  12.6 us
    pallas_call x1, Pallas kernels, attend_far(): pl.pallas_call(far_kernel, out_shape=arrays(outs), in_specs=[SM, SM, ANY,...  9.31 us
    ppermute x1, waiting for transfers between devices, layer(): halo = lax.ppermute(tail, 'sp', [(i, i + 1) for i in range(15)])  7.91 us
    ppermute x3, starting transfers between devices, layer(): zs[d] = lax.ppermute(pz, 'sp', moves(0, -d))  7.36 us
    all_to_all x1, starting transfers between devices, layer(): attn_parts = lax.all_to_all(mixed, 'tp', 0, 0, tiled=True)  7.08 us
    unnamed x16, local copies, waits for them, and re-layouts  6.76 us
    all_to_all x1, starting transfers between devices, layer(): conv_parts = lax.all_to_all(conv, 'tp', 0, 0, tiled=True)  6.75 us
  transfers between devices with their start and end apart: 15, of which 5 were waited for; matrix products, arithmetic and copies ran while one was open for 0% of the time, Pallas kernels for 27%

profile of v4, /device:TPU:1, one launch (start us, length us, event | category | flops | bytes accessed | tf_op | source)
XLA Modules:
  0.0 106.7 jit_solution(2534816002705652863)
XLA Ops:
  0.7 5.9 %project.1 = (bf16[1296,256]{1,0:T(8,128)(2,1)S(1)}, bf16[1296,256]{1,0:T(8,128)(2,1)S(1)}, bf16[1024,128]{1,0:T(8,128)(2,1)S(1)}, bf16[32,128]{1,0:T(8,128)(2,1)S(1)}) custom-call(bf16[1024,2048]{1,0:T(8,128)(2,1)} %x_hbm.1, bf16[2048,128]{1,0:T(8,128)(2,1)} %wq.1, bf16[2048,128]{1,0:T(8,128)(2,1)} %wk.1, bf16[2048,128]{1,0:T(8,128)(2,1)} %wv.1, ...), custom_call_target="tpu_custom_call" | custom-call | flops 2684354560 | bytes 8388608 | tf_op jit(solution)/shard_map/project/pallas_call | solution.py:139
  6.6 3.4 %collective-permute-start.2 = (bf16[1296,256]{1,0:T(8,128)(2,1)S(1)}, bf16[1296,256]{1,0:T(8,128)(2,1)S(1)}, u32[]{:S(2)}, u32[]{:S(2)}) collective-permute-start(bf16[1296,256]{1,0:T(8,128)(2,1)S(1)} %get-tuple-element.25.px), channel_id=1, source_target_pairs={{0,24},{8,0},{16,8},{24,16},{32,56},{40,32},{48,40},{56,48},{64,88... | collective-permute-start | bytes 1990664 | tf_op jit(solution)/shard_map/ppermute | solution.py:507
  10.0 3.8 %collective-permute-start.4 = (bf16[1296,256]{1,0:T(8,128)(2,1)S(1)}, bf16[1296,256]{1,0:T(8,128)(2,1)}, u32[]{:S(2)}, u32[]{:S(2)}) collective-permute-start(bf16[1296,256]{1,0:T(8,128)(2,1)S(1)} %get-tuple-element.26.pz), channel_id=1, source_target_pairs={{0,96},{8,104},{16,112},{24,120},{32,0},{40,8},{48,16},{56,24},{64... | collective-permute-start | bytes 1990664 | tf_op jit(solution)/shard_map/ppermute | solution.py:508
  13.8 2.1 %collective-permute-start.12 = (bf16[32,128]{1,0:T(8,128)(2,1)S(1)}, bf16[32,128]{1,0:T(8,128)(2,1)S(1)}, u32[]{:S(2)}, u32[]{:S(2)}) collective-permute-start(bf16[32,128]{1,0:T(8,128)(2,1)S(1)} %get-tuple-element.42), channel_id=1, source_target_pairs={{0,8},{8,16},{16,24},{24,32},{32,40},{40,48},{48,56},{56,64},{64,7... | collective-permute-start | bytes 24584 | tf_op jit(solution)/shard_map/ppermute | solution.py:504
  15.9 7.9 %collective-permute-done.12.halo = bf16[32,128]{1,0:T(8,128)(2,1)S(1)} collective-permute-done((bf16[32,128]{1,0:T(8,128)(2,1)S(1)}, bf16[32,128]{1,0:T(8,128)(2,1)S(1)}, u32[]{:S(2)}, u32[]{:S(2)}) %collective-permute-start.12) | collective-permute-done | bytes 8224 | tf_op jit(solution)/shard_map/ppermute | solution.py:504
  23.8 2.5 %collective-permute-start = (bf16[1296,256]{1,0:T(8,128)(2,1)S(1)}, bf16[1296,256]{1,0:T(8,128)(2,1)S(1)}, u32[]{:S(2)}, u32[]{:S(2)}) collective-permute-start(bf16[1296,256]{1,0:T(8,128)(2,1)S(1)} %get-tuple-element.25.px), channel_id=1, source_target_pairs={{0,16},{8,24},{16,0},{24,8},{32,48},{40,56},{48,32},{56,40},{64,80... | collective-permute-start | bytes 1990664 | tf_op jit(solution)/shard_map/ppermute | solution.py:507
  27.2 3.6 %collective-permute-start.1 = (bf16[1296,256]{1,0:T(8,128)(2,1)S(1)}, bf16[1296,256]{1,0:T(8,128)(2,1)S(1)}, u32[]{:S(2)}, u32[]{:S(2)}) collective-permute-start(bf16[1296,256]{1,0:T(8,128)(2,1)S(1)} %get-tuple-element.26.pz), channel_id=1, source_target_pairs={{0,64},{8,72},{16,80},{24,88},{32,96},{40,104},{48,112},{56,120},{... | collective-permute-start | bytes 1990664 | tf_op jit(solution)/shard_map/ppermute | solution.py:508
  30.8 2.2 %convolve.1 = f32[8,136,128]{2,1,0:T(8,128)} custom-call(bf16[1024,128]{1,0:T(8,128)(2,1)S(1)} %get-tuple-element.41.gated, bf16[32,128]{1,0:T(8,128)(2,1)S(1)} %collective-permute-done.12.halo, f32[31,128]{1,0:T(8,128)S(1)} %copy-done.5, f32[1,128]{1,0:T(1,128)S(1)} %bitcast.4), custom_call_target="tpu_custom_call" | custom-call | flops 520093696 | bytes 1048576 | tf_op jit(solution)/shard_map/convolve/pallas_call | solution.py:181
  33.0 6.7 %all-to-all-start.1 = ((f32[8,136,128]{2,1,0:T(8,128)}), f32[8,136,128]{2,1,0:T(8,128)S(1)}, u32[]{:S(2)}, u32[]{:S(2)}) async-start(f32[8,136,128]{2,1,0:T(8,128)} %convolve.1), calls=%async_computation.1 | async-start | bytes 1114112 | tf_op jit(solution)/shard_map/all_to_all | solution.py:510
  39.8 1.1 %copy-done.4 = bf16[1296,256]{1,0:T(8,128)(2,1)S(1)} copy-done((bf16[1296,256]{1,0:T(8,128)(2,1)S(1)}, bf16[1296,256]{1,0:T(8,128)(2,1)}, u32[]{:S(2)}) %copy-start.4) | copy-done | bytes 663576
  40.9 12.6 %attend_near.1 = (f32[8,512,128]{2,1,0:T(8,128)S(1)}, f32[8,512,128]{2,1,0:T(8,128)S(1)}, f32[8,512,128]{2,1,0:T(8,128)S(1)}, bf16[8,1296,256]{2,1,0:T(8,128)(2,...) custom-call(s32[16,2,16]{2,1,0:T(2,128)S(1)} %copy-done, s32[1]{0:T(128)} %bitcast.own, ...), custom_call_target="tpu_custom_call" | custom-call | flops 4294967296 | bytes 8388608 | tf_op jit(solution)/shard_map/attend_near/pallas_call | solution.py:375
  53.5 9.3 %attend_far.1 = (f32[2,512,128]{2,1,0:T(8,128)S(1)}, f32[2,512,128]{2,1,0:T(8,128)S(1)}, bf16[528,128]{1,0:T(8,128)(2,1)S(1)}, bf16[528,128]{1,0:T(8,128)(2,1)S(...) custom-call(s32[16,2,16]{2,1,0:T(2,128)S(1)} %copy-done, ...), custom_call_target="tpu_custom_call" | custom-call | flops 3758096384 | bytes 8388608 | tf_op jit(solution)/shard_map/attend_far/pallas_call | solution.py:389
  62.9 14.8 %collective-permute-start.11 = (bf16[528,128]{1,0:T(8,128)(2,1)S(1)}, bf16[528,128]{1,0:T(8,128)(2,1)S(1)}, u32[]{:S(2)}, u32[]{:S(2)}) collective-permute-start(bf16[528,128]{1,0:T(8,128)(2,1)S(1)} %get-tuple-element.40), channel_id=1, source_target_pairs={{0,96},{8,104},{16,112},{24,120},{32,0},{40,8},{48,16},{56,24},{64... | collective-permute-start | bytes 405512 | tf_op jit(solution)/shard_map/ppermute | solution.py:515
  77.7 3.2 %collective-permute-start.7 = (bf16[528,128]{1,0:T(8,128)(2,1)S(1)}, bf16[528,128]{1,0:T(8,128)(2,1)S(1)}, u32[]{:S(2)}, u32[]{:S(2)}) collective-permute-start(bf16[528,128]{1,0:T(8,128)(2,1)S(1)} %get-tuple-element.36), channel_id=1, source_target_pairs={{0,16},{8,24},{16,0},{24,8},{32,48},{40,56},{48,32},{56,40},{64,80... | collective-permute-start | bytes 405512 | tf_op jit(solution)/shard_map/ppermute | solution.py:515
  80.9 2.1 %collective-permute-start.8 = (bf16[528,128]{1,0:T(8,128)(2,1)S(1)}, bf16[528,128]{1,0:T(8,128)(2,1)S(1)}, u32[]{:S(2)}, u32[]{:S(2)}) collective-permute-start(bf16[528,128]{1,0:T(8,128)(2,1)S(1)} %get-tuple-element.37), channel_id=1, source_target_pairs={{0,24},{8,0},{16,8},{24,16},{32,56},{40,32},{48,40},{56,48},{64,88... | collective-permute-start | bytes 405512 | tf_op jit(solution)/shard_map/ppermute | solution.py:515
  83.5 1.3 %collective-permute-done.11.b3 = bf16[528,128]{1,0:T(8,128)(2,1)S(1)} collective-permute-done((bf16[528,128]{1,0:T(8,128)(2,1)S(1)}, bf16[528,128]{1,0:T(8,128)(2,1)S(1)}, u32[]{:S(2)}, u32[]{:S(2)}) %collective-permute-start.11) | collective-permute-done | bytes 135200 | tf_op jit(solution)/shard_map/ppermute | solution.py:515
  84.8 2.7 %collective-permute-done.7.a2 = bf16[528,128]{1,0:T(8,128)(2,1)S(1)} collective-permute-done((bf16[528,128]{1,0:T(8,128)(2,1)S(1)}, bf16[528,128]{1,0:T(8,128)(2,1)S(1)}, u32[]{:S(2)}, u32[]{:S(2)}) %collective-permute-start.7) | collective-permute-done | bytes 135200 | tf_op jit(solution)/shard_map/ppermute | solution.py:515
  88.0 1.4 %combine.1 = bf16[8,128,128]{2,1,0:T(8,128)(2,1)} custom-call(f32[2,512,128]{2,1,0:T(8,128)S(1)} %get-tuple-element.33.o_own, f32[2,512,128]{2,1,0:T(8,128)S(1)} %get-tuple-element.34.lse_own, bf16[528,128]{1,0:T(8,128)(2,1)S(1)} %collective-permute-done.6.a1, bf16[528,128]{1,0:T(8,128)(2,1)S(1)} %collective-permute-done.7.a2, ...), custom_call_target="tpu_custom_call" | custom-call | flops 536870912 | bytes 2097152 | tf_op jit(solution)/shard_map/combine/pallas_call | solution.py:420
  89.4 7.1 %all-to-all-start = ((bf16[8,128,128]{2,1,0:T(8,128)(2,1)}), bf16[8,128,128]{2,1,0:T(8,128)(2,1)S(1)}, u32[]{:S(2)}, u32[]{:S(2)}) async-start(bf16[8,128,128]{2,1,0:T(8,128)(2,1)} %combine.1), calls=%async_computation | async-start | bytes 524288 | tf_op jit(solution)/shard_map/all_to_all | solution.py:520
  96.5 3.6 %conv_out.1 = (f32[128,2048]{1,0:T(8,128)S(1)}, bf16[1024,2048]{1,0:T(8,128)(2,1)S(1)}) custom-call(f32[8,136,128]{2,1,0:T(8,128)S(1)} %all-to-all-done.1.parts, bf16[2048,2048]{1,0:T(8,128)(2,1)} %w_hbm.1), custom_call_target="tpu_custom_call" | custom-call | flops 2147483648 | bytes 6291456 | tf_op jit(solution)/shard_map/conv_out/pallas_call | solution.py:457
  100.1 1.9 %copy-done.1 = bf16[1024,2048]{1,0:T(8,128)(2,1)} copy-done((bf16[1024,2048]{1,0:T(8,128)(2,1)}, bf16[1024,2048]{1,0:T(8,128)(2,1)S(1)}, u32[]{:S(2)}) %copy-start.1) | copy-done | bytes 4194328
  102.1 0.9 all-to-all-done.parts
  103.0 2.2 %copy-done.2 = bf16[1024,2048]{1,0:T(8,128)(2,1)S(1)} copy-done((bf16[1024,2048]{1,0:T(8,128)(2,1)S(1)}, bf16[1024,2048]{1,0:T(8,128)(2,1)}, u32[]{:S(2)}) %copy-start.2) | copy-done | bytes 4194328
  105.2 1.5 %attn_out.1 = bf16[128,2048]{1,0:T(8,128)(2,1)} custom-call(bf16[8,128,128]{2,1,0:T(8,128)(2,1)S(1)} %all-to-all-done.parts, f32[128,2048]{1,0:T(8,128)S(1)} %get-tuple-element.43.conv, bf16[1024,2048]{1,0:T(8,128)(2,1)S(1)} %copy-done.2), custom_call_target="tpu_custom_call" | custom-call | flops 2147483648 | bytes 6291456 | tf_op jit(solution)/shard_map/attn_out/pallas_call | solution.py:485
  (29 shorter events, 2.8 us)
Async XLA Ops:
  0.0 0.7 copy-start.6
  0.7 30.1 %copy-start.5 = (f32[31,128]{1,0:T(8,128)S(1)}, f32[31,128]{1,0:T(8,128)}, u32[]{:S(2)}) copy-start(f32[31,128]{1,0:T(8,128)} %taps.1) | copy-start | bytes 47620
  0.7 30.1 %copy-start.7 = (f32[128]{0:T(128)S(1)}, f32[128]{0:T(128)}, u32[]{:S(2)}) copy-start(f32[128]{0:T(128)} %param.18) | copy-start | bytes 1540
  0.7 39.1 %copy-start = (s32[16,2,16]{2,1,0:T(2,128)S(1)}, s32[16,2,16]{2,1,0:T(2,128)}, u32[]{:S(2)}) copy-start(s32[16,2,16]{2,1,0:T(2,128)} %constant.8.clone.table) | copy-start | bytes 6148
  6.6 19.7 %collective-permute-start.2 = (bf16[1296,256]{1,0:T(8,128)(2,1)S(1)}, bf16[1296,256]{1,0:T(8,128)(2,1)S(1)}, u32[]{:S(2)}, u32[]{:S(2)}) collective-permute-start(bf16[1296,256]{1,0:T(8,128)(2,1)S(1)} %get-tuple-element.25.px), channel_id=1, source_target_pairs={{0,24},{8,0},{16,8},{24,16},{32,56},{40,32},{48,40},{56,48},{64,88... | collective-permute-start | bytes 1990664 | tf_op jit(solution)/shard_map/ppermute | solution.py:507
  10.0 29.8 %collective-permute-start.3 = (bf16[1296,256]{1,0:T(8,128)(2,1)S(1)}, bf16[1296,256]{1,0:T(8,128)(2,1)}, u32[]{:S(2)}, u32[]{:S(2)}) collective-permute-start(bf16[1296,256]{1,0:T(8,128)(2,1)S(1)} %get-tuple-element.25.px), channel_id=1, source_target_pairs={{0,8},{8,16},{16,24},{24,0},{32,40},{40,48},{48,56},{56,32},{64,72... | collective-permute-start | bytes 1990664 | tf_op jit(solution)/shard_map/ppermute | solution.py:507
  10.0 29.8 %collective-permute-start.4 = (bf16[1296,256]{1,0:T(8,128)(2,1)S(1)}, bf16[1296,256]{1,0:T(8,128)(2,1)}, u32[]{:S(2)}, u32[]{:S(2)}) collective-permute-start(bf16[1296,256]{1,0:T(8,128)(2,1)S(1)} %get-tuple-element.26.pz), channel_id=1, source_target_pairs={{0,96},{8,104},{16,112},{24,120},{32,0},{40,8},{48,16},{56,24},{64... | collective-permute-start | bytes 1990664 | tf_op jit(solution)/shard_map/ppermute | solution.py:508
  13.8 26.0 %collective-permute-start.5 = (bf16[1296,256]{1,0:T(8,128)(2,1)S(1)}, bf16[1296,256]{1,0:T(8,128)(2,1)}, u32[]{:S(2)}, u32[]{:S(2)}) collective-permute-start(bf16[1296,256]{1,0:T(8,128)(2,1)S(1)} %get-tuple-element.26.pz), channel_id=1, source_target_pairs={{0,32},{8,40},{16,48},{24,56},{32,64},{40,72},{48,80},{56,88},{64,... | collective-permute-start | bytes 1990664 | tf_op jit(solution)/shard_map/ppermute | solution.py:508
  13.8 10.0 %collective-permute-start.12 = (bf16[32,128]{1,0:T(8,128)(2,1)S(1)}, bf16[32,128]{1,0:T(8,128)(2,1)S(1)}, u32[]{:S(2)}, u32[]{:S(2)}) collective-permute-start(bf16[32,128]{1,0:T(8,128)(2,1)S(1)} %get-tuple-element.42), channel_id=1, source_target_pairs={{0,8},{8,16},{16,24},{24,32},{32,40},{40,48},{48,56},{56,64},{64,7... | collective-permute-start | bytes 24584 | tf_op jit(solution)/shard_map/ppermute | solution.py:504
  23.8 29.7 %collective-permute-start = (bf16[1296,256]{1,0:T(8,128)(2,1)S(1)}, bf16[1296,256]{1,0:T(8,128)(2,1)S(1)}, u32[]{:S(2)}, u32[]{:S(2)}) collective-permute-start(bf16[1296,256]{1,0:T(8,128)(2,1)S(1)} %get-tuple-element.25.px), channel_id=1, source_target_pairs={{0,16},{8,24},{16,0},{24,8},{32,48},{40,56},{48,32},{56,40},{64,80... | collective-permute-start | bytes 1990664 | tf_op jit(solution)/shard_map/ppermute | solution.py:507
  26.3 0.9 copy-start.3
  27.2 26.3 %collective-permute-start.1 = (bf16[1296,256]{1,0:T(8,128)(2,1)S(1)}, bf16[1296,256]{1,0:T(8,128)(2,1)S(1)}, u32[]{:S(2)}, u32[]{:S(2)}) collective-permute-start(bf16[1296,256]{1,0:T(8,128)(2,1)S(1)} %get-tuple-element.26.pz), channel_id=1, source_target_pairs={{0,64},{8,72},{16,80},{24,88},{32,96},{40,104},{48,112},{56,120},{... | collective-permute-start | bytes 1990664 | tf_op jit(solution)/shard_map/ppermute | solution.py:508
  33.0 56.4 %all-to-all-start.1 = ((f32[8,136,128]{2,1,0:T(8,128)}), f32[8,136,128]{2,1,0:T(8,128)S(1)}, u32[]{:S(2)}, u32[]{:S(2)}) async-start(f32[8,136,128]{2,1,0:T(8,128)} %convolve.1), calls=%async_computation.1 | async-start | bytes 1114112 | tf_op jit(solution)/shard_map/all_to_all | solution.py:510
  39.8 1.1 %copy-start.4 = (bf16[1296,256]{1,0:T(8,128)(2,1)S(1)}, bf16[1296,256]{1,0:T(8,128)(2,1)}, u32[]{:S(2)}) copy-start(bf16[1296,256]{1,0:T(8,128)(2,1)} %copy-done.3) | copy-start | bytes 1990660
  62.8 20.2 %collective-permute-start.10 = (bf16[528,128]{1,0:T(8,128)(2,1)S(1)}, bf16[528,128]{1,0:T(8,128)(2,1)S(1)}, u32[]{:S(2)}, u32[]{:S(2)}) collective-permute-start(bf16[528,128]{1,0:T(8,128)(2,1)S(1)} %get-tuple-element.39), channel_id=1, source_target_pairs={{0,64},{8,72},{16,80},{24,88},{32,96},{40,104},{48,112},{56,120},{... | collective-permute-start | bytes 405512 | tf_op jit(solution)/shard_map/ppermute | solution.py:515
  62.9 21.9 %collective-permute-start.11 = (bf16[528,128]{1,0:T(8,128)(2,1)S(1)}, bf16[528,128]{1,0:T(8,128)(2,1)S(1)}, u32[]{:S(2)}, u32[]{:S(2)}) collective-permute-start(bf16[528,128]{1,0:T(8,128)(2,1)S(1)} %get-tuple-element.40), channel_id=1, source_target_pairs={{0,96},{8,104},{16,112},{24,120},{32,0},{40,8},{48,16},{56,24},{64... | collective-permute-start | bytes 405512 | tf_op jit(solution)/shard_map/ppermute | solution.py:515
  77.7 7.1 %collective-permute-start.6 = (bf16[528,128]{1,0:T(8,128)(2,1)S(1)}, bf16[528,128]{1,0:T(8,128)(2,1)S(1)}, u32[]{:S(2)}, u32[]{:S(2)}) collective-permute-start(bf16[528,128]{1,0:T(8,128)(2,1)S(1)} %get-tuple-element.35), channel_id=1, source_target_pairs={{0,8},{8,16},{16,24},{24,0},{32,40},{40,48},{48,56},{56,32},{64,72... | collective-permute-start | bytes 405512 | tf_op jit(solution)/shard_map/ppermute | solution.py:515
  77.7 9.8 %collective-permute-start.7 = (bf16[528,128]{1,0:T(8,128)(2,1)S(1)}, bf16[528,128]{1,0:T(8,128)(2,1)S(1)}, u32[]{:S(2)}, u32[]{:S(2)}) collective-permute-start(bf16[528,128]{1,0:T(8,128)(2,1)S(1)} %get-tuple-element.36), channel_id=1, source_target_pairs={{0,16},{8,24},{16,0},{24,8},{32,48},{40,56},{48,32},{56,40},{64,80... | collective-permute-start | bytes 405512 | tf_op jit(solution)/shard_map/ppermute | solution.py:515
  80.9 6.6 %collective-permute-start.8 = (bf16[528,128]{1,0:T(8,128)(2,1)S(1)}, bf16[528,128]{1,0:T(8,128)(2,1)S(1)}, u32[]{:S(2)}, u32[]{:S(2)}) collective-permute-start(bf16[528,128]{1,0:T(8,128)(2,1)S(1)} %get-tuple-element.37), channel_id=1, source_target_pairs={{0,24},{8,0},{16,8},{24,16},{32,56},{40,32},{48,40},{56,48},{64,88... | collective-permute-start | bytes 405512 | tf_op jit(solution)/shard_map/ppermute | solution.py:515
  83.0 5.1 %collective-permute-start.9 = (bf16[528,128]{1,0:T(8,128)(2,1)S(1)}, bf16[528,128]{1,0:T(8,128)(2,1)S(1)}, u32[]{:S(2)}, u32[]{:S(2)}) collective-permute-start(bf16[528,128]{1,0:T(8,128)(2,1)S(1)} %get-tuple-element.38), channel_id=1, source_target_pairs={{0,32},{8,40},{16,48},{24,56},{32,64},{40,72},{48,80},{56,88},{64,... | collective-permute-start | bytes 405512 | tf_op jit(solution)/shard_map/ppermute | solution.py:515
  89.4 13.5 %all-to-all-start = ((bf16[8,128,128]{2,1,0:T(8,128)(2,1)}), bf16[8,128,128]{2,1,0:T(8,128)(2,1)S(1)}, u32[]{:S(2)}, u32[]{:S(2)}) async-start(bf16[8,128,128]{2,1,0:T(8,128)(2,1)} %combine.1), calls=%async_computation | async-start | bytes 524288 | tf_op jit(solution)/shard_map/all_to_all | solution.py:520
  100.1 1.9 %copy-start.1 = (bf16[1024,2048]{1,0:T(8,128)(2,1)}, bf16[1024,2048]{1,0:T(8,128)(2,1)S(1)}, u32[]{:S(2)}) copy-start(bf16[1024,2048]{1,0:T(8,128)(2,1)S(1)} %get-tuple-element.44.w) | copy-start | bytes 12582916
  103.0 2.2 %copy-start.2 = (bf16[1024,2048]{1,0:T(8,128)(2,1)S(1)}, bf16[1024,2048]{1,0:T(8,128)(2,1)}, u32[]{:S(2)}) copy-start(bf16[1024,2048]{1,0:T(8,128)(2,1)} %copy-done.1) | copy-start | bytes 12582916

commit v5 on v4

v5 whole, which is shorter than its diff:
```python
import functools

import jax
import jax.numpy as jnp
import numpy as np
from jax import lax
from jax.experimental import pallas as pl
from jax.experimental.pallas import tpu as pltpu
from jax.sharding import PartitionSpec as P


BF16, F32, I32 = jnp.bfloat16, jnp.float32, jnp.int32
SIDE = 4
HEAD = 128
TOK = 1024
HALF = 512
TAPS = 31
GATE_ROW = TOK
PACK_ROWS = TOK + 16
BACK_ROWS = HALF + 16
TILES = 15
LOG2E = 1.4426950408889634
SCALE = HEAD**-0.5 * LOG2E
LOW = -1e30
TINY = 1e-37
EPS = 1e-05

VM = pl.BlockSpec(memory_space=pltpu.VMEM)
SM = pl.BlockSpec(memory_space=pltpu.SMEM)
ANY = pl.BlockSpec(memory_space=pl.ANY)
HBM = pl.BlockSpec(memory_space=pltpu.HBM)


def dot(a, b):
    return jnp.dot(a, b, preferred_element_type=F32)


def params(mib):
    return pltpu.CompilerParams(vmem_limit_bytes=mib << 20)


def cost(flops, moved):
    return pl.CostEstimate(flops=flops, bytes_accessed=moved, transcendentals=0)


def moves(dx, dz):
    return [
        (z * SIDE + x, (z + dz) % SIDE * SIDE + (x + dx) % SIDE)
        for z in range(SIDE)
        for x in range(SIDE)
    ]


def eye():
    return lax.broadcasted_iota(I32, (128, 128), 0) == lax.broadcasted_iota(I32, (128, 128), 1)


def to_row(column):
    return jnp.sum(jnp.where(eye(), column, 0.0), axis=0, keepdims=True)


def to_column(row):
    return jnp.sum(jnp.where(eye(), row, 0.0), axis=1, keepdims=True)


def split3(value):
    top = value.astype(BF16)
    rest = value - top.astype(F32)
    mid = rest.astype(BF16)
    return top, mid, (rest - mid.astype(F32)).astype(BF16)


UP_HALVES = np.array([[0, 0, 0, 1], [0, 0, 1, 2], [0, 1, 2, 2], [1, 2, 2, 2]])


def work_table():
    table = np.zeros((SIDE * SIDE, 3, TILES + 1), np.int32)
    for z in range(SIDE):
        for x in range(SIDE):
            tiles = []
            for d in range(SIDE):
                other = (x + d) % SIDE
                late = d == 2
                for h in range(2):
                    if z < 2:
                        tiles.append((late, 2 + h, d))
                        if other < x:
                            tiles.append((late, h, d))
                        if h < 2 - UP_HALVES[x, other]:
                            tiles.append((late, 4 + h, d))
                    else:
                        tiles.append((late, 2 * d + h, 2))
                        if other > x:
                            tiles.append((late, 2 * d + h, 0))
                        if h >= 2 - UP_HALVES[other, x]:
                            tiles.append((late, 2 * d + h, 1))
            near = sum(not t[0] for t in tiles)
            assert len(tiles) == TILES and near % 2 == 1
            for n, (_, q, k) in enumerate(sorted(tiles)):
                table[z * SIDE + x, :2, n] = q, k
            table[z * SIDE + x, 2, 0] = near
    return table


def gate_rows(both):
    return (both[:, :128] * jax.nn.sigmoid(both[:, 128:])).astype(BF16)


def project_kernel(
    own, x_hbm, wq, wk, wv, wu, wg, gate, pkv, pxx, pq, gated, tail, x, w, sems
):
    low_level = own[0] < 8
    arrivals = [
        pltpu.make_async_copy(
            x_hbm.at[pl.ds(256 * i, 256)], x.at[pl.ds(256 * i, 256)], sems.at[i]
        )
        for i in range(4)
    ]
    loads = [
        pltpu.make_async_copy(source, w.at[:, pl.ds(128 * n, 128)], sems.at[4 + n])
        for n, source in enumerate((wk, wv, wq, wu, wg))
    ]
    for c in (*loads[:3], *arrivals, *loads[3:]):
        c.start()
    zero = jnp.zeros((8, 128), BF16)
    top, mid, low = split3(gate[...] * (-LOG2E))
    gates = jnp.concatenate(
        [jnp.concatenate([top, mid], axis=1), jnp.concatenate([low, zero], axis=1)], axis=0
    )
    pkv[GATE_ROW : GATE_ROW + 16, :] = gates
    pxx[GATE_ROW : GATE_ROW + 16, :] = gates
    for c in loads[:3]:
        c.wait()
    for i in range(4):
        arrivals[i].wait()
        out = dot(x[256 * i : 256 * i + 256, :], w[:, :384])
        both = out[:, :256].astype(BF16)
        query = (out[:, 256:] * SCALE).astype(BF16)
        rows = slice(256 * i, 256 * i + 256)
        half = slice(256 * (i % 2), 256 * (i % 2) + 256)
        lanes = slice(128 * (i // 2), 128 * (i // 2) + 128)
        pkv[rows, :] = both
        pq[half, lanes] = query
        if i >= 2:
            pxx[rows, :] = both
        else:

            @pl.when(low_level)
            def _():
                pxx[rows, :] = both

        @pl.when(jnp.logical_not(low_level))
        def _():
            pxx[half, lanes] = query

    for c in loads[3:]:
        c.wait()
    for i in range(4):
        rows = gate_rows(dot(x[256 * i : 256 * i + 256, :], w[:, 384:]))
        gated[256 * i : 256 * i + 256, :] = rows
    tail[...] = rows[224:, :]


def project(own, x, wq, wk, wv, wu, wg, gate):
    pack = jax.ShapeDtypeStruct((PACK_ROWS, 256), BF16)
    return pl.pallas_call(
        project_kernel,
        out_shape=(
            pack,
            pack,
            jax.ShapeDtypeStruct((HALF, 256), BF16),
            jax.ShapeDtypeStruct((TOK, 128), BF16),
            jax.ShapeDtypeStruct((32, 128), BF16),
        ),
        in_specs=[SM] + [HBM] * 6 + [VM],
        out_specs=(VM,) * 5,
        scratch_shapes=[
            pltpu.VMEM((TOK, 2048), BF16),
            pltpu.VMEM((2048, 640), BF16),
            pltpu.SemaphoreType.DMA((9,)),
        ],
        compiler_params=params(12),
        cost_estimate=cost(2 * TOK * 2048 * 640, 8 << 20),
        name="project",
    )(own, x, wq, wk, wv, wu, wg, gate)


def conv_kernel(gated, halo, taps, gain, out, padded):
    padded[0:32, :] = halo[...].astype(F32)
    padded[32 : 32 + TOK, :] = gated[...].astype(F32)
    padded[32 + TOK :, :] = jnp.zeros((8, 128), F32)
    for block in range(8):
        start = 128 * block
        total = None
        for r in range(8):
            part = None
            for q in range(5):
                j = 8 * q + r - 2
                if 0 <= j < TAPS:
                    term = taps[j : j + 1, :] * padded[start + 8 * q : start + 8 * q + 136, :]
                    part = term if part is None else part + term
            part = part[r : r + 128, :]
            total = part if total is None else total + part
        out[block, 0:128, :] = total
        out[block, 128:136, :] = jnp.broadcast_to(gain[...], (8, 128))


def convolve(gated, halo, taps, gain):
    return pl.pallas_call(
        conv_kernel,
        out_shape=jax.ShapeDtypeStruct((8, 136, 128), F32),
        in_specs=[VM] * 4,
        out_specs=VM,
        scratch_shapes=[pltpu.VMEM((TOK + 40, 128), F32)],
        compiler_params=params(8),
        cost_estimate=cost(2 * TOK * 128 * 31 * 64, 1 << 20),
        name="convolve",
    )(gated, halo, taps, gain)


def diagonal(pkv, pq, m, l, acc):
    top = pkv[GATE_ROW : GATE_ROW + 8, :].astype(F32)
    low = pkv[GATE_ROW + 8 : GATE_ROW + 16, :].astype(F32)
    gates = top[:, :128] + top[:, 128:] + low[:, :128]
    for half in range(2):
        keys = HALF * (half + 1)
        scores = lax.dot_general(
            pq[:, 128 * half : 128 * half + 128],
            pkv[:keys, :128],
            (((1,), (1,)), ((), ())),
            preferred_element_type=F32,
        )
        row = lax.broadcasted_iota(I32, (HALF, 128), 0) + HALF * half
        lane = lax.broadcasted_iota(I32, (HALF, 128), 1)
        parts = []
        for c in range(keys // 128):
            t = scores[:, 128 * c : 128 * c + 128] + gates[c : c + 1, :]
            parts.append(jnp.where(lane + 128 * c <= row, t, LOW))
        most = functools.reduce(jnp.maximum, parts)
        most = jnp.broadcast_to(jnp.max(most, axis=1, keepdims=True), (HALF, 128))
        weights = [jnp.exp2(t - most) for t in parts]
        m[half] = most
        rounded = jnp.concatenate([w.astype(BF16) for w in weights], axis=1)
        ones = jnp.ones((keys, 128), BF16)
        out = dot(rounded, jnp.concatenate([pkv[:keys, 128:], ones], axis=1))
        acc[half] = out[:, :128]
        l[half] = out[:, 128:]


QUERIES = 8


def key_copies(source, packs, slot, sems):
    return [
        pltpu.make_async_copy(
            source.at[pl.ds(at, rows)], packs.at[slot, pl.ds(at, rows)], sems.at[n, slot]
        )
        for n, (at, rows) in enumerate(((0, HALF), (HALF, PACK_ROWS - HALF)))
    ]


def query_copy(source, qpacks, slot, sems):
    return pltpu.make_async_copy(source.at[pl.ds(0, HALF)], qpacks.at[slot], sems.at[2, slot])


def unpack_keys(packs, slots, gates):
    for n in slots:
        top = packs[n, GATE_ROW : GATE_ROW + 8, :].astype(F32)
        low = packs[n, GATE_ROW + 8 : GATE_ROW + 16, :].astype(F32)
        gates[n] = top[:, :128] + top[:, 128:] + low[:, :128]


def unpack_queries(qpacks, slots, query):
    for n in slots:
        query[2 * n] = qpacks[n, :, :128]
        query[2 * n + 1] = qpacks[n, :, 128:]


def each(copies, action):
    for c in copies:
        getattr(c, action)()


def finish(m, l, acc, first, out):
    for n in range(2):
        total = jnp.maximum(l[first + n], TINY)
        lse = m[first + n] + jnp.log2(total)
        base = BACK_ROWS * n
        out[base : base + HALF, :] = (acc[first + n] / total).astype(BF16)
        rows = [to_row(lse[128 * b : 128 * b + 128, :]) for b in range(4)]
        parts = split3(jnp.concatenate(rows + rows, axis=0))
        out[base + HALF : base + BACK_ROWS, :] = jnp.concatenate(
            [parts[0][:4], parts[1][:4], parts[2]], axis=0
        )


def run_tiles(table, own, start, count, even, packs, query, gates, per_tile, m, l, acc):
    sa, sb, ma, mb, aa, ab = per_tile
    row = own[0]
    first, second = (sa, ma, aa), (sb, mb, ab)

    def scores_of(n, s, most, shrink):
        q, k = table[row, 0, n], table[row, 1, n]
        raw = lax.dot_general(
            query[q], packs[k, :TOK, :128], (((1,), (1,)), ((), ())), preferred_element_type=F32
        )
        best = None
        for c in range(8):
            t = raw[:, 128 * c : 128 * c + 128] + gates[k, c : c + 1, :]
            s[:, 128 * c : 128 * c + 128] = t
            best = t if best is None else jnp.maximum(best, t)
        old = m[q]
        new = jnp.maximum(old, jnp.max(best, axis=1, keepdims=True))
        shrink[...] = jnp.exp2(old - new)
        m[q] = new
        most[...] = new

    def weigh(n, s, most, shrink):
        q, k = table[row, 0, n], table[row, 1, n]
        top = most[...]
        by = shrink[...]
        w = [jnp.exp2(s[:, 128 * c : 128 * c + 128] - top) for c in range(8)]
        rounded = jnp.concatenate([v.astype(BF16) for v in w], axis=1)
        ones = jnp.ones((TOK, 128), BF16)
        out = dot(rounded, jnp.concatenate([packs[k, :TOK, 128:], ones], axis=1))
        acc[q] = acc[q] * by + out[:, :128]
        l[q] = l[q] * by + out[:, 128:]


    scores_of(start, *first)

    def two_tiles(i, carry):
        n = start + 2 * i
        scores_of(n + 1, *second)
        weigh(n, *first)
        scores_of(n + 2, *first)
        weigh(n + 1, *second)
        return carry

    lax.fori_loop(0, (count - 1) // 2, two_tiles, 0)
    if even:
        scores_of(start + count - 1, *second)
        weigh(start + count - 2, *first)
        weigh(start + count - 1, *second)
    else:
        weigh(start + count - 1, *first)


def near_kernel(
    table, own, pkv, pq, x1, x3, u, w, kx, ky,
    m, l, acc, packs, query, gates, b1, b3, qpacks, sems, *per_tile,
):
    low_level = own[0] < 8
    high_level = jnp.logical_not(low_level)
    low_copies = [
        *key_copies(x1, packs, 1, sems),
        *key_copies(x3, packs, 3, sems),
        query_copy(u, qpacks, 1, sems),
        query_copy(w, qpacks, 2, sems),
    ]
    high_copies = [
        *key_copies(kx, packs, 1, sems),
        *key_copies(ky, packs, 2, sems),
        query_copy(x1, qpacks, 1, sems),
        query_copy(x3, qpacks, 3, sems),
    ]
    pl.when(low_level)(lambda: each(low_copies, "start"))
    pl.when(high_level)(lambda: each(high_copies, "start"))
    for n in range(2, QUERIES):
        m[n] = jnp.full((HALF, 128), LOW, F32)
        l[n] = jnp.zeros((HALF, 128), F32)
        acc[n] = jnp.zeros((HALF, 128), F32)
    packs[0] = pkv[...]
    unpack_keys(packs, (0,), gates)
    query[0] = pq[:, :128]
    query[1] = pq[:, 128:]
    diagonal(pkv, pq, m, l, acc)

    @pl.when(low_level)
    def _():
        each(low_copies, "wait")
        unpack_keys(packs, (1, 3), gates)
        unpack_queries(qpacks, (1, 2), query)

    @pl.when(high_level)
    def _():
        each(high_copies, "wait")
        unpack_keys(packs, (1, 2), gates)
        unpack_queries(qpacks, (1, 3), query)

    count = table[own[0], 2, 0]
    run_tiles(table, own, 0, count, False, packs, query, gates, per_tile, m, l, acc)
    finish(m, l, acc, 2, b1)
    finish(m, l, acc, 6, b3)


def far_kernel(
    table, own, x2, m_in, l_in, acc_in, packs_in, query_in, gates_in,
    o_own, lse_own, b1, b2,
    m, l, acc, packs, query, gates, qpacks, sems, *per_tile,
):
    low_level = own[0] < 8
    high_level = jnp.logical_not(low_level)
    low_copies = key_copies(x2, packs, 2, sems)
    high_copies = [query_copy(x2, qpacks, 2, sems)]
    pl.when(low_level)(lambda: each(low_copies, "start"))
    pl.when(high_level)(lambda: each(high_copies, "start"))
    for n in range(6):
        m[n] = m_in[n]
        l[n] = l_in[n]
        acc[n] = acc_in[n]
        query[n] = query_in[n]
    for n in (0, 1, 3):
        packs[n, :TOK, :] = packs_in[n, :TOK, :]
        gates[n] = gates_in[n]

    @pl.when(low_level)
    def _():
        each(low_copies, "wait")
        unpack_keys(packs, (2,), gates)

    @pl.when(high_level)
    def _():
        packs[2, :TOK, :] = packs_in[2, :TOK, :]
        gates[2] = gates_in[2]
        each(high_copies, "wait")
        unpack_queries(qpacks, (2,), query)

    near = table[own[0], 2, 0]
    run_tiles(table, own, near, TILES - near, True, packs, query, gates, per_tile, m, l, acc)
    for n in range(2):
        total = jnp.maximum(l[n], TINY)
        o_own[n] = acc[n] / total
        lse_own[n] = m[n] + jnp.log2(total)
    finish(m, l, acc, 2, b1)
    finish(m, l, acc, 4, b2)


SEMS = [pltpu.SemaphoreType.DMA((3, 4))]
QPACKS = [((4, HALF, 256), BF16)]
SLOTS = [((4, PACK_ROWS, 256), BF16), ((QUERIES, HALF, 128), BF16), ((4, 8, 128), F32)]
STATE = [((QUERIES, HALF, 128), F32)] * 3
TILE = [((HALF, TOK), F32)] * 2 + [((HALF, 128), F32)] * 4
BACK = [((2 * BACK_ROWS, 128), BF16)]


def arrays(shapes):
    return tuple(jax.ShapeDtypeStruct(*v) for v in shapes)


def scratch(shapes):
    return [pltpu.VMEM(*v) for v in shapes]


def attend_near(table, own, *packs):
    return pl.pallas_call(
        near_kernel,
        out_shape=arrays(STATE + SLOTS + BACK * 2),
        in_specs=[SM, SM, VM, VM] + [ANY] * 6,
        out_specs=(VM,) * 8,
        scratch_shapes=scratch(QPACKS) + SEMS + scratch(TILE),
        compiler_params=params(24),
        cost_estimate=cost(12 * 4 * HALF * TOK * 256, 8 << 20),
        name="attend_near",
    )(table, own, *packs)


def attend_far(table, own, x2, state):
    return pl.pallas_call(
        far_kernel,
        out_shape=arrays([((2, HALF, 128), F32)] * 2 + BACK * 2),
        in_specs=[SM, SM, ANY] + [VM] * 6,
        out_specs=(VM,) * 4,
        scratch_shapes=scratch(STATE + SLOTS + QPACKS) + SEMS + scratch(TILE),
        compiler_params=params(30),
        cost_estimate=cost(5 * 4 * HALF * TOK * 256, 8 << 20),
        name="attend_far",
    )(table, own, x2, *state)


def combine_kernel(own, o_own, lse_own, x1, x2, x3, u, w, out):
    z = own[0] // SIDE
    high = z >= 2
    backs = ((x1, high), (x2, high), (x3, high), (u, z % 2 == 1), (w, high))
    for half in range(2):
        base = BACK_ROWS * half
        lses = []
        for back, there in backs:
            tail = back[base + HALF : base + BACK_ROWS, :].astype(F32)
            lses.append(jnp.where(there, tail[0:4] + tail[4:8] + tail[8:12], LOW))
        for b in range(4):
            rows = slice(128 * b, 128 * b + 128)
            columns = [lse_own[half, rows, :]]
            columns += [jnp.broadcast_to(to_column(v[b : b + 1, :]), (128, 128)) for v in lses]
            most = functools.reduce(jnp.maximum, columns)
            shares = [jnp.exp2(c - most) for c in columns]
            mixed = shares[0] * o_own[half, rows, :]
            for share, (back, _) in zip(shares[1:], backs):
                mixed = mixed + share * back[base + 128 * b : base + 128 * b + 128, :].astype(F32)
            out[4 * half + b] = (mixed / functools.reduce(jnp.add, shares)).astype(BF16)


def combine(own, o_own, lse_own, backs):
    return pl.pallas_call(
        combine_kernel,
        out_shape=jax.ShapeDtypeStruct((8, 128, 128), BF16),
        in_specs=[SM] + [VM] * 7,
        out_specs=VM,
        compiler_params=params(16),
        cost_estimate=cost(1 << 29, 2 << 20),
        name="combine",
    )(own, o_own, lse_own, *backs)


def conv_out_kernel(parts, w_hbm, out, later, rows, w, sems):
    copies = []
    for j in range(4):
        cols = pl.ds(512 * j, 512)
        copies.append(
            pltpu.make_async_copy(w_hbm.at[pl.ds(0, 1024), cols], w.at[:, cols], sems.at[j])
        )
    copies.append(pltpu.make_async_copy(w_hbm.at[pl.ds(1024, 1024)], later, sems.at[4]))
    for c in copies:
        c.start()
    total = functools.reduce(jnp.add, [parts[c, :128, :] for c in range(8)])
    mean = jnp.sum(total, axis=1, keepdims=True) * (1.0 / 1024)
    far = [parts[c, :128, :] - mean for c in range(8)]
    spread = functools.reduce(jnp.add, [v * v for v in far])
    spread = jnp.sum(spread, axis=1, keepdims=True) * (1.0 / 1024)
    inverse = lax.rsqrt(spread + EPS)
    for c in range(8):
        v = far[c] * inverse * parts[c, 128:129, :]
        rows[:, 128 * c : 128 * c + 128] = (v * jax.nn.sigmoid(v)).astype(BF16)
    for j in range(4):
        copies[j].wait()
        out[:, 512 * j : 512 * j + 512] = dot(rows[...], w[:, 512 * j : 512 * j + 512])
    copies[4].wait()


def conv_out(parts, w):
    return pl.pallas_call(
        conv_out_kernel,
        out_shape=(
            jax.ShapeDtypeStruct((128, 2048), F32),
            jax.ShapeDtypeStruct((1024, 2048), BF16),
        ),
        in_specs=[VM, HBM],
        out_specs=(VM, VM),
        scratch_shapes=[
            pltpu.VMEM((128, 1024), BF16),
            pltpu.VMEM((1024, 2048), BF16),
            pltpu.SemaphoreType.DMA((5,)),
        ],
        compiler_params=params(14),
        cost_estimate=cost(2 * 128 * 1024 * 2048 * 4, 6 << 20),
        name="conv_out",
    )(parts, w)


def attn_out_kernel(parts, conv, w, out, rows):
    for c in range(8):
        rows[:, 128 * c : 128 * c + 128] = parts[c]
    for j in range(4):
        cols = slice(512 * j, 512 * j + 512)
        out[:, cols] = (dot(rows[...], w[:, cols]) + conv[:, cols]).astype(BF16)


def attn_out(parts, conv, w):
    return pl.pallas_call(
        attn_out_kernel,
        out_shape=jax.ShapeDtypeStruct((128, 2048), BF16),
        in_specs=[VM, VM, VM],
        out_specs=VM,
        scratch_shapes=[pltpu.VMEM((128, 1024), BF16)],
        compiler_params=params(10),
        cost_estimate=cost(2 * 128 * 1024 * 2048 * 4, 6 << 20),
        name="attn_out",
    )(parts, conv, w)


def levels(*pairs):
    return [(a * SIDE + x, b * SIDE + x) for a, b in pairs for x in range(SIDE)]


def along_x(d):
    return [(z * SIDE + x, z * SIDE + (x + d) % SIDE) for z in (2, 3) for x in range(SIDE)]


def layer(x, wq, wk, wv, wu, wg, taps, gain, gate, w_out):
    x, wq, wk, wv, wu, wg, w_out = (
        pltpu.with_memory_space_constraint(v, pltpu.HBM) for v in (x, wq, wk, wv, wu, wg, w_out)
    )
    own = lax.axis_index("sp").astype(I32).reshape(1)
    table = jnp.asarray(work_table())
    pkv, pxx, pq, gated, tail = project(own, x, wq, wk, wv, wu, wg, gate.reshape(8, 128))
    halo = lax.ppermute(tail, "sp", [(i, i + 1) for i in range(15)])
    x1 = lax.ppermute(pxx, "sp", moves(-1, 0))
    x3 = lax.ppermute(pxx, "sp", moves(-3, 0))
    ky = lax.ppermute(pkv, "sp", levels((2, 3), (0, 2)))
    u = lax.ppermute(pq, "sp", levels((1, 0), (3, 1)))
    kz = lax.ppermute(pkv, "sp", levels((1, 2), (0, 3)))
    w = lax.ppermute(pq, "sp", levels((2, 1), (3, 0)))
    x2 = lax.ppermute(pxx, "sp", moves(-2, 0))
    conv = convolve(gated, halo, taps, gain.reshape(1, 128))
    conv_parts = lax.all_to_all(conv, "tp", 0, 0, tiled=True)
    *state, b1, b3 = attend_near(table, own, pkv, pq, x1, x3, u, w, kz, ky)
    back1 = lax.ppermute(b1, "sp", along_x(1))
    back3 = lax.ppermute(b3, "sp", along_x(3))
    o_own, lse_own, bu, b2 = attend_far(table, own, x2, state)
    back2 = lax.ppermute(b2, "sp", along_x(2))
    back_u = lax.ppermute(bu, "sp", levels((0, 1), (1, 3)))
    back_w = lax.ppermute(b2, "sp", levels((1, 2), (0, 3)))
    conv_mixed, w_attn = conv_out(conv_parts, w_out)
    mixed = combine(own, o_own, lse_own, (back1, back2, back3, back_u, back_w))
    attn_parts = lax.all_to_all(mixed, "tp", 0, 0, tiled=True)
    return attn_out(attn_parts, conv_mixed, w_attn)


def solution(mesh):
    in_specs = (
        P("sp", None),
        P(None, "tp"),
        P(None, "tp"),
        P(None, "tp"),
        P(None, "tp"),
        P(None, "tp"),
        P(None, "tp"),
        P("tp"),
        P("sp", "tp"),
        P(),
    )
    out_specs = P(("sp", "tp"), None)
    return jax.shard_map(layer, mesh=mesh, in_specs=in_specs, out_specs=out_specs, check_vma=False)
```

time: 107 us -> 97.8 us (0.914)
  the two profiles are of different devices: /device:TPU:1 before, /device:TPU:102 now
where the time goes in v5:
time: 97.8 us; the launch traced here: 97.2 us
  starting transfers between devices  42.2 us (43%)
  Pallas kernels  33 us (34%)
  waiting for transfers between devices  15.4 us (16%)
  local copies, waits for them, and re-layouts  6.47 us (7%)
    pallas_call x1, Pallas kernels, attend_near(): pl.pallas_call(near_kernel, out_shape=arrays(STATE + SLOTS + BACK * 2), i...  12.6 us
    ppermute x1, starting transfers between devices, layer(): u = lax.ppermute(pq, 'sp', levels((1, 0), (3, 1)))  7.35 us
    unnamed x16, local copies, waits for them, and re-layouts  6.47 us
    ppermute x1, starting transfers between devices, layer(): w = lax.ppermute(pq, 'sp', levels((2, 1), (3, 0)))  6.29 us
    pallas_call x1, Pallas kernels, project(): pl.pallas_call(project_kernel, out_shape=(pack, pack, jax.ShapeDtypeStruc...  5.93 us
    pallas_call x1, Pallas kernels, attend_far(): pl.pallas_call(far_kernel, out_shape=arrays([((2, HALF, 128), F32)] * 2 +...  5.28 us
    all_to_all x1, starting transfers between devices, layer(): conv_parts = lax.all_to_all(conv, 'tp', 0, 0, tiled=True)  4.47 us
    all_to_all x1, starting transfers between devices, layer(): attn_parts = lax.all_to_all(mixed, 'tp', 0, 0, tiled=True)  4.41 us
  transfers between devices with their start and end apart: 15, of which 6 were waited for; matrix products, arithmetic and copies ran while one was open for 0% of the time, Pallas kernels for 26%

profile of v5, /device:TPU:102, one launch (start us, length us, event | category | flops | bytes accessed | tf_op | source)
XLA Modules:
  0.0 97.2 jit_solution(17367387226103572393)
XLA Ops:
  0.7 5.9 %project.1 = (bf16[1040,256]{1,0:T(8,128)(2,1)S(1)}, bf16[1040,256]{1,0:T(8,128)(2,1)S(1)}, bf16[512,256]{1,0:T(8,128)(2,1)S(1)}, bf16[1024,128]{1,0:T(8,128)(2,1)S(1)}, bf16[32,128]{1,0:T(8,128)(2,1)S(1)}) custom-call(s32[1]{0:T(128)} %bitcast.own, bf16[1024,2048]{1,0:T(8,128)(2,1)} %x_hbm.1, bf16[2048,128]{1,0:T(8,128)(2,1)} %wq.1, bf16[2048,128]{1,0:T(8,128)(2,1)} %wk.1, ...), custom_call_target="tpu_custom_call" | custom-call | flops 2684354560 | bytes 8388608 | tf_op jit(solution)/shard_map/project/pallas_call | solution.py:166
  6.6 1.3 %collective-permute-start.12 = (bf16[32,128]{1,0:T(8,128)(2,1)S(1)}, bf16[32,128]{1,0:T(8,128)(2,1)S(1)}, u32[]{:S(2)}, u32[]{:S(2)}) collective-permute-start(bf16[32,128]{1,0:T(8,128)(2,1)S(1)} %get-tuple-element.40), channel_id=1, source_target_pairs={{0,8},{8,16},{16,24},{24,32},{32,40},{40,48},{48,56},{56,64},{64,7... | collective-permute-start | bytes 24584 | tf_op jit(solution)/shard_map/ppermute | solution.py:596
  7.9 2.7 %collective-permute-start.1 = (bf16[1040,256]{1,0:T(8,128)(2,1)S(1)}, bf16[1040,256]{1,0:T(8,128)(2,1)S(1)}, u32[]{:S(2)}, u32[]{:S(2)}) collective-permute-start(bf16[1040,256]{1,0:T(8,128)(2,1)S(1)} %get-tuple-element.24), channel_id=1, source_target_pairs={{0,24},{8,0},{16,8},{24,16},{32,56},{40,32},{48,40},{56,48},{64,88... | collective-permute-start | bytes 1597448 | tf_op jit(solution)/shard_map/ppermute | solution.py:597
  13.8 7.3 %collective-permute-start.3 = (bf16[512,256]{1,0:T(8,128)(2,1)S(1)}, bf16[512,256]{1,0:T(8,128)(2,1)S(1)}, u32[]{:S(2)}, u32[]{:S(2)}) collective-permute-start(bf16[512,256]{1,0:T(8,128)(2,1)S(1)} %get-tuple-element.26.pq), channel_id=1, source_target_pairs={{32,0},{40,8},{48,16},{56,24},{96,32},{104,40},{112,48},{120,56},{... | collective-permute-start | bytes 786440 | tf_op jit(solution)/shard_map/ppermute | solution.py:600
  21.2 4.4 %collective-permute-done.3.u = bf16[512,256]{1,0:T(8,128)(2,1)S(1)} collective-permute-done((bf16[512,256]{1,0:T(8,128)(2,1)S(1)}, bf16[512,256]{1,0:T(8,128)(2,1)S(1)}, u32[]{:S(2)}, u32[]{:S(2)}) %collective-permute-start.3) | collective-permute-done | bytes 262176 | tf_op jit(solution)/shard_map/ppermute | solution.py:600
  26.3 6.3 %collective-permute-start.4 = (bf16[512,256]{1,0:T(8,128)(2,1)S(1)}, bf16[512,256]{1,0:T(8,128)(2,1)}, u32[]{:S(2)}, u32[]{:S(2)}) collective-permute-start(bf16[512,256]{1,0:T(8,128)(2,1)S(1)} %get-tuple-element.26.pq), channel_id=1, source_target_pairs={{64,32},{72,40},{80,48},{88,56},{96,0},{104,8},{112,16},{120,24},{... | collective-permute-start | bytes 786440 | tf_op jit(solution)/shard_map/ppermute | solution.py:602
  32.6 2.3 %convolve.1 = f32[8,136,128]{2,1,0:T(8,128)} custom-call(bf16[1024,128]{1,0:T(8,128)(2,1)S(1)} %get-tuple-element.39.gated, bf16[32,128]{1,0:T(8,128)(2,1)S(1)} %collective-permute-done.12.halo, f32[31,128]{1,0:T(8,128)S(1)} %copy-done.5, f32[1,128]{1,0:T(1,128)S(1)} %bitcast.4), custom_call_target="tpu_custom_call" | custom-call | flops 520093696 | bytes 1048576 | tf_op jit(solution)/shard_map/convolve/pallas_call | solution.py:209
  34.9 4.5 %all-to-all-start.1 = ((f32[8,136,128]{2,1,0:T(8,128)}), f32[8,136,128]{2,1,0:T(8,128)S(1)}, u32[]{:S(2)}, u32[]{:S(2)}) async-start(f32[8,136,128]{2,1,0:T(8,128)} %convolve.1), calls=%async_computation.1 | async-start | bytes 1114112 | tf_op jit(solution)/shard_map/all_to_all | solution.py:605
  40.8 12.6 %attend_near.1 = (f32[8,512,128]{2,1,0:T(8,128)S(1)}, f32[8,512,128]{2,1,0:T(8,128)S(1)}, f32[8,512,128]{2,1,0:T(8,128)S(1)}, bf16[4,1040,256]{2,1,0:T(8,128)(2,...) custom-call(s32[16,3,16]{2,1,0:T(4,128)S(1)} %copy-done, ...), custom_call_target="tpu_custom_call" | custom-call | flops 6442450944 | bytes 8388608 | tf_op jit(solution)/shard_map/attend_near/pallas_call | solution.py:456
  53.4 2.0 %collective-permute-done.x2 = bf16[1040,256]{1,0:T(8,128)(2,1)S(1)} collective-permute-done((bf16[1040,256]{1,0:T(8,128)(2,1)S(1)}, bf16[1040,256]{1,0:T(8,128)(2,1)S(1)}, u32[]{:S(2)}, u32[]{:S(2)}) %collective-permute-start) | collective-permute-done | bytes 532512 | tf_op jit(solution)/shard_map/ppermute | solution.py:603
  55.4 5.3 %attend_far.1 = (f32[2,512,128]{2,1,0:T(8,128)S(1)}, f32[2,512,128]{2,1,0:T(8,128)S(1)}, bf16[1056,128]{1,0:T(8,128)(2,1)S(1)}, bf16[1056,128]{1,0:T(8,128)(2,1)S(1)}) custom-call(s32[16,3,16]{2,1,0:T(4,128)S(1)} %copy-done, s32[1]{0:T(128)} %bitcast.own, bf16[1040,256]{1,0:T(8,128)(2,1)S(1)} %collective-permute-done.x2, ...), custom_call_target="tpu_custom_call" | custom-call | flops 2684354560 | bytes 8388608 | tf_op jit(solution)/shard_map/attend_far/pallas_call | solution.py:469
  60.7 1.3 %collective-permute-start.11 = (bf16[1056,128]{1,0:T(8,128)(2,1)S(1)}, bf16[1056,128]{1,0:T(8,128)(2,1)S(1)}, u32[]{:S(2)}, u32[]{:S(2)}) collective-permute-start(bf16[1056,128]{1,0:T(8,128)(2,1)S(1)} %get-tuple-element.36), channel_id=1, source_target_pairs={{32,64},{40,72},{48,80},{56,88},{0,96},{8,104},{16,112},{24,120},{... | collective-permute-start | bytes 811016 | tf_op jit(solution)/shard_map/ppermute | solution.py:612
  62.0 3.6 %collective-permute-start.8 = (bf16[1056,128]{1,0:T(8,128)(2,1)S(1)}, bf16[1056,128]{1,0:T(8,128)(2,1)S(1)}, u32[]{:S(2)}, u32[]{:S(2)}) collective-permute-start(bf16[1056,128]{1,0:T(8,128)(2,1)S(1)} %get-tuple-element.36), channel_id=1, source_target_pairs={{64,80},{72,88},{80,64},{88,72},{96,112},{104,120},{112,96},{120,1... | collective-permute-start | bytes 811016 | tf_op jit(solution)/shard_map/ppermute | solution.py:610
  66.9 1.9 %collective-permute-start.7 = (bf16[1056,128]{1,0:T(8,128)(2,1)S(1)}, bf16[1056,128]{1,0:T(8,128)(2,1)S(1)}, u32[]{:S(2)}, u32[]{:S(2)}) collective-permute-start(bf16[1056,128]{1,0:T(8,128)(2,1)S(1)} %get-tuple-element.35), channel_id=1, source_target_pairs={{64,72},{72,80},{80,88},{88,64},{96,104},{104,112},{112,120},{120,... | collective-permute-start | bytes 811016 | tf_op jit(solution)/shard_map/ppermute | solution.py:607
  68.8 3.9 %collective-permute-start.9 = (bf16[1056,128]{1,0:T(8,128)(2,1)S(1)}, bf16[1056,128]{1,0:T(8,128)(2,1)S(1)}, u32[]{:S(2)}, u32[]{:S(2)}) collective-permute-start(bf16[1056,128]{1,0:T(8,128)(2,1)S(1)} %get-tuple-element.37), channel_id=1, source_target_pairs={{64,88},{72,64},{80,72},{88,80},{96,120},{104,96},{112,104},{120,1... | collective-permute-start | bytes 811016 | tf_op jit(solution)/shard_map/ppermute | solution.py:608
  72.8 4.0 %collective-permute-done.10.u = bf16[1056,128]{1,0:T(8,128)(2,1)S(1)} collective-permute-done((bf16[1056,128]{1,0:T(8,128)(2,1)S(1)}, bf16[1056,128]{1,0:T(8,128)(2,1)S(1)}, u32[]{:S(2)}, u32[]{:S(2)}) %collective-permute-start.10) | collective-permute-done | bytes 270368 | tf_op jit(solution)/shard_map/ppermute | solution.py:611
  77.5 2.3 %collective-permute-done.9.x3 = bf16[1056,128]{1,0:T(8,128)(2,1)S(1)} collective-permute-done((bf16[1056,128]{1,0:T(8,128)(2,1)S(1)}, bf16[1056,128]{1,0:T(8,128)(2,1)S(1)}, u32[]{:S(2)}, u32[]{:S(2)}) %collective-permute-start.9) | collective-permute-done | bytes 270368 | tf_op jit(solution)/shard_map/ppermute | solution.py:608
  79.8 1.8 %combine.1 = bf16[8,128,128]{2,1,0:T(8,128)(2,1)} custom-call(s32[1]{0:T(128)} %bitcast.own, f32[2,512,128]{2,1,0:T(8,128)S(1)} %get-tuple-element.33.o_own, f32[2,512,128]{2,1,0:T(8,128)S(1)} %get-tuple-element.34.lse_own, bf16[1056,128]{1,0:T(8,128)(2,1)S(1)} %collective-permute-done.7.x1, bf16[1056,128]{1,0:T(8,128)(2,1)S(1)} %collective-permute-done.8.x2, ...), custom_call_target="tpu_custom_call" | custom-call | flops 536870912 | bytes 2097152 | tf_op jit(solution)/shard_map/combine/pallas_call | solution.py:504
  81.6 4.4 %all-to-all-start = ((bf16[8,128,128]{2,1,0:T(8,128)(2,1)}), bf16[8,128,128]{2,1,0:T(8,128)(2,1)S(1)}, u32[]{:S(2)}, u32[]{:S(2)}) async-start(bf16[8,128,128]{2,1,0:T(8,128)(2,1)} %combine.1), calls=%async_computation | async-start | bytes 524288 | tf_op jit(solution)/shard_map/all_to_all | solution.py:615
  86.0 3.6 %conv_out.1 = (f32[128,2048]{1,0:T(8,128)S(1)}, bf16[1024,2048]{1,0:T(8,128)(2,1)S(1)}) custom-call(f32[8,136,128]{2,1,0:T(8,128)S(1)} %all-to-all-done.1.parts, bf16[2048,2048]{1,0:T(8,128)(2,1)} %w_hbm.1), custom_call_target="tpu_custom_call" | custom-call | flops 2147483648 | bytes 6291456 | tf_op jit(solution)/shard_map/conv_out/pallas_call | solution.py:541
  89.6 1.9 %copy-done.1 = bf16[1024,2048]{1,0:T(8,128)(2,1)} copy-done((bf16[1024,2048]{1,0:T(8,128)(2,1)}, bf16[1024,2048]{1,0:T(8,128)(2,1)S(1)}, u32[]{:S(2)}) %copy-start.1) | copy-done | bytes 4194328
  91.5 2.0 %all-to-all-done.parts = bf16[8,128,128]{2,1,0:T(8,128)(2,1)S(1)} async-done(((bf16[8,128,128]{2,1,0:T(8,128)(2,1)}), bf16[8,128,128]{2,1,0:T(8,128)(2,1)S(1)}, u32[]{:S(2)}, u32[]{:S(2)}) %all-to-all-start) | async-done | bytes 262176 | tf_op jit(solution)/shard_map/all_to_all | solution.py:615
  93.5 2.2 %copy-done.2 = bf16[1024,2048]{1,0:T(8,128)(2,1)S(1)} copy-done((bf16[1024,2048]{1,0:T(8,128)(2,1)S(1)}, bf16[1024,2048]{1,0:T(8,128)(2,1)}, u32[]{:S(2)}) %copy-start.2) | copy-done | bytes 4194328
  95.7 1.5 %attn_out.1 = bf16[128,2048]{1,0:T(8,128)(2,1)} custom-call(bf16[8,128,128]{2,1,0:T(8,128)(2,1)S(1)} %all-to-all-done.parts, f32[128,2048]{1,0:T(8,128)S(1)} %get-tuple-element.41.conv, bf16[1024,2048]{1,0:T(8,128)(2,1)S(1)} %copy-done.2), custom_call_target="tpu_custom_call" | custom-call | flops 2147483648 | bytes 6291456 | tf_op jit(solution)/shard_map/attn_out/pallas_call | solution.py:569
  (29 shorter events, 8.0 us)
Async XLA Ops:
  0.0 0.7 copy-start.6
  0.7 31.9 %copy-start.5 = (f32[31,128]{1,0:T(8,128)S(1)}, f32[31,128]{1,0:T(8,128)}, u32[]{:S(2)}) copy-start(f32[31,128]{1,0:T(8,128)} %taps.1) | copy-start | bytes 47620
  0.7 31.9 %copy-start.7 = (f32[128]{0:T(128)S(1)}, f32[128]{0:T(128)}, u32[]{:S(2)}) copy-start(f32[128]{0:T(128)} %param.18) | copy-start | bytes 1540
  6.6 33.2 %copy-start = (s32[16,3,16]{2,1,0:T(4,128)S(1)}, s32[16,3,16]{2,1,0:T(4,128)}, u32[]{:S(2)}) copy-start(s32[16,3,16]{2,1,0:T(4,128)} %constant.8.clone.table) | copy-start | bytes 9220
  6.6 7.2 %collective-permute-start.12 = (bf16[32,128]{1,0:T(8,128)(2,1)S(1)}, bf16[32,128]{1,0:T(8,128)(2,1)S(1)}, u32[]{:S(2)}, u32[]{:S(2)}) collective-permute-start(bf16[32,128]{1,0:T(8,128)(2,1)S(1)} %get-tuple-element.40), channel_id=1, source_target_pairs={{0,8},{8,16},{16,24},{24,32},{32,40},{40,48},{48,56},{56,64},{64,7... | collective-permute-start | bytes 24584 | tf_op jit(solution)/shard_map/ppermute | solution.py:596
  7.9 31.8 %collective-permute-start.1 = (bf16[1040,256]{1,0:T(8,128)(2,1)S(1)}, bf16[1040,256]{1,0:T(8,128)(2,1)S(1)}, u32[]{:S(2)}, u32[]{:S(2)}) collective-permute-start(bf16[1040,256]{1,0:T(8,128)(2,1)S(1)} %get-tuple-element.24), channel_id=1, source_target_pairs={{0,24},{8,0},{16,8},{24,16},{32,56},{40,32},{48,40},{56,48},{64,88... | collective-permute-start | bytes 1597448 | tf_op jit(solution)/shard_map/ppermute | solution.py:597
  10.7 29.1 %collective-permute-start.2 = (bf16[1040,256]{1,0:T(8,128)(2,1)S(1)}, bf16[1040,256]{1,0:T(8,128)(2,1)S(1)}, u32[]{:S(2)}, u32[]{:S(2)}) collective-permute-start(bf16[1040,256]{1,0:T(8,128)(2,1)S(1)} %get-tuple-element.24), channel_id=1, source_target_pairs={{0,8},{8,16},{16,24},{24,0},{32,40},{40,48},{48,56},{56,32},{64,72... | collective-permute-start | bytes 1597448 | tf_op jit(solution)/shard_map/ppermute | solution.py:598
  11.3 28.5 %collective-permute-start.5 = (bf16[1040,256]{1,0:T(8,128)(2,1)S(1)}, bf16[1040,256]{1,0:T(8,128)(2,1)S(1)}, u32[]{:S(2)}, u32[]{:S(2)}) collective-permute-start(bf16[1040,256]{1,0:T(8,128)(2,1)S(1)} %get-tuple-element.25.pkv), channel_id=1, source_target_pairs={{32,64},{40,72},{48,80},{56,88},{0,96},{8,104},{16,112},{24,120},{... | collective-permute-start | bytes 1597448 | tf_op jit(solution)/shard_map/ppermute | solution.py:601
  12.5 27.3 %collective-permute-start.6 = (bf16[1040,256]{1,0:T(8,128)(2,1)S(1)}, bf16[1040,256]{1,0:T(8,128)(2,1)}, u32[]{:S(2)}, u32[]{:S(2)}) collective-permute-start(bf16[1040,256]{1,0:T(8,128)(2,1)S(1)} %get-tuple-element.25.pkv), channel_id=1, source_target_pairs={{64,96},{72,104},{80,112},{88,120},{0,64},{8,72},{16,80},{24,88},{... | collective-permute-start | bytes 1597448 | tf_op jit(solution)/shard_map/ppermute | solution.py:599
  13.8 11.8 %collective-permute-start.3 = (bf16[512,256]{1,0:T(8,128)(2,1)S(1)}, bf16[512,256]{1,0:T(8,128)(2,1)S(1)}, u32[]{:S(2)}, u32[]{:S(2)}) collective-permute-start(bf16[512,256]{1,0:T(8,128)(2,1)S(1)} %get-tuple-element.26.pq), channel_id=1, source_target_pairs={{32,0},{40,8},{48,16},{56,24},{96,32},{104,40},{112,48},{120,56},{... | collective-permute-start | bytes 786440 | tf_op jit(solution)/shard_map/ppermute | solution.py:600
  25.6 0.7 copy-start.3
  26.3 13.0 %collective-permute-start.4 = (bf16[512,256]{1,0:T(8,128)(2,1)S(1)}, bf16[512,256]{1,0:T(8,128)(2,1)}, u32[]{:S(2)}, u32[]{:S(2)}) collective-permute-start(bf16[512,256]{1,0:T(8,128)(2,1)S(1)} %get-tuple-element.26.pq), channel_id=1, source_target_pairs={{64,32},{72,40},{80,48},{88,56},{96,0},{104,8},{112,16},{120,24},{... | collective-permute-start | bytes 786440 | tf_op jit(solution)/shard_map/ppermute | solution.py:602
  34.9 46.7 %all-to-all-start.1 = ((f32[8,136,128]{2,1,0:T(8,128)}), f32[8,136,128]{2,1,0:T(8,128)S(1)}, u32[]{:S(2)}, u32[]{:S(2)}) async-start(f32[8,136,128]{2,1,0:T(8,128)} %convolve.1), calls=%async_computation.1 | async-start | bytes 1114112 | tf_op jit(solution)/shard_map/all_to_all | solution.py:605
  39.4 16.0 %collective-permute-start = (bf16[1040,256]{1,0:T(8,128)(2,1)S(1)}, bf16[1040,256]{1,0:T(8,128)(2,1)S(1)}, u32[]{:S(2)}, u32[]{:S(2)}) collective-permute-start(bf16[1040,256]{1,0:T(8,128)(2,1)S(1)} %get-tuple-element.24), channel_id=1, source_target_pairs={{0,16},{8,24},{16,0},{24,8},{32,48},{40,56},{48,32},{56,40},{64,80... | collective-permute-start | bytes 1597448 | tf_op jit(solution)/shard_map/ppermute | solution.py:603
  39.8 1.0 copy-start.4
  60.7 16.9 %collective-permute-start.11 = (bf16[1056,128]{1,0:T(8,128)(2,1)S(1)}, bf16[1056,128]{1,0:T(8,128)(2,1)S(1)}, u32[]{:S(2)}, u32[]{:S(2)}) collective-permute-start(bf16[1056,128]{1,0:T(8,128)(2,1)S(1)} %get-tuple-element.36), channel_id=1, source_target_pairs={{32,64},{40,72},{48,80},{56,88},{0,96},{8,104},{16,112},{24,120},{... | collective-permute-start | bytes 811016 | tf_op jit(solution)/shard_map/ppermute | solution.py:612
  62.0 15.6 %collective-permute-start.8 = (bf16[1056,128]{1,0:T(8,128)(2,1)S(1)}, bf16[1056,128]{1,0:T(8,128)(2,1)S(1)}, u32[]{:S(2)}, u32[]{:S(2)}) collective-permute-start(bf16[1056,128]{1,0:T(8,128)(2,1)S(1)} %get-tuple-element.36), channel_id=1, source_target_pairs={{64,80},{72,88},{80,64},{88,72},{96,112},{104,120},{112,96},{120,1... | collective-permute-start | bytes 811016 | tf_op jit(solution)/shard_map/ppermute | solution.py:610
  65.6 11.2 %collective-permute-start.10 = (bf16[1056,128]{1,0:T(8,128)(2,1)S(1)}, bf16[1056,128]{1,0:T(8,128)(2,1)S(1)}, u32[]{:S(2)}, u32[]{:S(2)}) collective-permute-start(bf16[1056,128]{1,0:T(8,128)(2,1)S(1)} %get-tuple-element.38), channel_id=1, source_target_pairs={{0,32},{8,40},{16,48},{24,56},{32,96},{40,104},{48,112},{56,120},{... | collective-permute-start | bytes 811016 | tf_op jit(solution)/shard_map/ppermute | solution.py:611
  66.9 10.6 %collective-permute-start.7 = (bf16[1056,128]{1,0:T(8,128)(2,1)S(1)}, bf16[1056,128]{1,0:T(8,128)(2,1)S(1)}, u32[]{:S(2)}, u32[]{:S(2)}) collective-permute-start(bf16[1056,128]{1,0:T(8,128)(2,1)S(1)} %get-tuple-element.35), channel_id=1, source_target_pairs={{64,72},{72,80},{80,88},{88,64},{96,104},{104,112},{112,120},{120,... | collective-permute-start | bytes 811016 | tf_op jit(solution)/shard_map/ppermute | solution.py:607
  68.8 10.9 %collective-permute-start.9 = (bf16[1056,128]{1,0:T(8,128)(2,1)S(1)}, bf16[1056,128]{1,0:T(8,128)(2,1)S(1)}, u32[]{:S(2)}, u32[]{:S(2)}) collective-permute-start(bf16[1056,128]{1,0:T(8,128)(2,1)S(1)} %get-tuple-element.37), channel_id=1, source_target_pairs={{64,88},{72,64},{80,72},{88,80},{96,120},{104,96},{112,104},{120,1... | collective-permute-start | bytes 811016 | tf_op jit(solution)/shard_map/ppermute | solution.py:608
  81.6 11.9 %all-to-all-start = ((bf16[8,128,128]{2,1,0:T(8,128)(2,1)}), bf16[8,128,128]{2,1,0:T(8,128)(2,1)S(1)}, u32[]{:S(2)}, u32[]{:S(2)}) async-start(bf16[8,128,128]{2,1,0:T(8,128)(2,1)} %combine.1), calls=%async_computation | async-start | bytes 524288 | tf_op jit(solution)/shard_map/all_to_all | solution.py:615
  89.6 1.9 %copy-start.1 = (bf16[1024,2048]{1,0:T(8,128)(2,1)}, bf16[1024,2048]{1,0:T(8,128)(2,1)S(1)}, u32[]{:S(2)}) copy-start(bf16[1024,2048]{1,0:T(8,128)(2,1)S(1)} %get-tuple-element.42.w) | copy-start | bytes 12582916
  93.5 2.2 %copy-start.2 = (bf16[1024,2048]{1,0:T(8,128)(2,1)S(1)}, bf16[1024,2048]{1,0:T(8,128)(2,1)}, u32[]{:S(2)}) copy-start(bf16[1024,2048]{1,0:T(8,128)(2,1)} %copy-done.1) | copy-start | bytes 12582916

commit v6 on v5

--- a/solution.py
+++ b/solution.py
@@ -83,13 +83,13 @@
                 late = d == 2
                 for h in range(2):
                     if z < 2:
-                        tiles.append((late, 2 + h, d))
+                        tiles.append((True, 2 + h, d))
                         if other < x:
                             tiles.append((late, h, d))
                         if h < 2 - UP_HALVES[x, other]:
                             tiles.append((late, 4 + h, d))
                     else:
-                        tiles.append((late, 2 * d + h, 2))
+                        tiles.append((True, 2 * d + h, 2))
                         if other > x:
                             tiles.append((late, 2 * d + h, 0))
                         if h >= 2 - UP_HALVES[other, x]:
@@ -107,9 +107,10 @@
 
 
 def project_kernel(
-    own, x_hbm, wq, wk, wv, wu, wg, gate, pkv, pxx, pq, gated, tail, x, w, sems
+    own, x_hbm, wq, wk, wv, wu, wg, gate, pkv, pxx, pr, pq, gated, tail, x, w, sems
 ):
     low_level = own[0] < 8
+    even_level = own[0] // SIDE % 2 == 0
     arrivals = [
         pltpu.make_async_copy(
             x_hbm.at[pl.ds(256 * i, 256)], x.at[pl.ds(256 * i, 256)], sems.at[i]
@@ -129,6 +130,7 @@
     )
     pkv[GATE_ROW : GATE_ROW + 16, :] = gates
     pxx[GATE_ROW : GATE_ROW + 16, :] = gates
+    pr[GATE_ROW : GATE_ROW + 16, :] = gates
     for c in loads[:3]:
         c.wait()
     for i in range(4):
@@ -141,17 +143,18 @@
         lanes = slice(128 * (i // 2), 128 * (i // 2) + 128)
         pkv[rows, :] = both
         pq[half, lanes] = query
-        if i >= 2:
-            pxx[rows, :] = both
-        else:
-
-            @pl.when(low_level)
-            def _():
-                pxx[rows, :] = both
-
-        @pl.when(jnp.logical_not(low_level))
-        def _():
-            pxx[half, lanes] = query
+        for pack, keys_go in ((pxx, low_level), (pr, even_level)):
+            if i >= 2:
+                pack[rows, :] = both
+            else:
+
+                @pl.when(keys_go)
+                def _(pack=pack):
+                    pack[rows, :] = both
+
+            @pl.when(jnp.logical_not(keys_go))
+            def _(pack=pack):
+                pack[half, lanes] = query
 
     for c in loads[3:]:
         c.wait()
@@ -168,12 +171,13 @@
         out_shape=(
             pack,
             pack,
+            pack,
             jax.ShapeDtypeStruct((HALF, 256), BF16),
             jax.ShapeDtypeStruct((TOK, 128), BF16),
             jax.ShapeDtypeStruct((32, 128), BF16),
         ),
         in_specs=[SM] + [HBM] * 6 + [VM],
-        out_specs=(VM,) * 5,
+        out_specs=(VM,) * 6,
         scratch_shapes=[
             pltpu.VMEM((TOK, 2048), BF16),
             pltpu.VMEM((2048, 640), BF16),
@@ -346,66 +350,61 @@
         weigh(start + count - 1, *first)
 
 
+def by_level(own, low_job, high_job):
+    pl.when(own[0] < 8)(low_job)
+    pl.when(own[0] >= 8)(high_job)
+
+
 def near_kernel(
-    table, own, pkv, pq, x1, x3, u, w, kx, ky,
-    m, l, acc, packs, query, gates, b1, b3, qpacks, sems, *per_tile,
+    table, own, pkv, pq, x1, x3, swapped,
+    m, l, acc, packs, query, gates, qpacks, sems, *per_tile,
 ):
-    low_level = own[0] < 8
-    high_level = jnp.logical_not(low_level)
+    own_copies = [*key_copies(pkv, packs, 0, sems), query_copy(pq, qpacks, 0, sems)]
     low_copies = [
         *key_copies(x1, packs, 1, sems),
         *key_copies(x3, packs, 3, sems),
-        query_copy(u, qpacks, 1, sems),
-        query_copy(w, qpacks, 2, sems),
+        query_copy(swapped, qpacks, 2, sems),
     ]
     high_copies = [
-        *key_copies(kx, packs, 1, sems),
-        *key_copies(ky, packs, 2, sems),
+        *key_copies(swapped, packs, 1, sems),
         query_copy(x1, qpacks, 1, sems),
         query_copy(x3, qpacks, 3, sems),
     ]
-    pl.when(low_level)(lambda: each(low_copies, "start"))
-    pl.when(high_level)(lambda: each(high_copies, "start"))
+    each(own_copies, "start")
+    by_level(own, lambda: each(low_copies, "start"), lambda: each(high_copies, "start"))
     for n in range(2, QUERIES):
         m[n] = jnp.full((HALF, 128), LOW, F32)
         l[n] = jnp.zeros((HALF, 128), F32)
         acc[n] = jnp.zeros((HALF, 128), F32)
-    packs[0] = pkv[...]
+    each(own_copies, "wait")
     unpack_keys(packs, (0,), gates)
-    query[0] = pq[:, :128]
-    query[1] = pq[:, 128:]
-    diagonal(pkv, pq, m, l, acc)
-
-    @pl.when(low_level)
-    def _():
+    unpack_queries(qpacks, (0,), query)
+    diagonal(packs.at[0], qpacks.at[0], m, l, acc)
+
+    def low_job():
         each(low_copies, "wait")
         unpack_keys(packs, (1, 3), gates)
-        unpack_queries(qpacks, (1, 2), query)
-
-    @pl.when(high_level)
-    def _():
+        unpack_queries(qpacks, (2,), query)
+
+    def high_job():
         each(high_copies, "wait")
-        unpack_keys(packs, (1, 2), gates)
+        unpack_keys(packs, (1,), gates)
         unpack_queries(qpacks, (1, 3), query)
 
+    by_level(own, low_job, high_job)
     count = table[own[0], 2, 0]
     run_tiles(table, own, 0, count, False, packs, query, gates, per_tile, m, l, acc)
-    finish(m, l, acc, 2, b1)
-    finish(m, l, acc, 6, b3)
 
 
 def far_kernel(
-    table, own, x2, m_in, l_in, acc_in, packs_in, query_in, gates_in,
-    o_own, lse_own, b1, b2,
+    table, own, x2, turned, m_in, l_in, acc_in, packs_in, query_in, gates_in,
+    o_own, lse_own, b1, b2, b3,
     m, l, acc, packs, query, gates, qpacks, sems, *per_tile,
 ):
-    low_level = own[0] < 8
-    high_level = jnp.logical_not(low_level)
-    low_copies = key_copies(x2, packs, 2, sems)
-    high_copies = [query_copy(x2, qpacks, 2, sems)]
-    pl.when(low_level)(lambda: each(low_copies, "start"))
-    pl.when(high_level)(lambda: each(high_copies, "start"))
-    for n in range(6):
+    low_copies = [*key_copies(x2, packs, 2, sems), query_copy(turned, qpacks, 1, sems)]
+    high_copies = [*key_copies(turned, packs, 2, sems), query_copy(x2, qpacks, 2, sems)]
+    by_level(own, lambda: each(low_copies, "start"), lambda: each(high_copies, "start"))
+    for n in range(QUERIES):
         m[n] = m_in[n]
         l[n] = l_in[n]
         acc[n] = acc_in[n]
@@ -414,26 +413,24 @@
         packs[n, :TOK, :] = packs_in[n, :TOK, :]
         gates[n] = gates_in[n]
 
-    @pl.when(low_level)
-    def _():
+    def low_job():
         each(low_copies, "wait")
-        unpack_keys(packs, (2,), gates)
-
-    @pl.when(high_level)
-    def _():
-        packs[2, :TOK, :] = packs_in[2, :TOK, :]
-        gates[2] = gates_in[2]
+        unpack_queries(qpacks, (1,), query)
+
+    def high_job():
         each(high_copies, "wait")
         unpack_queries(qpacks, (2,), query)
 
+    by_level(own, low_job, high_job)
+    unpack_keys(packs, (2,), gates)
     near = table[own[0], 2, 0]
     run_tiles(table, own, near, TILES - near, True, packs, query, gates, per_tile, m, l, acc)
     for n in range(2):
         total = jnp.maximum(l[n], TINY)
         o_own[n] = acc[n] / total
         lse_own[n] = m[n] + jnp.log2(total)
-    finish(m, l, acc, 2, b1)
-    finish(m, l, acc, 4, b2)
+    for n, back in enumerate((b1, b2, b3)):
+        finish(m, l, acc, 2 * n + 2, back)
 
 
 SEMS = [pltpu.SemaphoreType.DMA((3, 4))]
@@ -455,27 +452,27 @@
 def attend_near(table, own, *packs):
     return pl.pallas_call(
         near_kernel,
-        out_shape=arrays(STATE + SLOTS + BACK * 2),
-        in_specs=[SM, SM, VM, VM] + [ANY] * 6,
-        out_specs=(VM,) * 8,
+        out_shape=arrays(STATE + SLOTS),
+        in_specs=[SM, SM] + [ANY] * 5,
+        out_specs=(VM,) * 6,
         scratch_shapes=scratch(QPACKS) + SEMS + scratch(TILE),
         compiler_params=params(24),
-        cost_estimate=cost(12 * 4 * HALF * TOK * 256, 8 << 20),
+        cost_estimate=cost(6 * 4 * HALF * TOK * 256, 8 << 20),
         name="attend_near",
     )(table, own, *packs)
 
 
-def attend_far(table, own, x2, state):
+def attend_far(table, own, x2, turned, state):
     return pl.pallas_call(
         far_kernel,
-        out_shape=arrays([((2, HALF, 128), F32)] * 2 + BACK * 2),
-        in_specs=[SM, SM, ANY] + [VM] * 6,
-        out_specs=(VM,) * 4,
+        out_shape=arrays([((2, HALF, 128), F32)] * 2 + BACK * 3),
+        in_specs=[SM, SM, ANY, ANY] + [VM] * 6,
+        out_specs=(VM,) * 5,
         scratch_shapes=scratch(STATE + SLOTS + QPACKS) + SEMS + scratch(TILE),
         compiler_params=params(30),
-        cost_estimate=cost(5 * 4 * HALF * TOK * 256, 8 << 20),
+        cost_estimate=cost(10 * 4 * HALF * TOK * 256, 8 << 20),
         name="attend_far",
-    )(table, own, x2, *state)
+    )(table, own, x2, turned, *state)
 
 
 def combine_kernel(own, o_own, lse_own, x1, x2, x3, u, w, out):
@@ -592,28 +589,32 @@
     )
     own = lax.axis_index("sp").astype(I32).reshape(1)
     table = jnp.asarray(work_table())
-    pkv, pxx, pq, gated, tail = project(own, x, wq, wk, wv, wu, wg, gate.reshape(8, 128))
+    pkv, pxx, pr, pq, gated, tail = project(own, x, wq, wk, wv, wu, wg, gate.reshape(8, 128))
     halo = lax.ppermute(tail, "sp", [(i, i + 1) for i in range(15)])
     x1 = lax.ppermute(pxx, "sp", moves(-1, 0))
     x3 = lax.ppermute(pxx, "sp", moves(-3, 0))
-    ky = lax.ppermute(pkv, "sp", levels((2, 3), (0, 2)))
-    u = lax.ppermute(pq, "sp", levels((1, 0), (3, 1)))
-    kz = lax.ppermute(pkv, "sp", levels((1, 2), (0, 3)))
-    w = lax.ppermute(pq, "sp", levels((2, 1), (3, 0)))
+    turned = lax.ppermute(pr, "sp", levels((0, 2), (2, 3), (3, 1), (1, 0)))
+    swapped = lax.ppermute(pxx, "sp", levels((0, 3), (1, 2), (2, 1), (3, 0)))
     x2 = lax.ppermute(pxx, "sp", moves(-2, 0))
     conv = convolve(gated, halo, taps, gain.reshape(1, 128))
     conv_parts = lax.all_to_all(conv, "tp", 0, 0, tiled=True)
-    *state, b1, b3 = attend_near(table, own, pkv, pq, x1, x3, u, w, kz, ky)
+    near = (in_hbm(pkv), in_hbm(pq), x1, x3, swapped)
+    state = attend_near(table, own, *near)
+    far = attend_far(table, own, x2, turned, state)
+    o_own, lse_own, b1, b2, b3 = far
     back1 = lax.ppermute(b1, "sp", along_x(1))
     back3 = lax.ppermute(b3, "sp", along_x(3))
-    o_own, lse_own, bu, b2 = attend_far(table, own, x2, state)
     back2 = lax.ppermute(b2, "sp", along_x(2))
-    back_u = lax.ppermute(bu, "sp", levels((0, 1), (1, 3)))
+    back_u = lax.ppermute(b1, "sp", levels((0, 1), (1, 3)))
     back_w = lax.ppermute(b2, "sp", levels((1, 2), (0, 3)))
     conv_mixed, w_attn = conv_out(conv_parts, w_out)
     mixed = combine(own, o_own, lse_own, (back1, back2, back3, back_u, back_w))
     attn_parts = lax.all_to_all(mixed, "tp", 0, 0, tiled=True)
     return attn_out(attn_parts, conv_mixed, w_attn)
+
+
+def in_hbm(value):
+    return pltpu.with_memory_space_constraint(value, pltpu.HBM)
 
 
 def solution(mesh):

time: 97.8 us -> 108 us (1.10)
  the two profiles are of different devices: /device:TPU:102 before, /device:TPU:1 now
where the time goes in v6:
time: 108 us; the launch traced here: 107 us
  starting transfers between devices  54.1 us (50%)
  Pallas kernels  33.3 us (31%)
  waiting for transfers between devices  13.2 us (12%)
  local copies, waits for them, and re-layouts  6.31 us (6%)
    all_to_all x1, starting transfers between devices, layer(): conv_parts = lax.all_to_all(conv, 'tp', 0, 0, tiled=True)  17.3 us
    ppermute x1, waiting for transfers between devices, layer(): back_w = lax.ppermute(b2, 'sp', levels((1, 2), (0, 3)))  10.9 us
    pallas_call x1, Pallas kernels, attend_far(): pl.pallas_call(far_kernel, out_shape=arrays([((2, HALF, 128), F32)] * 2 +...  10.1 us
    ppermute x1, starting transfers between devices, layer(): back_w = lax.ppermute(b2, 'sp', levels((1, 2), (0, 3)))  8.69 us
    pallas_call x1, Pallas kernels, attend_near(): pl.pallas_call(near_kernel, out_shape=arrays(STATE + SLOTS), in_specs=[SM...  8.14 us
    ppermute x1, starting transfers between devices, layer(): turned = lax.ppermute(pr, 'sp', levels((0, 2), (2, 3), (3, 1), (1, 0)))  6.93 us
    unnamed x16, local copies, waits for them, and re-layouts  6.31 us
    pallas_call x1, Pallas kernels, project(): pl.pallas_call(project_kernel, out_shape=(pack, pack, pack, jax.ShapeDtyp...  5.95 us
  transfers between devices with their start and end apart: 13, of which 3 were waited for; matrix products, arithmetic and copies ran while one was open for 0% of the time, Pallas kernels for 24%

profile of v6, /device:TPU:1, one launch (start us, length us, event | category | flops | bytes accessed | tf_op | source)
XLA Modules:
  0.0 107.1 jit_solution(18098550461703523405)
XLA Ops:
  0.0 0.7 copy-done.3
  0.7 6.0 %project.1 = (bf16[1040,256]{1,0:T(8,128)(2,1)S(1)}, bf16[1040,256]{1,0:T(8,128)(2,1)S(1)}, bf16[1040,256]{1,0:T(8,128)(2,1)S(1)}, bf16[512,256]{1,0:T(8,128)(2,...) custom-call(s32[1]{0:T(128)} %bitcast.own, bf16[1024,2048]{1,0:T(8,128)(2,1)} %x_hbm.1, ...), custom_call_target="tpu_custom_call" | custom-call | flops 2684354560 | bytes 8388608 | tf_op jit(solution)/shard_map/project/pallas_call | solution.py:169
  6.7 0.8 copy-done.6
  7.5 0.7 copy-done.7
  8.2 3.3 %collective-permute-start.2 = (bf16[1040,256]{1,0:T(8,128)(2,1)S(1)}, bf16[1040,256]{1,0:T(8,128)(2,1)S(1)}, u32[]{:S(2)}, u32[]{:S(2)}) collective-permute-start(bf16[1040,256]{1,0:T(8,128)(2,1)S(1)} %get-tuple-element.24), channel_id=1, source_target_pairs={{0,24},{8,0},{16,8},{24,16},{32,56},{40,32},{48,40},{56,48},{64,88... | collective-permute-start | bytes 1597448 | tf_op jit(solution)/shard_map/ppermute | solution.py:594
  11.5 3.8 %collective-permute-start.4 = (bf16[1040,256]{1,0:T(8,128)(2,1)S(1)}, bf16[1040,256]{1,0:T(8,128)(2,1)}, u32[]{:S(2)}, u32[]{:S(2)}) collective-permute-start(bf16[1040,256]{1,0:T(8,128)(2,1)S(1)} %get-tuple-element.24), channel_id=1, source_target_pairs={{0,96},{8,104},{16,112},{24,120},{32,64},{40,72},{48,80},{56,88},{... | collective-permute-start | bytes 1597448 | tf_op jit(solution)/shard_map/ppermute | solution.py:597
  15.3 2.1 %collective-permute-start.10 = (bf16[32,128]{1,0:T(8,128)(2,1)S(1)}, bf16[32,128]{1,0:T(8,128)(2,1)S(1)}, u32[]{:S(2)}, u32[]{:S(2)}) collective-permute-start(bf16[32,128]{1,0:T(8,128)(2,1)S(1)} %get-tuple-element.40), channel_id=1, source_target_pairs={{0,8},{8,16},{16,24},{24,32},{32,40},{40,48},{48,56},{56,64},{64,7... | collective-permute-start | bytes 24584 | tf_op jit(solution)/shard_map/ppermute | solution.py:593
  17.3 3.7 %collective-permute-start = (bf16[1040,256]{1,0:T(8,128)(2,1)S(1)}, bf16[1040,256]{1,0:T(8,128)(2,1)S(1)}, u32[]{:S(2)}, u32[]{:S(2)}) collective-permute-start(bf16[1040,256]{1,0:T(8,128)(2,1)S(1)} %get-tuple-element.24), channel_id=1, source_target_pairs={{0,16},{8,24},{16,0},{24,8},{32,48},{40,56},{48,32},{56,40},{64,80... | collective-permute-start | bytes 1597448 | tf_op jit(solution)/shard_map/ppermute | solution.py:598
  21.1 1.3 %collective-permute-done.10.halo = bf16[32,128]{1,0:T(8,128)(2,1)S(1)} collective-permute-done((bf16[32,128]{1,0:T(8,128)(2,1)S(1)}, bf16[32,128]{1,0:T(8,128)(2,1)S(1)}, u32[]{:S(2)}, u32[]{:S(2)}) %collective-permute-start.10) | collective-permute-done | bytes 8224 | tf_op jit(solution)/shard_map/ppermute | solution.py:593
  22.4 6.9 %collective-permute-start.1 = (bf16[1040,256]{1,0:T(8,128)(2,1)S(1)}, bf16[1040,256]{1,0:T(8,128)(2,1)}, u32[]{:S(2)}, u32[]{:S(2)}) collective-permute-start(bf16[1040,256]{1,0:T(8,128)(2,1)S(1)} %get-tuple-element.25), channel_id=1, source_target_pairs={{0,64},{8,72},{16,80},{24,88},{64,96},{72,104},{80,112},{88,120},{... | collective-permute-start | bytes 1597448 | tf_op jit(solution)/shard_map/ppermute | solution.py:596
  29.4 2.2 %convolve.1 = f32[8,136,128]{2,1,0:T(8,128)} custom-call(bf16[1024,128]{1,0:T(8,128)(2,1)S(1)} %get-tuple-element.39.gated, bf16[32,128]{1,0:T(8,128)(2,1)S(1)} %collective-permute-done.10.halo, f32[31,128]{1,0:T(8,128)S(1)} %copy-done.2, f32[1,128]{1,0:T(1,128)S(1)} %bitcast.4), custom_call_target="tpu_custom_call" | custom-call | flops 520093696 | bytes 1048576 | tf_op jit(solution)/shard_map/convolve/pallas_call | solution.py:213
  31.6 17.3 %all-to-all-start.1 = ((f32[8,136,128]{2,1,0:T(8,128)}), f32[8,136,128]{2,1,0:T(8,128)S(1)}, u32[]{:S(2)}, u32[]{:S(2)}) async-start(f32[8,136,128]{2,1,0:T(8,128)} %convolve.1), calls=%async_computation.1 | async-start | bytes 1114112 | tf_op jit(solution)/shard_map/all_to_all | solution.py:600
  49.0 8.1 %attend_near.1 = (f32[8,512,128]{2,1,0:T(8,128)S(1)}, f32[8,512,128]{2,1,0:T(8,128)S(1)}, f32[8,512,128]{2,1,0:T(8,128)S(1)}, bf16[4,1040,256]{2,1,0:T(8,128)(2,...) custom-call(s32[16,3,16]{2,1,0:T(4,128)S(1)} %copy-done.5, s32[1]{0:T(128)} %bitcast.own, ...), custom_call_target="tpu_custom_call" | custom-call | flops 3221225472 | bytes 8388608 | tf_op jit(solution)/shard_map/attend_near/pallas_call | solution.py:453
  57.1 10.1 %attend_far.1 = (f32[2,512,128]{2,1,0:T(8,128)S(1)}, f32[2,512,128]{2,1,0:T(8,128)S(1)}, bf16[1056,128]{1,0:T(8,128)(2,1)S(1)}, bf16[1056,128]{1,0:T(8,128)(2,1)S(1)}, bf16[1056,128]{1,0:T(8,128)(2,1)S(1)}) custom-call(s32[16,3,16]{2,1,0:T(4,128)S(1)} %copy-done.5, s32[1]{0:T(128)} %bitcast.own, bf16[1040,256]{1,0:T(8,128)(2,1)S(1)} %collective-permute-done.x2, ...), custom_call_target="tpu_custom_call" | custom-call | flops 5368709120 | bytes 8388608 | tf_op jit(solution)/shard_map/attend_far/pallas_call | solution.py:466
  69.3 1.3 %collective-permute-start.8 = (bf16[1056,128]{1,0:T(8,128)(2,1)S(1)}, bf16[1056,128]{1,0:T(8,128)(2,1)S(1)}, u32[]{:S(2)}, u32[]{:S(2)}) collective-permute-start(bf16[1056,128]{1,0:T(8,128)(2,1)S(1)} %get-tuple-element.36), channel_id=1, source_target_pairs={{0,32},{8,40},{16,48},{24,56},{32,96},{40,104},{48,112},{56,120},{... | collective-permute-start | bytes 811016 | tf_op jit(solution)/shard_map/ppermute | solution.py:608
  70.6 8.7 %collective-permute-start.9 = (bf16[1056,128]{1,0:T(8,128)(2,1)S(1)}, bf16[1056,128]{1,0:T(8,128)(2,1)S(1)}, u32[]{:S(2)}, u32[]{:S(2)}) collective-permute-start(bf16[1056,128]{1,0:T(8,128)(2,1)S(1)} %get-tuple-element.37), channel_id=1, source_target_pairs={{32,64},{40,72},{48,80},{56,88},{0,96},{8,104},{16,112},{24,120},{... | collective-permute-start | bytes 811016 | tf_op jit(solution)/shard_map/ppermute | solution.py:609
  79.3 10.9 %collective-permute-done.9.w = bf16[1056,128]{1,0:T(8,128)(2,1)S(1)} collective-permute-done((bf16[1056,128]{1,0:T(8,128)(2,1)S(1)}, bf16[1056,128]{1,0:T(8,128)(2,1)S(1)}, u32[]{:S(2)}, u32[]{:S(2)}) %collective-permute-start.9) | collective-permute-done | bytes 270368 | tf_op jit(solution)/shard_map/ppermute | solution.py:609
  90.2 1.8 %combine.1 = bf16[8,128,128]{2,1,0:T(8,128)(2,1)} custom-call(s32[1]{0:T(128)} %bitcast.own, f32[2,512,128]{2,1,0:T(8,128)S(1)} %get-tuple-element.34.o_own, f32[2,512,128]{2,1,0:T(8,128)S(1)} %get-tuple-element.35.lse_own, bf16[1056,128]{1,0:T(8,128)(2,1)S(1)} %collective-permute-done.5.x1, bf16[1056,128]{1,0:T(8,128)(2,1)S(1)} %collective-permute-done.6.x2, ...), custom_call_target="tpu_custom_call" | custom-call | flops 536870912 | bytes 2097152 | tf_op jit(solution)/shard_map/combine/pallas_call | solution.py:501
  92.0 4.9 %all-to-all-start = ((bf16[8,128,128]{2,1,0:T(8,128)(2,1)}), bf16[8,128,128]{2,1,0:T(8,128)(2,1)S(1)}, u32[]{:S(2)}, u32[]{:S(2)}) async-start(bf16[8,128,128]{2,1,0:T(8,128)(2,1)} %combine.1), calls=%async_computation | async-start | bytes 524288 | tf_op jit(solution)/shard_map/all_to_all | solution.py:612
  96.9 3.6 %conv_out.1 = (f32[128,2048]{1,0:T(8,128)S(1)}, bf16[1024,2048]{1,0:T(8,128)(2,1)S(1)}) custom-call(f32[8,136,128]{2,1,0:T(8,128)S(1)} %all-to-all-done.1.parts, bf16[2048,2048]{1,0:T(8,128)(2,1)} %w_hbm.1), custom_call_target="tpu_custom_call" | custom-call | flops 2147483648 | bytes 6291456 | tf_op jit(solution)/shard_map/conv_out/pallas_call | solution.py:538
  100.5 1.9 %copy-done = bf16[1024,2048]{1,0:T(8,128)(2,1)} copy-done((bf16[1024,2048]{1,0:T(8,128)(2,1)}, bf16[1024,2048]{1,0:T(8,128)(2,1)S(1)}, u32[]{:S(2)}) %copy-start) | copy-done | bytes 4194328
  102.5 0.9 all-to-all-done.parts
  103.4 2.2 %copy-done.1 = bf16[1024,2048]{1,0:T(8,128)(2,1)S(1)} copy-done((bf16[1024,2048]{1,0:T(8,128)(2,1)S(1)}, bf16[1024,2048]{1,0:T(8,128)(2,1)}, u32[]{:S(2)}) %copy-start.1) | copy-done | bytes 4194328
  105.6 1.5 %attn_out.1 = bf16[128,2048]{1,0:T(8,128)(2,1)} custom-call(bf16[8,128,128]{2,1,0:T(8,128)(2,1)S(1)} %all-to-all-done.parts, f32[128,2048]{1,0:T(8,128)S(1)} %get-tuple-element.41.conv, bf16[1024,2048]{1,0:T(8,128)(2,1)S(1)} %copy-done.1), custom_call_target="tpu_custom_call" | custom-call | flops 2147483648 | bytes 6291456 | tf_op jit(solution)/shard_map/attn_out/pallas_call | solution.py:566
  (25 shorter events, 2.1 us)
Async XLA Ops:
  0.0 0.7 copy-start.3
  0.7 28.7 %copy-start.2 = (f32[31,128]{1,0:T(8,128)S(1)}, f32[31,128]{1,0:T(8,128)}, u32[]{:S(2)}) copy-start(f32[31,128]{1,0:T(8,128)} %taps.1) | copy-start | bytes 47620
  0.7 28.7 %copy-start.4 = (f32[128]{0:T(128)S(1)}, f32[128]{0:T(128)}, u32[]{:S(2)}) copy-start(f32[128]{0:T(128)} %param.18) | copy-start | bytes 1540
  6.7 0.8 copy-start.6
  7.5 0.7 copy-start.7
  8.2 40.8 %copy-start.5 = (s32[16,3,16]{2,1,0:T(4,128)S(1)}, s32[16,3,16]{2,1,0:T(4,128)}, u32[]{:S(2)}) copy-start(s32[16,3,16]{2,1,0:T(4,128)} %constant.8.clone.table) | copy-start | bytes 9220
  8.2 40.8 %collective-permute-start.2 = (bf16[1040,256]{1,0:T(8,128)(2,1)S(1)}, bf16[1040,256]{1,0:T(8,128)(2,1)S(1)}, u32[]{:S(2)}, u32[]{:S(2)}) collective-permute-start(bf16[1040,256]{1,0:T(8,128)(2,1)S(1)} %get-tuple-element.24), channel_id=1, source_target_pairs={{0,24},{8,0},{16,8},{24,16},{32,56},{40,32},{48,40},{56,48},{64,88... | collective-permute-start | bytes 1597448 | tf_op jit(solution)/shard_map/ppermute | solution.py:594
  11.5 37.5 %collective-permute-start.3 = (bf16[1040,256]{1,0:T(8,128)(2,1)S(1)}, bf16[1040,256]{1,0:T(8,128)(2,1)S(1)}, u32[]{:S(2)}, u32[]{:S(2)}) collective-permute-start(bf16[1040,256]{1,0:T(8,128)(2,1)S(1)} %get-tuple-element.24), channel_id=1, source_target_pairs={{0,8},{8,16},{16,24},{24,0},{32,40},{40,48},{48,56},{56,32},{64,72... | collective-permute-start | bytes 1597448 | tf_op jit(solution)/shard_map/ppermute | solution.py:595
  11.5 37.5 %collective-permute-start.4 = (bf16[1040,256]{1,0:T(8,128)(2,1)S(1)}, bf16[1040,256]{1,0:T(8,128)(2,1)}, u32[]{:S(2)}, u32[]{:S(2)}) collective-permute-start(bf16[1040,256]{1,0:T(8,128)(2,1)S(1)} %get-tuple-element.24), channel_id=1, source_target_pairs={{0,96},{8,104},{16,112},{24,120},{32,64},{40,72},{48,80},{56,88},{... | collective-permute-start | bytes 1597448 | tf_op jit(solution)/shard_map/ppermute | solution.py:597
  15.3 7.2 %collective-permute-start.10 = (bf16[32,128]{1,0:T(8,128)(2,1)S(1)}, bf16[32,128]{1,0:T(8,128)(2,1)S(1)}, u32[]{:S(2)}, u32[]{:S(2)}) collective-permute-start(bf16[32,128]{1,0:T(8,128)(2,1)S(1)} %get-tuple-element.40), channel_id=1, source_target_pairs={{0,8},{8,16},{16,24},{24,32},{32,40},{40,48},{48,56},{56,64},{64,7... | collective-permute-start | bytes 24584 | tf_op jit(solution)/shard_map/ppermute | solution.py:593
  17.3 39.8 %collective-permute-start = (bf16[1040,256]{1,0:T(8,128)(2,1)S(1)}, bf16[1040,256]{1,0:T(8,128)(2,1)S(1)}, u32[]{:S(2)}, u32[]{:S(2)}) collective-permute-start(bf16[1040,256]{1,0:T(8,128)(2,1)S(1)} %get-tuple-element.24), channel_id=1, source_target_pairs={{0,16},{8,24},{16,0},{24,8},{32,48},{40,56},{48,32},{56,40},{64,80... | collective-permute-start | bytes 1597448 | tf_op jit(solution)/shard_map/ppermute | solution.py:598
  22.4 34.7 %collective-permute-start.1 = (bf16[1040,256]{1,0:T(8,128)(2,1)S(1)}, bf16[1040,256]{1,0:T(8,128)(2,1)}, u32[]{:S(2)}, u32[]{:S(2)}) collective-permute-start(bf16[1040,256]{1,0:T(8,128)(2,1)S(1)} %get-tuple-element.25), channel_id=1, source_target_pairs={{0,64},{8,72},{16,80},{24,88},{64,96},{72,104},{80,112},{88,120},{... | collective-permute-start | bytes 1597448 | tf_op jit(solution)/shard_map/ppermute | solution.py:596
  31.6 60.4 %all-to-all-start.1 = ((f32[8,136,128]{2,1,0:T(8,128)}), f32[8,136,128]{2,1,0:T(8,128)S(1)}, u32[]{:S(2)}, u32[]{:S(2)}) async-start(f32[8,136,128]{2,1,0:T(8,128)} %convolve.1), calls=%async_computation.1 | async-start | bytes 1114112 | tf_op jit(solution)/shard_map/all_to_all | solution.py:600
  67.2 12.1 %collective-permute-start.5 = (bf16[1056,128]{1,0:T(8,128)(2,1)S(1)}, bf16[1056,128]{1,0:T(8,128)(2,1)S(1)}, u32[]{:S(2)}, u32[]{:S(2)}) collective-permute-start(bf16[1056,128]{1,0:T(8,128)(2,1)S(1)} %get-tuple-element.36), channel_id=1, source_target_pairs={{64,72},{72,80},{80,88},{88,64},{96,104},{104,112},{112,120},{120,... | collective-permute-start | bytes 811016 | tf_op jit(solution)/shard_map/ppermute | solution.py:605
  67.9 11.4 %collective-permute-start.6 = (bf16[1056,128]{1,0:T(8,128)(2,1)S(1)}, bf16[1056,128]{1,0:T(8,128)(2,1)S(1)}, u32[]{:S(2)}, u32[]{:S(2)}) collective-permute-start(bf16[1056,128]{1,0:T(8,128)(2,1)S(1)} %get-tuple-element.37), channel_id=1, source_target_pairs={{64,80},{72,88},{80,64},{88,72},{96,112},{104,120},{112,96},{120,1... | collective-permute-start | bytes 811016 | tf_op jit(solution)/shard_map/ppermute | solution.py:607
  68.6 10.7 %collective-permute-start.7 = (bf16[1056,128]{1,0:T(8,128)(2,1)S(1)}, bf16[1056,128]{1,0:T(8,128)(2,1)S(1)}, u32[]{:S(2)}, u32[]{:S(2)}) collective-permute-start(bf16[1056,128]{1,0:T(8,128)(2,1)S(1)} %get-tuple-element.38), channel_id=1, source_target_pairs={{64,88},{72,64},{80,72},{88,80},{96,120},{104,96},{112,104},{120,1... | collective-permute-start | bytes 811016 | tf_op jit(solution)/shard_map/ppermute | solution.py:606
  69.3 10.0 %collective-permute-start.8 = (bf16[1056,128]{1,0:T(8,128)(2,1)S(1)}, bf16[1056,128]{1,0:T(8,128)(2,1)S(1)}, u32[]{:S(2)}, u32[]{:S(2)}) collective-permute-start(bf16[1056,128]{1,0:T(8,128)(2,1)S(1)} %get-tuple-element.36), channel_id=1, source_target_pairs={{0,32},{8,40},{16,48},{24,56},{32,96},{40,104},{48,112},{56,120},{... | collective-permute-start | bytes 811016 | tf_op jit(solution)/shard_map/ppermute | solution.py:608
  70.6 19.7 %collective-permute-start.9 = (bf16[1056,128]{1,0:T(8,128)(2,1)S(1)}, bf16[1056,128]{1,0:T(8,128)(2,1)S(1)}, u32[]{:S(2)}, u32[]{:S(2)}) collective-permute-start(bf16[1056,128]{1,0:T(8,128)(2,1)S(1)} %get-tuple-element.37), channel_id=1, source_target_pairs={{32,64},{40,72},{48,80},{56,88},{0,96},{8,104},{16,112},{24,120},{... | collective-permute-start | bytes 811016 | tf_op jit(solution)/shard_map/ppermute | solution.py:609
  92.0 11.4 %all-to-all-start = ((bf16[8,128,128]{2,1,0:T(8,128)(2,1)}), bf16[8,128,128]{2,1,0:T(8,128)(2,1)S(1)}, u32[]{:S(2)}, u32[]{:S(2)}) async-start(bf16[8,128,128]{2,1,0:T(8,128)(2,1)} %combine.1), calls=%async_computation | async-start | bytes 524288 | tf_op jit(solution)/shard_map/all_to_all | solution.py:612
  100.5 1.9 %copy-start = (bf16[1024,2048]{1,0:T(8,128)(2,1)}, bf16[1024,2048]{1,0:T(8,128)(2,1)S(1)}, u32[]{:S(2)}) copy-start(bf16[1024,2048]{1,0:T(8,128)(2,1)S(1)} %get-tuple-element.42.w) | copy-start | bytes 12582916
  103.4 2.2 %copy-start.1 = (bf16[1024,2048]{1,0:T(8,128)(2,1)S(1)}, bf16[1024,2048]{1,0:T(8,128)(2,1)}, u32[]{:S(2)}) copy-start(bf16[1024,2048]{1,0:T(8,128)(2,1)} %copy-done) | copy-start | bytes 12582916

commit v7 on v6

--- a/solution.py
+++ b/solution.py
@@ -18,7 +18,7 @@
 GATE_ROW = TOK
 PACK_ROWS = TOK + 16
 BACK_ROWS = HALF + 16
-TILES = 15
+TILES = 17
 LOG2E = 1.4426950408889634
 SCALE = HEAD**-0.5 * LOG2E
 LOW = -1e30
@@ -70,7 +70,7 @@
     return top, mid, (rest - mid.astype(F32)).astype(BF16)
 
 
-UP_HALVES = np.array([[0, 0, 0, 1], [0, 0, 1, 2], [0, 1, 2, 2], [1, 2, 2, 2]])
+UP_HALVES = np.array([[0, 0, 0, 1], [0, 0, 1, 0], [0, 1, 0, 2], [1, 0, 2, 2]])
 
 
 def work_table():
@@ -95,10 +95,10 @@
                         if h >= 2 - UP_HALVES[other, x]:
                             tiles.append((late, 2 * d + h, 1))
             near = sum(not t[0] for t in tiles)
-            assert len(tiles) == TILES and near % 2 == 1
+            assert len(tiles) <= TILES and len(tiles) % 2 == 1 and near % 2 == 1
             for n, (_, q, k) in enumerate(sorted(tiles)):
                 table[z * SIDE + x, :2, n] = q, k
-            table[z * SIDE + x, 2, 0] = near
+            table[z * SIDE + x, 2, :2] = near, len(tiles)
     return table
 
 
@@ -107,7 +107,8 @@
 
 
 def project_kernel(
-    own, x_hbm, wq, wk, wv, wu, wg, gate, pkv, pxx, pr, pq, gated, tail, x, w, sems
+    own, x_hbm, wq, wk, wv, wu, wg, gate_hbm, pkv_hbm, pxx, pr, pq_hbm, gated, tail,
+    x, w, pkv, pq, gate, sems,
 ):
     low_level = own[0] < 8
     even_level = own[0] // SIDE % 2 == 0
@@ -121,8 +122,10 @@
         pltpu.make_async_copy(source, w.at[:, pl.ds(128 * n, 128)], sems.at[4 + n])
         for n, source in enumerate((wk, wv, wq, wu, wg))
     ]
-    for c in (*loads[:3], *arrivals, *loads[3:]):
+    gate_load = pltpu.make_async_copy(gate_hbm, gate, sems.at[9])
+    for c in (gate_load, *loads[:3], *arrivals, *loads[3:]):
         c.start()
+    gate_load.wait()
     zero = jnp.zeros((8, 128), BF16)
     top, mid, low = split3(gate[...] * (-LOG2E))
     gates = jnp.concatenate(
@@ -156,12 +159,20 @@
             def _(pack=pack):
                 pack[half, lanes] = query
 
+    keeps = [
+        pltpu.make_async_copy(pkv, pkv_hbm, sems.at[10]),
+        pltpu.make_async_copy(pq, pq_hbm, sems.at[11]),
+    ]
+    for c in keeps:
+        c.start()
     for c in loads[3:]:
         c.wait()
     for i in range(4):
         rows = gate_rows(dot(x[256 * i : 256 * i + 256, :], w[:, 384:]))
         gated[256 * i : 256 * i + 256, :] = rows
     tail[...] = rows[224:, :]
+    for c in keeps:
+        c.wait()
 
 
 def project(own, x, wq, wk, wv, wu, wg, gate):
@@ -169,19 +180,22 @@
     return pl.pallas_call(
         project_kernel,
         out_shape=(
+            pltpu.HBM((PACK_ROWS, 256), BF16),
             pack,
             pack,
-            pack,
-            jax.ShapeDtypeStruct((HALF, 256), BF16),
+            pltpu.HBM((HALF, 256), BF16),
             jax.ShapeDtypeStruct((TOK, 128), BF16),
             jax.ShapeDtypeStruct((32, 128), BF16),
         ),
-        in_specs=[SM] + [HBM] * 6 + [VM],
-        out_specs=(VM,) * 6,
+        in_specs=[SM] + [HBM] * 7,
+        out_specs=(HBM, VM, VM, HBM, VM, VM),
         scratch_shapes=[
             pltpu.VMEM((TOK, 2048), BF16),
             pltpu.VMEM((2048, 640), BF16),
-            pltpu.SemaphoreType.DMA((9,)),
+            pltpu.VMEM((PACK_ROWS, 256), BF16),
+            pltpu.VMEM((HALF, 256), BF16),
+            pltpu.VMEM((8, 128), F32),
+            pltpu.SemaphoreType.DMA((12,)),
         ],
         compiler_params=params(12),
         cost_estimate=cost(2 * TOK * 2048 * 640, 8 << 20),
@@ -424,7 +438,7 @@
     by_level(own, low_job, high_job)
     unpack_keys(packs, (2,), gates)
     near = table[own[0], 2, 0]
-    run_tiles(table, own, near, TILES - near, True, packs, query, gates, per_tile, m, l, acc)
+    run_tiles(table, own, near, table[own[0], 2, 1] - near, True, packs, query, gates, per_tile, m, l, acc)
     for n in range(2):
         total = jnp.maximum(l[n], TINY)
         o_own[n] = acc[n] / total
@@ -589,7 +603,7 @@
     )
     own = lax.axis_index("sp").astype(I32).reshape(1)
     table = jnp.asarray(work_table())
-    pkv, pxx, pr, pq, gated, tail = project(own, x, wq, wk, wv, wu, wg, gate.reshape(8, 128))
+    pkv, pxx, pr, pq, gated, tail = project(own, x, wq, wk, wv, wu, wg, in_hbm(gate.reshape(8, 128)))
     halo = lax.ppermute(tail, "sp", [(i, i + 1) for i in range(15)])
     x1 = lax.ppermute(pxx, "sp", moves(-1, 0))
     x3 = lax.ppermute(pxx, "sp", moves(-3, 0))

time: 108 us -> 106 us (0.981)
  local copies, waits for them, and re-layouts: 6.31 us -> 4.13 us
    unnamed x16 -> x10, local copies, waits for them, and re-layouts: 6.31 us -> 4.13 us
  transfers between devices with their start and end apart: 13 -> 13, of which waited for: 3 -> 3; matrix products, arithmetic and copies ran while one was open for 0% -> 0% of each run, Pallas kernels for 24% -> 25%
where the time goes in v7:
time: 106 us; the launch traced here: 105 us
  starting transfers between devices  54.2 us (51%)
  Pallas kernels  33.4 us (32%)
  waiting for transfers between devices  13.2 us (12%)
  local copies, waits for them, and re-layouts  4.13 us (4%)
    all_to_all x1, starting transfers between devices, layer(): conv_parts = lax.all_to_all(conv, 'tp', 0, 0, tiled=True)  17.3 us
    ppermute x1, waiting for transfers between devices, layer(): back_w = lax.ppermute(b2, 'sp', levels((1, 2), (0, 3)))  10.9 us
    pallas_call x1, Pallas kernels, attend_far(): pl.pallas_call(far_kernel, out_shape=arrays([((2, HALF, 128), F32)] * 2 +...  10.1 us
    ppermute x1, starting transfers between devices, layer(): back_w = lax.ppermute(b2, 'sp', levels((1, 2), (0, 3)))  8.68 us
    pallas_call x1, Pallas kernels, attend_near(): pl.pallas_call(near_kernel, out_shape=arrays(STATE + SLOTS), in_specs=[SM...  8.15 us
    ppermute x1, starting transfers between devices, layer(): turned = lax.ppermute(pr, 'sp', levels((0, 2), (2, 3), (3, 1), (1, 0)))  6.93 us
    pallas_call x1, Pallas kernels, project(): pl.pallas_call(project_kernel, out_shape=(pltpu.HBM((PACK_ROWS, 256), BF1...  6 us
    all_to_all x1, starting transfers between devices, layer(): attn_parts = lax.all_to_all(mixed, 'tp', 0, 0, tiled=True)  4.9 us
  transfers between devices with their start and end apart: 13, of which 3 were waited for; matrix products, arithmetic and copies ran while one was open for 0% of the time, Pallas kernels for 25%

profile of v7, /device:TPU:1, one launch (start us, length us, event | category | flops | bytes accessed | tf_op | source)
XLA Modules:
  0.0 105.0 jit_solution(13658967475532873904)
XLA Ops:
  0.0 6.0 %project.1 = (bf16[1040,256]{1,0:T(8,128)(2,1)}, bf16[1040,256]{1,0:T(8,128)(2,1)S(1)}, bf16[1040,256]{1,0:T(8,128)(2,1)S(1)}, bf16[512,256]{1,0:T(8,128)(2,1)},...) custom-call(s32[1]{0:T(128)} %bitcast.own, bf16[1024,2048]{1,0:T(8,128)(2,1)} %x_hbm.1, bf16[2048,128]{1,0:T(8,128)(2,1)} %wq.1, ...), custom_call_target="tpu_custom_call" | custom-call | flops 2684354560 | bytes 8388608 | tf_op jit(solution)/shard_map/project/pallas_call | solution.py:180
  6.0 3.4 %collective-permute-start.2 = (bf16[1040,256]{1,0:T(8,128)(2,1)S(1)}, bf16[1040,256]{1,0:T(8,128)(2,1)S(1)}, u32[]{:S(2)}, u32[]{:S(2)}) collective-permute-start(bf16[1040,256]{1,0:T(8,128)(2,1)S(1)} %get-tuple-element.24), channel_id=1, source_target_pairs={{0,24},{8,0},{16,8},{24,16},{32,56},{40,32},{48,40},{56,48},{64,88... | collective-permute-start | bytes 1597448 | tf_op jit(solution)/shard_map/ppermute | solution.py:608
  9.4 3.8 %collective-permute-start.4 = (bf16[1040,256]{1,0:T(8,128)(2,1)S(1)}, bf16[1040,256]{1,0:T(8,128)(2,1)}, u32[]{:S(2)}, u32[]{:S(2)}) collective-permute-start(bf16[1040,256]{1,0:T(8,128)(2,1)S(1)} %get-tuple-element.24), channel_id=1, source_target_pairs={{0,96},{8,104},{16,112},{24,120},{32,64},{40,72},{48,80},{56,88},{... | collective-permute-start | bytes 1597448 | tf_op jit(solution)/shard_map/ppermute | solution.py:611
  13.2 2.1 %collective-permute-start.10 = (bf16[32,128]{1,0:T(8,128)(2,1)S(1)}, bf16[32,128]{1,0:T(8,128)(2,1)S(1)}, u32[]{:S(2)}, u32[]{:S(2)}) collective-permute-start(bf16[32,128]{1,0:T(8,128)(2,1)S(1)} %get-tuple-element.40), channel_id=1, source_target_pairs={{0,8},{8,16},{16,24},{24,32},{32,40},{40,48},{48,56},{56,64},{64,7... | collective-permute-start | bytes 24584 | tf_op jit(solution)/shard_map/ppermute | solution.py:607
  15.3 3.7 %collective-permute-start = (bf16[1040,256]{1,0:T(8,128)(2,1)S(1)}, bf16[1040,256]{1,0:T(8,128)(2,1)S(1)}, u32[]{:S(2)}, u32[]{:S(2)}) collective-permute-start(bf16[1040,256]{1,0:T(8,128)(2,1)S(1)} %get-tuple-element.24), channel_id=1, source_target_pairs={{0,16},{8,24},{16,0},{24,8},{32,48},{40,56},{48,32},{56,40},{64,80... | collective-permute-start | bytes 1597448 | tf_op jit(solution)/shard_map/ppermute | solution.py:612
  19.0 1.3 %collective-permute-done.10.halo = bf16[32,128]{1,0:T(8,128)(2,1)S(1)} collective-permute-done((bf16[32,128]{1,0:T(8,128)(2,1)S(1)}, bf16[32,128]{1,0:T(8,128)(2,1)S(1)}, u32[]{:S(2)}, u32[]{:S(2)}) %collective-permute-start.10) | collective-permute-done | bytes 8224 | tf_op jit(solution)/shard_map/ppermute | solution.py:607
  20.3 6.9 %collective-permute-start.1 = (bf16[1040,256]{1,0:T(8,128)(2,1)S(1)}, bf16[1040,256]{1,0:T(8,128)(2,1)}, u32[]{:S(2)}, u32[]{:S(2)}) collective-permute-start(bf16[1040,256]{1,0:T(8,128)(2,1)S(1)} %get-tuple-element.25), channel_id=1, source_target_pairs={{0,64},{8,72},{16,80},{24,88},{64,96},{72,104},{80,112},{88,120},{... | collective-permute-start | bytes 1597448 | tf_op jit(solution)/shard_map/ppermute | solution.py:610
  27.3 2.2 %convolve.1 = f32[8,136,128]{2,1,0:T(8,128)} custom-call(bf16[1024,128]{1,0:T(8,128)(2,1)S(1)} %get-tuple-element.39.gated, bf16[32,128]{1,0:T(8,128)(2,1)S(1)} %collective-permute-done.10.halo, f32[31,128]{1,0:T(8,128)S(1)} %copy-done.2, f32[1,128]{1,0:T(1,128)S(1)} %bitcast.3), custom_call_target="tpu_custom_call" | custom-call | flops 520093696 | bytes 1048576 | tf_op jit(solution)/shard_map/convolve/pallas_call | solution.py:227
  29.5 17.3 %all-to-all-start.1 = ((f32[8,136,128]{2,1,0:T(8,128)}), f32[8,136,128]{2,1,0:T(8,128)S(1)}, u32[]{:S(2)}, u32[]{:S(2)}) async-start(f32[8,136,128]{2,1,0:T(8,128)} %convolve.1), calls=%async_computation.1 | async-start | bytes 1114112 | tf_op jit(solution)/shard_map/all_to_all | solution.py:614
  46.9 8.2 %attend_near.1 = (f32[8,512,128]{2,1,0:T(8,128)S(1)}, f32[8,512,128]{2,1,0:T(8,128)S(1)}, f32[8,512,128]{2,1,0:T(8,128)S(1)}, bf16[4,1040,256]{2,1,0:T(8,128)(2,...) custom-call(s32[16,3,18]{2,1,0:T(4,128)S(1)} %copy-done.4, s32[1]{0:T(128)} %bitcast.own, ...), custom_call_target="tpu_custom_call" | custom-call | flops 3221225472 | bytes 8388608 | tf_op jit(solution)/shard_map/attend_near/pallas_call | solution.py:467
  55.1 10.1 %attend_far.1 = (f32[2,512,128]{2,1,0:T(8,128)S(1)}, f32[2,512,128]{2,1,0:T(8,128)S(1)}, bf16[1056,128]{1,0:T(8,128)(2,1)S(1)}, bf16[1056,128]{1,0:T(8,128)(2,1)S(1)}, bf16[1056,128]{1,0:T(8,128)(2,1)S(1)}) custom-call(s32[16,3,18]{2,1,0:T(4,128)S(1)} %copy-done.4, s32[1]{0:T(128)} %bitcast.own, bf16[1040,256]{1,0:T(8,128)(2,1)S(1)} %collective-permute-done.x2, ...), custom_call_target="tpu_custom_call" | custom-call | flops 5368709120 | bytes 8388608 | tf_op jit(solution)/shard_map/attend_far/pallas_call | solution.py:480
  65.1 0.7 collective-permute-start.5
  65.8 0.7 collective-permute-start.6
  66.5 0.7 collective-permute-start.7
  67.2 1.3 %collective-permute-start.8 = (bf16[1056,128]{1,0:T(8,128)(2,1)S(1)}, bf16[1056,128]{1,0:T(8,128)(2,1)S(1)}, u32[]{:S(2)}, u32[]{:S(2)}) collective-permute-start(bf16[1056,128]{1,0:T(8,128)(2,1)S(1)} %get-tuple-element.36), channel_id=1, source_target_pairs={{0,32},{8,40},{16,48},{24,56},{32,96},{40,104},{48,112},{56,120},{... | collective-permute-start | bytes 811016 | tf_op jit(solution)/shard_map/ppermute | solution.py:622
  68.5 8.7 %collective-permute-start.9 = (bf16[1056,128]{1,0:T(8,128)(2,1)S(1)}, bf16[1056,128]{1,0:T(8,128)(2,1)S(1)}, u32[]{:S(2)}, u32[]{:S(2)}) collective-permute-start(bf16[1056,128]{1,0:T(8,128)(2,1)S(1)} %get-tuple-element.37), channel_id=1, source_target_pairs={{32,64},{40,72},{48,80},{56,88},{0,96},{8,104},{16,112},{24,120},{... | collective-permute-start | bytes 811016 | tf_op jit(solution)/shard_map/ppermute | solution.py:623
  77.2 10.9 %collective-permute-done.9.w = bf16[1056,128]{1,0:T(8,128)(2,1)S(1)} collective-permute-done((bf16[1056,128]{1,0:T(8,128)(2,1)S(1)}, bf16[1056,128]{1,0:T(8,128)(2,1)S(1)}, u32[]{:S(2)}, u32[]{:S(2)}) %collective-permute-start.9) | collective-permute-done | bytes 270368 | tf_op jit(solution)/shard_map/ppermute | solution.py:623
  88.2 1.8 %combine.1 = bf16[8,128,128]{2,1,0:T(8,128)(2,1)} custom-call(s32[1]{0:T(128)} %bitcast.own, f32[2,512,128]{2,1,0:T(8,128)S(1)} %get-tuple-element.34.o_own, f32[2,512,128]{2,1,0:T(8,128)S(1)} %get-tuple-element.35.lse_own, bf16[1056,128]{1,0:T(8,128)(2,1)S(1)} %collective-permute-done.5.x1, bf16[1056,128]{1,0:T(8,128)(2,1)S(1)} %collective-permute-done.6.x2, ...), custom_call_target="tpu_custom_call" | custom-call | flops 536870912 | bytes 2097152 | tf_op jit(solution)/shard_map/combine/pallas_call | solution.py:515
  90.0 4.9 %all-to-all-start = ((bf16[8,128,128]{2,1,0:T(8,128)(2,1)}), bf16[8,128,128]{2,1,0:T(8,128)(2,1)S(1)}, u32[]{:S(2)}, u32[]{:S(2)}) async-start(bf16[8,128,128]{2,1,0:T(8,128)(2,1)} %combine.1), calls=%async_computation | async-start | bytes 524288 | tf_op jit(solution)/shard_map/all_to_all | solution.py:626
  94.9 3.6 %conv_out.1 = (f32[128,2048]{1,0:T(8,128)S(1)}, bf16[1024,2048]{1,0:T(8,128)(2,1)S(1)}) custom-call(f32[8,136,128]{2,1,0:T(8,128)S(1)} %all-to-all-done.1.parts, bf16[2048,2048]{1,0:T(8,128)(2,1)} %w_hbm.1), custom_call_target="tpu_custom_call" | custom-call | flops 2147483648 | bytes 6291456 | tf_op jit(solution)/shard_map/conv_out/pallas_call | solution.py:552
  98.5 1.9 %copy-done = bf16[1024,2048]{1,0:T(8,128)(2,1)} copy-done((bf16[1024,2048]{1,0:T(8,128)(2,1)}, bf16[1024,2048]{1,0:T(8,128)(2,1)S(1)}, u32[]{:S(2)}) %copy-start) | copy-done | bytes 4194328
  100.4 1.0 all-to-all-done.parts
  101.3 2.2 %copy-done.1 = bf16[1024,2048]{1,0:T(8,128)(2,1)S(1)} copy-done((bf16[1024,2048]{1,0:T(8,128)(2,1)S(1)}, bf16[1024,2048]{1,0:T(8,128)(2,1)}, u32[]{:S(2)}) %copy-start.1) | copy-done | bytes 4194328
  103.5 1.5 %attn_out.1 = bf16[128,2048]{1,0:T(8,128)(2,1)} custom-call(bf16[8,128,128]{2,1,0:T(8,128)(2,1)S(1)} %all-to-all-done.parts, f32[128,2048]{1,0:T(8,128)S(1)} %get-tuple-element.41.conv, bf16[1024,2048]{1,0:T(8,128)(2,1)S(1)} %copy-done.1), custom_call_target="tpu_custom_call" | custom-call | flops 2147483648 | bytes 6291456 | tf_op jit(solution)/shard_map/attn_out/pallas_call | solution.py:580
  (19 shorter events, 0.0 us)
Async XLA Ops:
  0.0 27.3 %copy-start.2 = (f32[31,128]{1,0:T(8,128)S(1)}, f32[31,128]{1,0:T(8,128)}, u32[]{:S(2)}) copy-start(f32[31,128]{1,0:T(8,128)} %taps.1) | copy-start | bytes 47620
  0.0 27.3 %copy-start.3 = (f32[128]{0:T(128)S(1)}, f32[128]{0:T(128)}, u32[]{:S(2)}) copy-start(f32[128]{0:T(128)} %param.18) | copy-start | bytes 1540
  6.0 40.9 %copy-start.4 = (s32[16,3,18]{2,1,0:T(4,128)S(1)}, s32[16,3,18]{2,1,0:T(4,128)}, u32[]{:S(2)}) copy-start(s32[16,3,18]{2,1,0:T(4,128)} %constant.8.clone.table) | copy-start | bytes 10372
  6.0 40.8 %collective-permute-start.2 = (bf16[1040,256]{1,0:T(8,128)(2,1)S(1)}, bf16[1040,256]{1,0:T(8,128)(2,1)S(1)}, u32[]{:S(2)}, u32[]{:S(2)}) collective-permute-start(bf16[1040,256]{1,0:T(8,128)(2,1)S(1)} %get-tuple-element.24), channel_id=1, source_target_pairs={{0,24},{8,0},{16,8},{24,16},{32,56},{40,32},{48,40},{56,48},{64,88... | collective-permute-start | bytes 1597448 | tf_op jit(solution)/shard_map/ppermute | solution.py:608
  9.4 37.5 %collective-permute-start.3 = (bf16[1040,256]{1,0:T(8,128)(2,1)S(1)}, bf16[1040,256]{1,0:T(8,128)(2,1)S(1)}, u32[]{:S(2)}, u32[]{:S(2)}) collective-permute-start(bf16[1040,256]{1,0:T(8,128)(2,1)S(1)} %get-tuple-element.24), channel_id=1, source_target_pairs={{0,8},{8,16},{16,24},{24,0},{32,40},{40,48},{48,56},{56,32},{64,72... | collective-permute-start | bytes 1597448 | tf_op jit(solution)/shard_map/ppermute | solution.py:609
  9.4 37.5 %collective-permute-start.4 = (bf16[1040,256]{1,0:T(8,128)(2,1)S(1)}, bf16[1040,256]{1,0:T(8,128)(2,1)}, u32[]{:S(2)}, u32[]{:S(2)}) collective-permute-start(bf16[1040,256]{1,0:T(8,128)(2,1)S(1)} %get-tuple-element.24), channel_id=1, source_target_pairs={{0,96},{8,104},{16,112},{24,120},{32,64},{40,72},{48,80},{56,88},{... | collective-permute-start | bytes 1597448 | tf_op jit(solution)/shard_map/ppermute | solution.py:611
  13.2 7.2 %collective-permute-start.10 = (bf16[32,128]{1,0:T(8,128)(2,1)S(1)}, bf16[32,128]{1,0:T(8,128)(2,1)S(1)}, u32[]{:S(2)}, u32[]{:S(2)}) collective-permute-start(bf16[32,128]{1,0:T(8,128)(2,1)S(1)} %get-tuple-element.40), channel_id=1, source_target_pairs={{0,8},{8,16},{16,24},{24,32},{32,40},{40,48},{48,56},{56,64},{64,7... | collective-permute-start | bytes 24584 | tf_op jit(solution)/shard_map/ppermute | solution.py:607
  15.3 39.8 %collective-permute-start = (bf16[1040,256]{1,0:T(8,128)(2,1)S(1)}, bf16[1040,256]{1,0:T(8,128)(2,1)S(1)}, u32[]{:S(2)}, u32[]{:S(2)}) collective-permute-start(bf16[1040,256]{1,0:T(8,128)(2,1)S(1)} %get-tuple-element.24), channel_id=1, source_target_pairs={{0,16},{8,24},{16,0},{24,8},{32,48},{40,56},{48,32},{56,40},{64,80... | collective-permute-start | bytes 1597448 | tf_op jit(solution)/shard_map/ppermute | solution.py:612
  20.3 34.7 %collective-permute-start.1 = (bf16[1040,256]{1,0:T(8,128)(2,1)S(1)}, bf16[1040,256]{1,0:T(8,128)(2,1)}, u32[]{:S(2)}, u32[]{:S(2)}) collective-permute-start(bf16[1040,256]{1,0:T(8,128)(2,1)S(1)} %get-tuple-element.25), channel_id=1, source_target_pairs={{0,64},{8,72},{16,80},{24,88},{64,96},{72,104},{80,112},{88,120},{... | collective-permute-start | bytes 1597448 | tf_op jit(solution)/shard_map/ppermute | solution.py:610
  29.5 60.4 %all-to-all-start.1 = ((f32[8,136,128]{2,1,0:T(8,128)}), f32[8,136,128]{2,1,0:T(8,128)S(1)}, u32[]{:S(2)}, u32[]{:S(2)}) async-start(f32[8,136,128]{2,1,0:T(8,128)} %convolve.1), calls=%async_computation.1 | async-start | bytes 1114112 | tf_op jit(solution)/shard_map/all_to_all | solution.py:614
  65.1 12.1 %collective-permute-start.5 = (bf16[1056,128]{1,0:T(8,128)(2,1)S(1)}, bf16[1056,128]{1,0:T(8,128)(2,1)S(1)}, u32[]{:S(2)}, u32[]{:S(2)}) collective-permute-start(bf16[1056,128]{1,0:T(8,128)(2,1)S(1)} %get-tuple-element.36), channel_id=1, source_target_pairs={{64,72},{72,80},{80,88},{88,64},{96,104},{104,112},{112,120},{120,... | collective-permute-start | bytes 811016 | tf_op jit(solution)/shard_map/ppermute | solution.py:619
  65.8 11.4 %collective-permute-start.6 = (bf16[1056,128]{1,0:T(8,128)(2,1)S(1)}, bf16[1056,128]{1,0:T(8,128)(2,1)S(1)}, u32[]{:S(2)}, u32[]{:S(2)}) collective-permute-start(bf16[1056,128]{1,0:T(8,128)(2,1)S(1)} %get-tuple-element.37), channel_id=1, source_target_pairs={{64,80},{72,88},{80,64},{88,72},{96,112},{104,120},{112,96},{120,1... | collective-permute-start | bytes 811016 | tf_op jit(solution)/shard_map/ppermute | solution.py:621
  66.5 10.7 %collective-permute-start.7 = (bf16[1056,128]{1,0:T(8,128)(2,1)S(1)}, bf16[1056,128]{1,0:T(8,128)(2,1)S(1)}, u32[]{:S(2)}, u32[]{:S(2)}) collective-permute-start(bf16[1056,128]{1,0:T(8,128)(2,1)S(1)} %get-tuple-element.38), channel_id=1, source_target_pairs={{64,88},{72,64},{80,72},{88,80},{96,120},{104,96},{112,104},{120,1... | collective-permute-start | bytes 811016 | tf_op jit(solution)/shard_map/ppermute | solution.py:620
  67.2 10.0 %collective-permute-start.8 = (bf16[1056,128]{1,0:T(8,128)(2,1)S(1)}, bf16[1056,128]{1,0:T(8,128)(2,1)S(1)}, u32[]{:S(2)}, u32[]{:S(2)}) collective-permute-start(bf16[1056,128]{1,0:T(8,128)(2,1)S(1)} %get-tuple-element.36), channel_id=1, source_target_pairs={{0,32},{8,40},{16,48},{24,56},{32,96},{40,104},{48,112},{56,120},{... | collective-permute-start | bytes 811016 | tf_op jit(solution)/shard_map/ppermute | solution.py:622
  68.5 19.6 %collective-permute-start.9 = (bf16[1056,128]{1,0:T(8,128)(2,1)S(1)}, bf16[1056,128]{1,0:T(8,128)(2,1)S(1)}, u32[]{:S(2)}, u32[]{:S(2)}) collective-permute-start(bf16[1056,128]{1,0:T(8,128)(2,1)S(1)} %get-tuple-element.37), channel_id=1, source_target_pairs={{32,64},{40,72},{48,80},{56,88},{0,96},{8,104},{16,112},{24,120},{... | collective-permute-start | bytes 811016 | tf_op jit(solution)/shard_map/ppermute | solution.py:623
  90.0 11.4 %all-to-all-start = ((bf16[8,128,128]{2,1,0:T(8,128)(2,1)}), bf16[8,128,128]{2,1,0:T(8,128)(2,1)S(1)}, u32[]{:S(2)}, u32[]{:S(2)}) async-start(bf16[8,128,128]{2,1,0:T(8,128)(2,1)} %combine.1), calls=%async_computation | async-start | bytes 524288 | tf_op jit(solution)/shard_map/all_to_all | solution.py:626
  98.5 1.9 %copy-start = (bf16[1024,2048]{1,0:T(8,128)(2,1)}, bf16[1024,2048]{1,0:T(8,128)(2,1)S(1)}, u32[]{:S(2)}) copy-start(bf16[1024,2048]{1,0:T(8,128)(2,1)S(1)} %get-tuple-element.42.w) | copy-start | bytes 12582916
  101.3 2.2 %copy-start.1 = (bf16[1024,2048]{1,0:T(8,128)(2,1)S(1)}, bf16[1024,2048]{1,0:T(8,128)(2,1)}, u32[]{:S(2)}) copy-start(bf16[1024,2048]{1,0:T(8,128)(2,1)} %copy-done) | copy-start | bytes 12582916
